TPU v7x, 512 devices: a whole 4x8x8 slice. The times are simulated.
512 devices in a mesh: gr: 2 (over z_hi), fs: 32 (over z_lo, y), tp: 8 (over x, core).
Axes of the slice: x: 4, y: 8, z: 8 (z_hi: 2, z_lo: 4; z = z_hi * 4 + z_lo), core: 2. Of those that a mesh axis runs over, the one named last changes fastest.
Arguments:
- prompt: bfloat16 [8192, 2048], P(('gr', 'fs')), may hold values from -6 to 6
- expert_ids: int32 [8192, 2], P(('gr', 'fs')), may hold values from 0 to 7, all different within a row; in each aligned block of 128 rows (0 to 127, 128 to 255, ...) at most 32 rows name the same one
- route_weights: float32 [8192, 2], P(('gr', 'fs')), may hold values from 0.2 to 1
- gate_master: float32 [8, 2048, 8192], P('gr', 'fs', 'tp'), may hold values from -0.125 to 0.125
- up_master: float32 [8, 2048, 8192], P('gr', 'fs', 'tp'), may hold values from -0.125 to 0.125
- down_master: float32 [8, 8192, 2048], P('gr', 'fs', 'tp'), may hold values from -0.0625 to 0.0625
- ffn_gain: float32 [2048], P('fs'), may hold values from 0.1 to 1.9
Outputs:
- gate_serving: bfloat16 [8, 2048, 8192], P('tp', None, 'fs')
- up_serving: bfloat16 [8, 2048, 8192], P('tp', None, 'fs')
- down_serving: bfloat16 [8, 8192, 2048], P('tp', 'fs')
- mixed: bfloat16 [8192, 2048], P(('gr', 'fs', 'tp'))
Inputs may be any that keep to these rules, and one draw needn't show every extreme that they name: `expert_ids`: the two experts of a token differ; the rows of one index of gr and fs name each expert exactly 32 times.
All inputs are finite; a program needn't handle non-finite values.
Results may differ from a plain program's by a relative error of at most 0.025.
Values may be sent and summed in bfloat16 or wider, within the bound.
No kernel may reach another device: no remote copies, remote signals or barrier semaphores. Data moves between devices by JAX's collectives and lax.ppermute only.
A program may use at most 64 MiB of HBM per device.

v0:
```python
import jax
import jax.numpy as jnp
from jax import lax
from jax.experimental import pallas as pl
from jax.experimental.pallas import tpu as pltpu
from jax.sharding import Mesh
from jax.sharding import PartitionSpec as P


SLOTS = 32
NORM_EPS = 1e-06
FS = ("zl", "y")
TP = ("xh", "xl", "c")


def cut_kernel(gain_ref, gate_ref, up_ref, out_ref):
    width = out_ref.shape[-1]
    gain = gain_ref[...]
    for i, w_ref in enumerate((gate_ref, up_ref)):
        for j in range(out_ref.shape[2]):
            cols = w_ref[0, :, j * width : (j + 1) * width]
            out_ref[0, i, j, 0] = (cols * gain).astype(jnp.bfloat16)


def cut(gate, up, gain):
    _, rows, width = gate.shape
    cols = width // 4
    weights = pl.BlockSpec((1, rows, width), lambda e: (e, 0, 0))
    return pl.pallas_call(
        cut_kernel,
        grid=(4,),
        in_specs=[pl.BlockSpec((rows, 1), lambda e: (0, 0)), weights, weights],
        out_specs=pl.BlockSpec((1, 2, 4, 1, rows, cols), lambda e: (e % 2, 0, 0, e // 2, 0, 0)),
        out_shape=jax.ShapeDtypeStruct((2, 2, 4, 2, rows, cols), jnp.bfloat16),
        name="cut",
    )(gain, gate, up)


def slots_of(ids, expert):
    tokens = ids.shape[1]
    chosen = (ids[0:1] == expert) | (ids[1:2] == expert)
    before = lax.broadcasted_iota(jnp.int32, (tokens, tokens), 0) < lax.broadcasted_iota(
        jnp.int32, (tokens, tokens), 1
    )
    place = jnp.dot(
        chosen.astype(jnp.float32), before.astype(jnp.float32), preferred_element_type=jnp.float32
    ).astype(jnp.int32)
    slot = lax.broadcasted_iota(jnp.int32, (SLOTS, tokens), 0)
    return (place == slot) & chosen


def dispatch_kernel(expert_ref, ids_ref, prompt_ref, out_ref):
    x = prompt_ref[...].astype(jnp.float32)
    scale = lax.rsqrt(jnp.mean(x * x, axis=1, keepdims=True) + NORM_EPS)
    normed = (x * scale).astype(jnp.bfloat16)
    pick = slots_of(ids_ref[...], expert_ref[0]).astype(jnp.bfloat16)
    rows = jnp.dot(pick, normed, preferred_element_type=jnp.float32).astype(jnp.bfloat16)
    for z in range(out_ref.shape[0]):
        out_ref[z] = rows


def dispatch(expert, ids, prompt, copies):
    return pl.pallas_call(
        dispatch_kernel,
        in_specs=[
            pl.BlockSpec(memory_space=pltpu.SMEM),
            pl.BlockSpec(memory_space=pltpu.VMEM),
            pl.BlockSpec(memory_space=pltpu.VMEM),
        ],
        out_specs=pl.BlockSpec(memory_space=pltpu.VMEM),
        out_shape=jax.ShapeDtypeStruct((copies, SLOTS, prompt.shape[1]), jnp.bfloat16),
        name="dispatch",
    )(expert, ids, prompt)


def combine_kernel(expert_ref, ids_ref, weights_ref, parts_ref, out_ref):
    pick = slots_of(ids_ref[...], expert_ref[0])
    w = jnp.where(ids_ref[0:1] == expert_ref[0], weights_ref[0:1], weights_ref[1:2])
    slot_weight = jnp.sum(jnp.where(pick, w, 0.0), axis=1, keepdims=True)
    total = parts_ref[0].astype(jnp.float32)
    for z in range(1, parts_ref.shape[0]):
        total = total + parts_ref[z].astype(jnp.float32)
    term = (total * slot_weight).astype(jnp.bfloat16)
    out_ref[...] = lax.dot_general(
        pick.astype(jnp.bfloat16),
        term,
        (((0,), (0,)), ((), ())),
        preferred_element_type=jnp.float32,
    ).astype(jnp.bfloat16)


def combine(expert, ids, weights, parts):
    return pl.pallas_call(
        combine_kernel,
        in_specs=[
            pl.BlockSpec(memory_space=pltpu.SMEM),
            pl.BlockSpec(memory_space=pltpu.VMEM),
            pl.BlockSpec(memory_space=pltpu.VMEM),
            pl.BlockSpec(memory_space=pltpu.VMEM),
        ],
        out_specs=pl.BlockSpec(memory_space=pltpu.VMEM),
        out_shape=jax.ShapeDtypeStruct((ids.shape[1], parts.shape[2]), jnp.bfloat16),
        name="combine",
    )(expert, ids, weights, parts)


def place_kernel(at_ref, *refs):
    *pieces, out_ref = refs
    for k, piece in enumerate(pieces):
        out_ref[k ^ at_ref[0]] = piece[...]


def place(at, pieces):
    return pl.pallas_call(
        place_kernel,
        in_specs=[pl.BlockSpec(memory_space=pltpu.SMEM)]
        + [pl.BlockSpec(memory_space=pltpu.VMEM)] * len(pieces),
        out_specs=pl.BlockSpec(memory_space=pltpu.VMEM),
        out_shape=jax.ShapeDtypeStruct((len(pieces), *pieces[0].shape), jnp.bfloat16),
        name="place",
    )(at, *pieces)


def place_cols_kernel(at_ref, blocks_ref, out_ref):
    out_ref[...] = blocks_ref[0, 0]


def place_cols(at, blocks):
    parts, pieces, rows, width = blocks.shape
    return pl.pallas_call(
        place_cols_kernel,
        grid_spec=pltpu.PrefetchScalarGridSpec(
            num_scalar_prefetch=1,
            grid=(pieces, parts),
            in_specs=[pl.BlockSpec((1, 1, rows, width), lambda k, i, at: (i, k, 0, 0))],
            out_specs=pl.BlockSpec((rows, width), lambda k, i, at: (0, (k ^ at[0]) * parts + i)),
        ),
        out_shape=jax.ShapeDtypeStruct((rows, pieces * parts * width), jnp.bfloat16),
        name="place_cols",
    )(at, blocks)


def exchange(value, axes):
    return lax.all_to_all(value, axes, split_axis=0, concat_axis=0, tiled=True)


def by_half(by_core, zl):
    _, _, _, rows, cols = by_core.shape
    by_y = exchange(by_core.reshape(16, rows, cols), ("y", "xl"))
    by_y = by_y.reshape(8, 2, rows, cols)
    own = lax.dynamic_index_in_dim(by_y, zl & 1, 1, keepdims=False).reshape(8 * rows, cols)
    other = lax.dynamic_index_in_dim(by_y, 1 - (zl & 1), 1, keepdims=False).reshape(8 * rows, cols)
    return own, other


def to_servers(own, other, zl, gr):
    pieces = []
    for k in range(4):
        pairs = []
        for g in range(2):
            for a in range(4):
                for p in range(2):
                    r, low = (k ^ a) >> 1, (k ^ a) & 1
                    pairs.append((g * 8 + a * 2 + p, r * 8 + (2 * p + low) * 2 + g))
        pieces.append(lax.ppermute(other if k & 1 else own, ("gr", "zl", "xh"), pairs))
    return place((2 * gr + (zl & 1)).reshape(1), pieces)


def down_to_servers(down, gr):
    pieces = []
    for k in range(2):
        pairs = [(g * 2 + p, (k ^ p) * 2 + g) for g in range(2) for p in range(2)]
        pieces.append(lax.ppermute(down, ("gr", "xh"), pairs))
    blocks = jnp.stack(pieces, axis=1)
    return place_cols(gr.reshape(1), exchange(blocks, ("xl", "c")))


def body(prompt, expert_ids, route_weights, gate_master, up_master, down_master, ffn_gain):
    gr, zl = lax.axis_index("gr"), lax.axis_index("zl")
    expert = lax.axis_index(TP).reshape(1)
    ids, weights = expert_ids.T, route_weights.T
    gain = ffn_gain[:, None]
    width = prompt.shape[1]

    routed = exchange(dispatch(expert, ids, prompt, lax.axis_size("zl")), "zl")
    down_serving = down_to_servers(down_master.astype(jnp.bfloat16), gr)
    blocks = cut(gate_master, up_master, gain)
    by_core = exchange(blocks, "c")
    own, other = by_half(by_core[:, 0], zl)
    own, other, up_blocks = lax.optimization_barrier((own, other, by_core[:, 1]))
    gate = to_servers(own, other, zl, gr)
    up = to_servers(*by_half(up_blocks, zl), zl, gr)
    gate_serving = gate.reshape(-1, gate.shape[-1])
    up_serving = up.reshape(-1, up.shape[-1])

    rows = lax.all_gather(routed, "y", axis=0, tiled=True).reshape(-1, width)
    gate_part = jnp.dot(rows, gate_serving, preferred_element_type=jnp.float32)
    up_part = jnp.dot(rows, up_serving, preferred_element_type=jnp.float32)
    hidden = (jax.nn.silu(gate_part) * up_part).astype(jnp.bfloat16)
    partial = jnp.dot(hidden, down_serving, preferred_element_type=jnp.float32).astype(jnp.bfloat16)
    partial = partial.reshape(-1, SLOTS, width)
    over_y = lax.psum_scatter(partial, "y", scatter_dimension=0, tiled=True)
    terms = combine(expert, ids, weights, exchange(over_y, "zl"))
    arrived = exchange(terms.reshape(lax.axis_size(TP), -1, width), TP)
    mixed = jnp.sum(arrived.astype(jnp.float32), axis=0).astype(jnp.bfloat16)
    return (gate_serving[None], up_serving[None], down_serving[None], mixed)


def solution(mesh):
    split = Mesh(
        mesh.devices.reshape(2, 4, 8, 2, 2, 2), ("gr", "zl", "y", "xh", "xl", "c")
    )
    placed = (
        P(("gr", *FS), None),
        P(("gr", *FS), None),
        P(("gr", *FS), None),
        P("gr", FS, TP),
        P("gr", FS, TP),
        P("gr", FS, TP),
        P(FS),
    )
    return jax.shard_map(
        body,
        mesh=split,
        in_specs=placed,
        out_specs=(P(TP, None, FS), P(TP, None, FS), P(TP, FS, None), P(("gr", *FS, *TP), None)),
        check_vma=False,
    )
```

profile of v0, /device:TPU:1, one launch (start us, length us, event | category | flops | bytes accessed | tf_op | source)
XLA Modules:
  0.0 316.5 jit_solution(13892923700495747470)
XLA Ops:
  7.2 0.0 all-gather.2.cloned.1.call-start
  7.2 2.3 dispatch.1
  9.5 20.8 %all_to_all.35 = bf16[4,32,2048]{2,1,0:T(8,128)(2,1)} all-to-all(bf16[4,32,2048]{2,1,0:T(8,128)(2,1)} %dispatch.1), channel_id=1, replica_groups=mesh['gr'=2,'zl'=4,'y'=8,'xh'=2,'xl'=2,'c'=2] {'zl'}, dimensions={0} | all-to-all | bytes 1048576 | tf_op jit(solution)/shard_map/all_to_all | solution.py:144
  30.3 0.0 all-gather.2.cloned.1.call-update
  30.3 1.4 copy.15.gain_ref
  31.7 3.7 %cut.1 = bf16[2,2,4,2,64,256]{5,4,3,2,1,0:T(8,128)(2,1)} custom-call(f32[64,1]{1,0:T(8,128)} %copy.15.gain_ref, f32[4,64,1024]{2,1,0:T(8,128)} %gate_ref.1, f32[4,64,1024]{2,1,0:T(8,128)} %up_ref.1), custom_call_target="tpu_custom_call" | custom-call | tf_op jit(solution)/shard_map/cut/pallas_call | solution.py:29
  35.4 0.0 copy-start.4
  35.4 8.0 %all_to_all.36 = bf16[2,2,4,2,64,256]{5,4,3,2,1,0:T(8,128)(2,1)S(1)} all-to-all(bf16[2,2,4,2,64,256]{5,4,3,2,1,0:T(8,128)(2,1)} %cut.1), channel_id=1, replica_groups=mesh['gr'=2,'zl'=4,'y'=8,'xh'=2,'xl'=2,'c'=2] {'c'}, dimensions={0} | all-to-all | bytes 2097152 | tf_op jit(solution)/shard_map/all_to_all | solution.py:144
  43.4 1.0 slice_bitcast_fusion
  44.4 7.8 %all-to-all-start.1 = ((bf16[16,64,256]{2,1,0:T(8,128)(2,1)}), bf16[16,64,256]{2,1,0:T(8,128)(2,1)S(1)}, u32[]{:S(2)}, u32[]{:S(2)}) async-start(bf16[16,64,256]{2,1,0:T(8,128)(2,1)} %bitcast.2), calls=%async_computation.1 | async-start | bytes 1048576 | tf_op jit(solution)/shard_map/all_to_all | solution.py:144
  52.3 22.5 %all-to-all-done.1 = bf16[16,64,256]{2,1,0:T(8,128)(2,1)S(1)} async-done(((bf16[16,64,256]{2,1,0:T(8,128)(2,1)}), bf16[16,64,256]{2,1,0:T(8,128)(2,1)S(1)}, u32[]{:S(2)}, u32[]{:S(2)}) %all-to-all-start.1) | async-done | bytes 524320 | tf_op jit(solution)/shard_map/all_to_all | solution.py:144
  74.8 3.6 %all-to-all-start.2 = ((bf16[16,64,256]{2,1,0:T(8,128)(2,1)}), bf16[16,64,256]{2,1,0:T(8,128)(2,1)S(1)}, u32[]{:S(2)}, u32[]{:S(2)}) async-start(bf16[16,64,256]{2,1,0:T(8,128)(2,1)} %bitcast.8), calls=%async_computation.2 | async-start | bytes 1048576 | tf_op jit(solution)/shard_map/all_to_all | solution.py:144
  78.5 0.0 copy-done.4
  78.5 0.1 convert_element_type.11
  78.6 7.9 %collective-permute-start.9 = (bf16[4,256,256]{2,1,0:T(8,128)(2,1)S(1)}, bf16[4,256,256]{2,1,0:T(8,128)(2,1)S(1)}, u32[]{:S(2)}, u32[]{:S(2)}) collective-permute-start(bf16[4,256,256]{2,1,0:T(8,128)(2,1)S(1)} %convert_element_type.11), channel_id=1, source_target_pairs={{0,256},{4,0},{256,260},{260,4},{1,257},{5,1},{257,261},{261,5},{2... | collective-permute-start | bytes 1572872 | tf_op jit(solution)/shard_map/ppermute | solution.py:173
  86.5 0.7 collective-permute-start.8
  87.2 22.5 %collective-permute-done.9 = bf16[4,256,256]{2,1,0:T(8,128)(2,1)S(1)} collective-permute-done((bf16[4,256,256]{2,1,0:T(8,128)(2,1)S(1)}, bf16[4,256,256]{2,1,0:T(8,128)(2,1)S(1)}, u32[]{:S(2)}, u32[]{:S(2)}) %collective-permute-start.9) | collective-permute-done | bytes 524320 | tf_op jit(solution)/shard_map/ppermute | solution.py:173
  109.7 0.0 collective-permute-done.8
  109.7 1.1 pad_maximum_fusion
  110.8 0.0 all-to-all-done.2
  110.8 6.1 %all-to-all-start.3 = ((bf16[4,2,256,256]{3,2,1,0:T(8,128)(2,1)}), bf16[4,2,256,256]{3,2,1,0:T(8,128)(2,1)S(1)}, u32[]{:S(2)}, u32[]{:S(2)}) async-start(bf16[4,2,256,256]{3,2,1,0:T(8,128)(2,1)} %pad_maximum_fusion), calls=%async_computation.3 | async-start | bytes 2097152 | tf_op jit(solution)/shard_map/all_to_all | solution.py:144
  116.9 0.0 reduce-scatter.2.cloned.1.call-start
  116.9 10.3 %collective-permute-start.2 = (bf16[512,256]{1,0:T(8,128)(2,1)S(1)}, bf16[512,256]{1,0:T(8,128)(2,1)S(1)}, u32[]{:S(2)}, u32[]{:S(2)}) collective-permute-start(bf16[512,256]{1,0:T(8,128)(2,1)S(1)} %bitcast.46), channel_id=1, source_target_pairs={{0,256},{4,384},{64,320},{68,448},{128,0},{132,128},{192,64},{196,... | collective-permute-start | bytes 786440 | tf_op jit(solution)/shard_map/ppermute | solution.py:165
  127.2 0.7 collective-permute-start
  127.9 10.1 %collective-permute-start.3 = (bf16[512,256]{1,0:T(8,128)(2,1)S(1)}, bf16[512,256]{1,0:T(8,128)(2,1)S(1)}, u32[]{:S(2)}, u32[]{:S(2)}) collective-permute-start(bf16[512,256]{1,0:T(8,128)(2,1)S(1)} %bitcast.44), channel_id=1, source_target_pairs={{0,320},{4,448},{64,256},{68,384},{128,64},{132,192},{192,0},{196,... | collective-permute-start | bytes 786440 | tf_op jit(solution)/shard_map/ppermute | solution.py:165
  138.1 3.8 %collective-permute-start.1 = (bf16[512,256]{1,0:T(8,128)(2,1)S(1)}, bf16[512,256]{1,0:T(8,128)(2,1)}, u32[]{:S(2)}, u32[]{:S(2)}) collective-permute-start(bf16[512,256]{1,0:T(8,128)(2,1)S(1)} %bitcast.45), channel_id=1, source_target_pairs={{0,64},{4,192},{64,0},{68,128},{128,320},{132,448},{192,256},{196,... | collective-permute-start | bytes 786440 | tf_op jit(solution)/shard_map/ppermute | solution.py:165
  141.8 0.1 constant_dynamic-slice_fusion
  141.9 1.9 collective-permute-start.6
  143.8 0.0 collective-permute-done.2.refs_2_
  143.8 0.0 copy-start.6
  143.9 0.7 collective-permute-start.4
  144.5 0.0 collective-permute-done.refs_0_
  144.5 0.0 copy-start.8
  144.6 30.6 %collective-permute-start.7 = (bf16[512,256]{1,0:T(8,128)(2,1)S(1)}, bf16[512,256]{1,0:T(8,128)(2,1)}, u32[]{:S(2)}, u32[]{:S(2)}) collective-permute-start(bf16[512,256]{1,0:T(8,128)(2,1)S(1)} %bitcast.48), channel_id=1, source_target_pairs={{0,320},{4,448},{64,256},{68,384},{128,64},{132,192},{192,0},{196,... | collective-permute-start | bytes 786440 | tf_op jit(solution)/shard_map/ppermute | solution.py:165
  175.1 0.0 collective-permute-done.3.refs_3_
  175.1 0.0 copy-done.8
  175.2 0.0 copy-start.9
  175.2 0.7 copy-done.9
  175.9 1.9 collective-permute-start.5
  177.8 0.0 collective-permute-done.1.refs_1_
  177.8 0.0 copy-done.6
  177.8 2.2 place.2
  180.0 0.0 all-to-all-done.3.blocks_ref
  180.0 1.0 copy-done
  181.0 5.2 %place_cols.1 = bf16[256,2048]{1,0:T(8,128)(2,1)} custom-call(s32[1]{0:T(128)} %bitcast.13.at_ref, bf16[4,2,256,256]{3,2,1,0:T(8,128)(2,1)} %copy-done), custom_call_target="tpu_custom_call" | custom-call | tf_op jit(solution)/shard_map/place_cols/pallas_call | solution.py:130
  186.2 0.0 collective-permute-done.6.refs_2_
  186.2 0.0 collective-permute-done.4.refs_0_
  186.2 0.0 copy-start.7
  186.2 4.6 %collective-permute-done.7.refs_3_ = bf16[512,256]{1,0:T(8,128)(2,1)} collective-permute-done((bf16[512,256]{1,0:T(8,128)(2,1)S(1)}, bf16[512,256]{1,0:T(8,128)(2,1)}, u32[]{:S(2)}, u32[]{:S(2)}) %collective-permute-start.7) | collective-permute-done | bytes 262176 | tf_op jit(solution)/shard_map/ppermute | solution.py:165
  190.8 0.0 collective-permute-done.5.refs_1_
  190.8 0.0 copy-done.5
  190.8 0.0 copy-done.7
  190.8 2.2 place.3
  193.0 0.0 copy-done.1
  193.1 4.6 %fusion.4 = f32[1024,256]{1,0:T(8,128)} fusion(bf16[1024,2048]{1,0:T(8,128)(2,1)} %bitcast.56, bf16[2048,256]{1,0:T(8,128)(2,1)S(1)} %bitcast.38), kind=kOutput, calls=%fused_computation.11 | convolution fusion | flops 1073741824 | bytes 6291456 | tf_op jit(solution)/shard_map/dot_general | solution.py:197
  197.7 0.0 copy-done.2
  197.7 0.0 copy-done.3
  197.7 8.9 %convolution_convert_fusion = bf16[1024,2048]{1,0:T(8,128)(2,1)} fusion(bf16[256,2048]{1,0:T(8,128)(2,1)S(1)} %copy-done.2, f32[1024,256]{1,0:T(8,128)} %fusion.4, bf16[1024,2048]{1,0:T(8,128)(2,1)} %bitcast.57, bf16[2048,256]{1,0:T(8,128)(2,1)S(1)} %bitcast.41), kind=kOutput, calls=%fused_computation | convolution fusion | flops 2151153664 | bytes 11534336 | tf_op jit(solution)/shard_map/dot_general | solution.py:200
  206.6 0.0 reduce-scatter.2.cloned.1.call-update
  206.6 66.1 %reduce-scatter.2.cloned.1.call-done = bf16[4,32,2048]{2,1,0:T(8,128)(2,1)} async-done(((bf16[32,32,2048]{2,1,0:T(8,128)(2,1)}), bf16[4,32,2048]{2,1,0:T(8,128)(2,1)}) %reduce-scatter.2.cloned.1.call-update) | async-done | bytes 524304 | tf_op jit(solution)/shard_map/reduce_scatter | solution.py:202
  272.7 18.5 %all_to_all.37.parts_ref = bf16[4,32,2048]{2,1,0:T(8,128)(2,1)} all-to-all(bf16[4,32,2048]{2,1,0:T(8,128)(2,1)} %reduce-scatter.2.cloned.1.call-done), channel_id=1, replica_groups=mesh['gr'=2,'zl'=4,'y'=8,'xh'=2,'xl'=2,'c'=2] {'zl'}, dimensions={0} | all-to-all | bytes 1048576 | tf_op jit(solution)/shard_map/all_to_all | solution.py:144
  291.2 2.4 combine.1
  293.6 15.4 %all_to_all.38 = bf16[8,16,2048]{2,1,0:T(8,128)(2,1)S(1)} all-to-all(bf16[8,16,2048]{2,1,0:T(8,128)(2,1)} %bitcast.36), channel_id=1, replica_groups=mesh['gr'=2,'zl'=4,'y'=8,'xh'=2,'xl'=2,'c'=2] {'xh','xl','c'}, dimensions={0} | all-to-all | bytes 1048576 | tf_op jit(solution)/shard_map/all_to_all | solution.py:144
  309.0 0.7 reduce_sum.12
  (7 shorter events, 0.1 us)
Async XLA Ops:
  7.2 185.9 %all-gather.2.cloned.1.call-start = ((), (), s32[]{:S(2)}) async-start(), calls=%async_computation.8 | async-start | bytes 4718592 | tf_op jit(solution)/shard_map/all_gather | solution.py:196
  35.4 43.1 %copy-start.4 = (f32[4,256,256]{2,1,0:T(8,128)S(1)}, f32[4,256,256]{2,1,0:T(8,128)}, u32[]{:S(2)}) copy-start(f32[4,256,256]{2,1,0:T(8,128)} %param.12) | copy-start | bytes 3145732
  44.4 30.4 %all-to-all-start.1 = ((bf16[16,64,256]{2,1,0:T(8,128)(2,1)}), bf16[16,64,256]{2,1,0:T(8,128)(2,1)S(1)}, u32[]{:S(2)}, u32[]{:S(2)}) async-start(bf16[16,64,256]{2,1,0:T(8,128)(2,1)} %bitcast.2), calls=%async_computation.1 | async-start | bytes 1048576 | tf_op jit(solution)/shard_map/all_to_all | solution.py:144
  74.8 35.9 %all-to-all-start.2 = ((bf16[16,64,256]{2,1,0:T(8,128)(2,1)}), bf16[16,64,256]{2,1,0:T(8,128)(2,1)S(1)}, u32[]{:S(2)}, u32[]{:S(2)}) async-start(bf16[16,64,256]{2,1,0:T(8,128)(2,1)} %bitcast.8), calls=%async_computation.2 | async-start | bytes 1048576 | tf_op jit(solution)/shard_map/all_to_all | solution.py:144
  78.6 31.2 %collective-permute-start.9 = (bf16[4,256,256]{2,1,0:T(8,128)(2,1)S(1)}, bf16[4,256,256]{2,1,0:T(8,128)(2,1)S(1)}, u32[]{:S(2)}, u32[]{:S(2)}) collective-permute-start(bf16[4,256,256]{2,1,0:T(8,128)(2,1)S(1)} %convert_element_type.11), channel_id=1, source_target_pairs={{0,256},{4,0},{256,260},{260,4},{1,257},{5,1},{257,261},{261,5},{2... | collective-permute-start | bytes 1572872 | tf_op jit(solution)/shard_map/ppermute | solution.py:173
  86.5 23.2 %collective-permute-start.8 = (bf16[4,256,256]{2,1,0:T(8,128)(2,1)S(1)}, bf16[4,256,256]{2,1,0:T(8,128)(2,1)S(1)}, u32[]{:S(2)}, u32[]{:S(2)}) collective-permute-start(bf16[4,256,256]{2,1,0:T(8,128)(2,1)S(1)} %convert_element_type.11), channel_id=1, source_target_pairs={{0,0},{4,256},{256,4},{260,260},{1,1},{5,257},{257,5},{261,261},{2... | collective-permute-start | bytes 1572872 | tf_op jit(solution)/shard_map/ppermute | solution.py:173
  110.8 69.2 %all-to-all-start.3 = ((bf16[4,2,256,256]{3,2,1,0:T(8,128)(2,1)}), bf16[4,2,256,256]{3,2,1,0:T(8,128)(2,1)S(1)}, u32[]{:S(2)}, u32[]{:S(2)}) async-start(bf16[4,2,256,256]{3,2,1,0:T(8,128)(2,1)} %pad_maximum_fusion), calls=%async_computation.3 | async-start | bytes 2097152 | tf_op jit(solution)/shard_map/all_to_all | solution.py:144
  116.9 155.8 %reduce-scatter.2.cloned.1.call-start = ((), (), s32[]{:S(2)}) async-start(), calls=%async_computation.9 | async-start | bytes 4718592 | tf_op jit(solution)/shard_map/reduce_scatter | solution.py:202
  116.9 26.9 %collective-permute-start.2 = (bf16[512,256]{1,0:T(8,128)(2,1)S(1)}, bf16[512,256]{1,0:T(8,128)(2,1)S(1)}, u32[]{:S(2)}, u32[]{:S(2)}) collective-permute-start(bf16[512,256]{1,0:T(8,128)(2,1)S(1)} %bitcast.46), channel_id=1, source_target_pairs={{0,256},{4,384},{64,320},{68,448},{128,0},{132,128},{192,64},{196,... | collective-permute-start | bytes 786440 | tf_op jit(solution)/shard_map/ppermute | solution.py:165
  127.2 17.3 %collective-permute-start = (bf16[512,256]{1,0:T(8,128)(2,1)S(1)}, bf16[512,256]{1,0:T(8,128)(2,1)S(1)}, u32[]{:S(2)}, u32[]{:S(2)}) collective-permute-start(bf16[512,256]{1,0:T(8,128)(2,1)S(1)} %bitcast.47), channel_id=1, source_target_pairs={{0,0},{4,128},{64,64},{68,192},{128,256},{132,384},{192,320},{196,... | collective-permute-start | bytes 786440 | tf_op jit(solution)/shard_map/ppermute | solution.py:165
  127.9 47.2 %collective-permute-start.3 = (bf16[512,256]{1,0:T(8,128)(2,1)S(1)}, bf16[512,256]{1,0:T(8,128)(2,1)S(1)}, u32[]{:S(2)}, u32[]{:S(2)}) collective-permute-start(bf16[512,256]{1,0:T(8,128)(2,1)S(1)} %bitcast.44), channel_id=1, source_target_pairs={{0,320},{4,448},{64,256},{68,384},{128,64},{132,192},{192,0},{196,... | collective-permute-start | bytes 786440 | tf_op jit(solution)/shard_map/ppermute | solution.py:165
  138.1 39.7 %collective-permute-start.1 = (bf16[512,256]{1,0:T(8,128)(2,1)S(1)}, bf16[512,256]{1,0:T(8,128)(2,1)}, u32[]{:S(2)}, u32[]{:S(2)}) collective-permute-start(bf16[512,256]{1,0:T(8,128)(2,1)S(1)} %bitcast.45), channel_id=1, source_target_pairs={{0,64},{4,192},{64,0},{68,128},{128,320},{132,448},{192,256},{196,... | collective-permute-start | bytes 786440 | tf_op jit(solution)/shard_map/ppermute | solution.py:165
  141.9 44.3 %collective-permute-start.6 = (bf16[512,256]{1,0:T(8,128)(2,1)S(1)}, bf16[512,256]{1,0:T(8,128)(2,1)S(1)}, u32[]{:S(2)}, u32[]{:S(2)}) collective-permute-start(bf16[512,256]{1,0:T(8,128)(2,1)S(1)} %bitcast.50), channel_id=1, source_target_pairs={{0,256},{4,384},{64,320},{68,448},{128,0},{132,128},{192,64},{196,... | collective-permute-start | bytes 786440 | tf_op jit(solution)/shard_map/ppermute | solution.py:165
  143.8 34.0 %copy-start.6 = (bf16[512,256]{1,0:T(8,128)(2,1)}, bf16[512,256]{1,0:T(8,128)(2,1)S(1)}, u32[]{:S(2)}) copy-start(bf16[512,256]{1,0:T(8,128)(2,1)S(1)} %collective-permute-done.2.refs_2_) | copy-start | bytes 786436
  143.9 42.3 %collective-permute-start.4 = (bf16[512,256]{1,0:T(8,128)(2,1)S(1)}, bf16[512,256]{1,0:T(8,128)(2,1)S(1)}, u32[]{:S(2)}, u32[]{:S(2)}) collective-permute-start(bf16[512,256]{1,0:T(8,128)(2,1)S(1)} %bitcast.51), channel_id=1, source_target_pairs={{0,0},{4,128},{64,64},{68,192},{128,256},{132,384},{192,320},{196,... | collective-permute-start | bytes 786440 | tf_op jit(solution)/shard_map/ppermute | solution.py:165
  144.5 30.6 %copy-start.8 = (bf16[512,256]{1,0:T(8,128)(2,1)}, bf16[512,256]{1,0:T(8,128)(2,1)S(1)}, u32[]{:S(2)}) copy-start(bf16[512,256]{1,0:T(8,128)(2,1)S(1)} %collective-permute-done.refs_0_) | copy-start | bytes 786436
  144.6 46.2 %collective-permute-start.7 = (bf16[512,256]{1,0:T(8,128)(2,1)S(1)}, bf16[512,256]{1,0:T(8,128)(2,1)}, u32[]{:S(2)}, u32[]{:S(2)}) collective-permute-start(bf16[512,256]{1,0:T(8,128)(2,1)S(1)} %bitcast.48), channel_id=1, source_target_pairs={{0,320},{4,448},{64,256},{68,384},{128,64},{132,192},{192,0},{196,... | collective-permute-start | bytes 786440 | tf_op jit(solution)/shard_map/ppermute | solution.py:165
  175.2 0.7 copy-start.9
  175.9 14.9 %collective-permute-start.5 = (bf16[512,256]{1,0:T(8,128)(2,1)S(1)}, bf16[512,256]{1,0:T(8,128)(2,1)}, u32[]{:S(2)}, u32[]{:S(2)}) collective-permute-start(bf16[512,256]{1,0:T(8,128)(2,1)S(1)} %bitcast.49), channel_id=1, source_target_pairs={{0,64},{4,192},{64,0},{68,128},{128,320},{132,448},{192,256},{196,... | collective-permute-start | bytes 786440 | tf_op jit(solution)/shard_map/ppermute | solution.py:165
  180.0 13.0 %copy-start.1 = (bf16[4,512,256]{2,1,0:T(8,128)(2,1)S(1)}, bf16[4,512,256]{2,1,0:T(8,128)(2,1)}, u32[]{:S(2)}) copy-start(bf16[4,512,256]{2,1,0:T(8,128)(2,1)} %place.2) | copy-start | bytes 3145732
  180.0 1.0 copy-start
  186.2 4.6 %copy-start.5 = (bf16[512,256]{1,0:T(8,128)(2,1)}, bf16[512,256]{1,0:T(8,128)(2,1)S(1)}, u32[]{:S(2)}) copy-start(bf16[512,256]{1,0:T(8,128)(2,1)S(1)} %collective-permute-done.6.refs_2_) | copy-start | bytes 786436
  186.2 4.6 %copy-start.7 = (bf16[512,256]{1,0:T(8,128)(2,1)}, bf16[512,256]{1,0:T(8,128)(2,1)S(1)}, u32[]{:S(2)}) copy-start(bf16[512,256]{1,0:T(8,128)(2,1)S(1)} %collective-permute-done.4.refs_0_) | copy-start | bytes 786436
  193.0 4.7 %copy-start.2 = (bf16[256,2048]{1,0:T(8,128)(2,1)S(1)}, bf16[256,2048]{1,0:T(8,128)(2,1)}, u32[]{:S(2)}) copy-start(bf16[256,2048]{1,0:T(8,128)(2,1)} %place_cols.1) | copy-start | bytes 3145732
  193.0 4.7 %copy-start.3 = (bf16[4,512,256]{2,1,0:T(8,128)(2,1)S(1)}, bf16[4,512,256]{2,1,0:T(8,128)(2,1)}, u32[]{:S(2)}) copy-start(bf16[4,512,256]{2,1,0:T(8,128)(2,1)} %place.3) | copy-start | bytes 3145732
Sparse Core Ops, SparseCore 0:
  30.4 83.1 all-gather.1
  206.7 65.9 reduce-scatter.1
where the time goes:
time: 318 us; the launch traced here: 317 us
  waiting for transfers between devices  116 us (36%)
  starting transfers between devices  86.2 us (27%)
  blocking collectives  62.7 us (20%)
  Pallas kernels  18 us (6%)
  between operations  14.3 us (4%)
  matrix products  13.5 us (4%)
  local copies, waits for them, and re-layouts  4.18 us (1%)
    reduce_scatter x1, waiting for transfers between devices, body(): over_y = lax.psum_scatter(partial, 'y', scatter_dimension=0, tiled=True)  66.1 us
    all_to_all x4, blocking collectives, exchange(): return lax.all_to_all(value, axes, split_axis=0, concat_axis=0, tiled=True)  62.7 us
    ppermute x8, starting transfers between devices, to_servers(): lax.ppermute(other if k & 1 else own, ('gr', 'zl', 'xh'), pairs)  60 us
    all_to_all x3, waiting for transfers between devices, exchange(): return lax.all_to_all(value, axes, split_axis=0, concat_axis=0, tiled=True)  22.5 us
    ppermute x2, waiting for transfers between devices, down_to_servers(): pieces.append(lax.ppermute(down, ('gr', 'xh'), pairs))  22.5 us
    all_to_all x3, starting transfers between devices, exchange(): return lax.all_to_all(value, axes, split_axis=0, concat_axis=0, tiled=True)  17.6 us
    dot_general x1, matrix products, body(): jnp.dot(hidden, down_serving, preferred_element_type=jnp.float32)  8.86 us
    ppermute x2, starting transfers between devices, down_to_servers(): pieces.append(lax.ppermute(down, ('gr', 'xh'), pairs))  8.63 us
  transfers between devices with their start and end apart: 15, of which 4 were waited for; matrix products, arithmetic and copies ran while one was open for 1% of the time, Pallas kernels for 4%

commit v1 on v0

--- a/solution.py
+++ b/solution.py
@@ -8,6 +8,7 @@
 
 
 SLOTS = 32
+NEAR = 1408
 NORM_EPS = 1e-06
 FS = ("zl", "y")
 TP = ("xh", "xl", "c")
@@ -54,12 +55,10 @@
     scale = lax.rsqrt(jnp.mean(x * x, axis=1, keepdims=True) + NORM_EPS)
     normed = (x * scale).astype(jnp.bfloat16)
     pick = slots_of(ids_ref[...], expert_ref[0]).astype(jnp.bfloat16)
-    rows = jnp.dot(pick, normed, preferred_element_type=jnp.float32).astype(jnp.bfloat16)
-    for z in range(out_ref.shape[0]):
-        out_ref[z] = rows
-
-
-def dispatch(expert, ids, prompt, copies):
+    out_ref[...] = jnp.dot(pick, normed, preferred_element_type=jnp.float32).astype(jnp.bfloat16)
+
+
+def dispatch(expert, ids, prompt):
     return pl.pallas_call(
         dispatch_kernel,
         in_specs=[
@@ -68,40 +67,48 @@
             pl.BlockSpec(memory_space=pltpu.VMEM),
         ],
         out_specs=pl.BlockSpec(memory_space=pltpu.VMEM),
-        out_shape=jax.ShapeDtypeStruct((copies, SLOTS, prompt.shape[1]), jnp.bfloat16),
+        out_shape=jax.ShapeDtypeStruct((SLOTS, prompt.shape[1]), jnp.bfloat16),
         name="dispatch",
     )(expert, ids, prompt)
 
 
-def combine_kernel(expert_ref, ids_ref, weights_ref, parts_ref, out_ref):
+def summed(parts):
+    total = parts[0].astype(jnp.float32)
+    for part in parts[1:]:
+        total = total + part.astype(jnp.float32)
+    return total
+
+
+def combine_kernel(expert_ref, ids_ref, weights_ref, far_ref, *refs):
+    *near_refs, out_ref = refs
     pick = slots_of(ids_ref[...], expert_ref[0])
     w = jnp.where(ids_ref[0:1] == expert_ref[0], weights_ref[0:1], weights_ref[1:2])
     slot_weight = jnp.sum(jnp.where(pick, w, 0.0), axis=1, keepdims=True)
-    total = parts_ref[0].astype(jnp.float32)
-    for z in range(1, parts_ref.shape[0]):
-        total = total + parts_ref[z].astype(jnp.float32)
-    term = (total * slot_weight).astype(jnp.bfloat16)
-    out_ref[...] = lax.dot_general(
-        pick.astype(jnp.bfloat16),
-        term,
-        (((0,), (0,)), ((), ())),
-        preferred_element_type=jnp.float32,
-    ).astype(jnp.bfloat16)
-
-
-def combine(expert, ids, weights, parts):
+    pick = pick.astype(jnp.bfloat16)
+    split = near_refs[0].shape[1]
+    totals = (
+        (0, summed([ref[...] for ref in near_refs])),
+        (split, summed([far_ref[i] for i in range(far_ref.shape[0])])),
+    )
+    for first, total in totals:
+        out_ref[:, first : first + total.shape[1]] = lax.dot_general(
+            pick,
+            (total * slot_weight).astype(jnp.bfloat16),
+            (((0,), (0,)), ((), ())),
+            preferred_element_type=jnp.float32,
+        ).astype(jnp.bfloat16)
+
+
+def combine(expert, ids, weights, near, far):
+    vmem = pl.BlockSpec(memory_space=pltpu.VMEM)
+    width = near[0].shape[1] + far.shape[2]
     return pl.pallas_call(
         combine_kernel,
-        in_specs=[
-            pl.BlockSpec(memory_space=pltpu.SMEM),
-            pl.BlockSpec(memory_space=pltpu.VMEM),
-            pl.BlockSpec(memory_space=pltpu.VMEM),
-            pl.BlockSpec(memory_space=pltpu.VMEM),
-        ],
-        out_specs=pl.BlockSpec(memory_space=pltpu.VMEM),
-        out_shape=jax.ShapeDtypeStruct((ids.shape[1], parts.shape[2]), jnp.bfloat16),
+        in_specs=[pl.BlockSpec(memory_space=pltpu.SMEM)] + [vmem] * (3 + len(near)),
+        out_specs=vmem,
+        out_shape=jax.ShapeDtypeStruct((ids.shape[1], width), jnp.bfloat16),
         name="combine",
-    )(expert, ids, weights, parts)
+    )(expert, ids, weights, far, *near)
 
 
 def place_kernel(at_ref, *refs):
@@ -142,6 +149,12 @@
 
 def exchange(value, axes):
     return lax.all_to_all(value, axes, split_axis=0, concat_axis=0, tiled=True)
+
+
+def shifted(value, step):
+    count = lax.axis_size("zl")
+    pairs = [(z, (z + step) % count) for z in range(count)]
+    return lax.ppermute(value, "zl", pairs)
 
 
 def by_half(by_core, zl):
@@ -182,12 +195,16 @@
     gain = ffn_gain[:, None]
     width = prompt.shape[1]
 
-    routed = exchange(dispatch(expert, ids, prompt, lax.axis_size("zl")), "zl")
+    own_rows = dispatch(expert, ids, prompt)
+    depth = lax.axis_size("zl")
+    routed = [own_rows] + [shifted(own_rows, s) for s in range(1, depth)]
     down_serving = down_to_servers(down_master.astype(jnp.bfloat16), gr)
     blocks = cut(gate_master, up_master, gain)
     by_core = exchange(blocks, "c")
     own, other = by_half(by_core[:, 0], zl)
-    own, other, up_blocks = lax.optimization_barrier((own, other, by_core[:, 1]))
+    own, other, up_blocks, routed = lax.optimization_barrier(
+        (own, other, by_core[:, 1], jnp.stack(routed))
+    )
     gate = to_servers(own, other, zl, gr)
     up = to_servers(*by_half(up_blocks, zl), zl, gr)
     gate_serving = gate.reshape(-1, gate.shape[-1])
@@ -197,10 +214,26 @@
     gate_part = jnp.dot(rows, gate_serving, preferred_element_type=jnp.float32)
     up_part = jnp.dot(rows, up_serving, preferred_element_type=jnp.float32)
     hidden = (jax.nn.silu(gate_part) * up_part).astype(jnp.bfloat16)
-    partial = jnp.dot(hidden, down_serving, preferred_element_type=jnp.float32).astype(jnp.bfloat16)
-    partial = partial.reshape(-1, SLOTS, width)
-    over_y = lax.psum_scatter(partial, "y", scatter_dimension=0, tiled=True)
-    terms = combine(expert, ids, weights, exchange(over_y, "zl"))
+    near = jnp.dot(
+        hidden, down_serving[:, :NEAR], preferred_element_type=jnp.float32
+    ).astype(jnp.bfloat16)
+    near = lax.psum_scatter(
+        near.reshape(-1, SLOTS, NEAR), "y", scatter_dimension=0, tiled=True
+    )
+    by_step = hidden.reshape(-1, depth, SLOTS, hidden.shape[1])
+    far = [
+        jnp.dot(
+            by_step[:, s].reshape(-1, hidden.shape[1]),
+            down_serving[:, NEAR:],
+            preferred_element_type=jnp.float32,
+        ).astype(jnp.bfloat16)
+        for s in range(depth)
+    ]
+    far = [far[0]] + [shifted(far[s], -s) for s in range(1, depth)]
+    far = summed(far).astype(jnp.bfloat16).reshape(-1, SLOTS, width - NEAR)
+    far = exchange(far, "y")
+    near = [near[0]] + [shifted(near[s], -s) for s in range(1, depth)]
+    terms = combine(expert, ids, weights, near, far)
     arrived = exchange(terms.reshape(lax.axis_size(TP), -1, width), TP)
     mixed = jnp.sum(arrived.astype(jnp.float32), axis=0).astype(jnp.bfloat16)
     return (gate_serving[None], up_serving[None], down_serving[None], mixed)

time: 318 us -> 286 us (0.90)
  blocking collectives: 62.7 us -> 30.8 us
  waiting for transfers between devices: 116 us -> 95.8 us
  starting transfers between devices: 86.2 us -> 106 us
  matrix products: 13.5 us -> 9.25 us
    reduce_scatter x1, waiting for transfers between devices: 66.1 us -> 3.72 us  [body(): lax.psum_scatter(near.reshape(-1, SLOTS, NEAR), 'y', scatter_dimension=0,...]
    ppermute x8, waiting for transfers between devices: 4.61 us -> 43.3 us  [to_servers(): lax.ppermute(other if k & 1 else own, ('gr', 'zl', 'xh'), pairs)]
    ppermute x0 -> x9, waiting for transfers between devices: none -> 34.8 us  [shifted(): return lax.ppermute(value, 'zl', pairs)]
    ppermute x0 -> x9, starting transfers between devices: none -> 34.6 us  [shifted(): return lax.ppermute(value, 'zl', pairs)]
    all_to_all x4 -> x2, blocking collectives: 62.7 us -> 30.8 us  [exchange(): return lax.all_to_all(value, axes, split_axis=0, concat_axis=0, tiled=True)]
    ppermute x8, starting transfers between devices: 60 us -> 32.2 us  [to_servers(): lax.ppermute(other if k & 1 else own, ('gr', 'zl', 'xh'), pairs)]
    all_to_all x3 -> x4, waiting for transfers between devices: 22.5 us -> 0.01 us  [exchange(): return lax.all_to_all(value, axes, split_axis=0, concat_axis=0, tiled=True)]
    all_to_all x3 -> x4, starting transfers between devices: 17.6 us -> 27.9 us  [exchange(): return lax.all_to_all(value, axes, split_axis=0, concat_axis=0, tiled=True)]
  transfers between devices with their start and end apart: 15 -> 25, of which waited for: 4 -> 10; matrix products, arithmetic and copies ran while one was open for 1% -> 2% of each run, Pallas kernels for 4% -> 4%
where the time goes in v1:
time: 286 us; the launch traced here: 285 us
  starting transfers between devices  106 us (37%)
  waiting for transfers between devices  95.8 us (33%)
  blocking collectives  30.8 us (11%)
  Pallas kernels  17.9 us (6%)
  between operations  14.5 us (5%)
  matrix products  9.25 us (3%)
  local copies, waits for them, and re-layouts  6.7 us (2%)
  other arithmetic  3.59 us (1%)
    ppermute x8, waiting for transfers between devices, to_servers(): lax.ppermute(other if k & 1 else own, ('gr', 'zl', 'xh'), pairs)  43.3 us
    ppermute x9, waiting for transfers between devices, shifted(): return lax.ppermute(value, 'zl', pairs)  34.8 us
    ppermute x9, starting transfers between devices, shifted(): return lax.ppermute(value, 'zl', pairs)  34.6 us
    ppermute x8, starting transfers between devices, to_servers(): lax.ppermute(other if k & 1 else own, ('gr', 'zl', 'xh'), pairs)  32.2 us
    all_to_all x2, blocking collectives, exchange(): return lax.all_to_all(value, axes, split_axis=0, concat_axis=0, tiled=True)  30.8 us
    all_to_all x4, starting transfers between devices, exchange(): return lax.all_to_all(value, axes, split_axis=0, concat_axis=0, tiled=True)  27.9 us
    ppermute x2, waiting for transfers between devices, down_to_servers(): pieces.append(lax.ppermute(down, ('gr', 'xh'), pairs))  13.9 us
    ppermute x2, starting transfers between devices, down_to_servers(): pieces.append(lax.ppermute(down, ('gr', 'xh'), pairs))  11.4 us
  transfers between devices with their start and end apart: 25, of which 10 were waited for; matrix products, arithmetic and copies ran while one was open for 2% of the time, Pallas kernels for 4%

profile of v1, /device:TPU:1, one launch (start us, length us, event | category | flops | bytes accessed | tf_op | source)
XLA Modules:
  0.0 284.5 jit_solution(8247204674680069330)
XLA Ops:
  7.2 1.4 copy.15.gain_ref
  8.5 3.7 %cut.1 = bf16[2,2,4,2,64,256]{5,4,3,2,1,0:T(8,128)(2,1)} custom-call(f32[64,1]{1,0:T(8,128)} %copy.15.gain_ref, f32[4,64,1024]{2,1,0:T(8,128)} %gate_ref.1, f32[4,64,1024]{2,1,0:T(8,128)} %up_ref.1), custom_call_target="tpu_custom_call" | custom-call | tf_op jit(solution)/shard_map/cut/pallas_call | solution.py:30
  12.2 12.1 %all_to_all.30 = bf16[2,2,4,2,64,256]{5,4,3,2,1,0:T(8,128)(2,1)S(1)} all-to-all(bf16[2,2,4,2,64,256]{5,4,3,2,1,0:T(8,128)(2,1)} %cut.1), channel_id=1, replica_groups=mesh['gr'=2,'zl'=4,'y'=8,'xh'=2,'xl'=2,'c'=2] {'c'}, dimensions={0} | all-to-all | bytes 2097152 | tf_op jit(solution)/shard_map/all_to_all | solution.py:151
  24.4 1.0 slice_bitcast_fusion
  25.4 3.6 %all-to-all-start.1 = ((bf16[16,64,256]{2,1,0:T(8,128)(2,1)}), bf16[16,64,256]{2,1,0:T(8,128)(2,1)S(1)}, u32[]{:S(2)}, u32[]{:S(2)}) async-start(bf16[16,64,256]{2,1,0:T(8,128)(2,1)} %bitcast.2), calls=%async_computation.1 | async-start | bytes 1048576 | tf_op jit(solution)/shard_map/all_to_all | solution.py:151
  29.0 0.0 all-gather.2.cloned.1.call-start
  29.1 2.1 dispatch.1
  31.2 2.9 %collective-permute-start = (bf16[32,2048]{1,0:T(8,128)(2,1)}, bf16[32,2048]{1,0:T(8,128)(2,1)S(1)}, u32[]{:S(2)}, u32[]{:S(2)}) collective-permute-start(bf16[32,2048]{1,0:T(8,128)(2,1)} %dispatch.1), channel_id=1, source_target_pairs={{0,64},{64,128},{128,192},{192,0},{1,65},{65,129},{129,193},{193,1... | collective-permute-start | bytes 393224 | tf_op jit(solution)/shard_map/ppermute | solution.py:157
  34.1 5.8 %collective-permute-start.1 = (bf16[32,2048]{1,0:T(8,128)(2,1)}, bf16[32,2048]{1,0:T(8,128)(2,1)S(1)}, u32[]{:S(2)}, u32[]{:S(2)}) collective-permute-start(bf16[32,2048]{1,0:T(8,128)(2,1)} %dispatch.1), channel_id=1, source_target_pairs={{0,128},{64,192},{128,0},{192,64},{1,129},{65,193},{129,1},{193,65... | collective-permute-start | bytes 393224 | tf_op jit(solution)/shard_map/ppermute | solution.py:157
  39.9 2.2 collective-permute-start.2
  42.1 5.4 %collective-permute-done.1 = bf16[32,2048]{1,0:T(8,128)(2,1)S(1)} collective-permute-done((bf16[32,2048]{1,0:T(8,128)(2,1)}, bf16[32,2048]{1,0:T(8,128)(2,1)S(1)}, u32[]{:S(2)}, u32[]{:S(2)}) %collective-permute-start.1) | collective-permute-done | bytes 131104 | tf_op jit(solution)/shard_map/ppermute | solution.py:157
  47.5 2.3 collective-permute-done.2
  49.8 1.8 pad_maximum_fusion.1
  51.7 0.0 all-gather.2.cloned.1.call-update
  51.7 7.6 %all-to-all-start.2 = ((bf16[16,64,256]{2,1,0:T(8,128)(2,1)}), bf16[16,64,256]{2,1,0:T(8,128)(2,1)S(1)}, u32[]{:S(2)}, u32[]{:S(2)}) async-start(bf16[16,64,256]{2,1,0:T(8,128)(2,1)} %bitcast.14), calls=%async_computation.2 | async-start | bytes 1048576 | tf_op jit(solution)/shard_map/all_to_all | solution.py:151
  59.3 0.1 convert_element_type.38
  59.3 0.7 collective-permute-start.11
  60.0 10.7 %collective-permute-start.12 = (bf16[4,256,256]{2,1,0:T(8,128)(2,1)S(1)}, bf16[4,256,256]{2,1,0:T(8,128)(2,1)S(1)}, u32[]{:S(2)}, u32[]{:S(2)}) collective-permute-start(bf16[4,256,256]{2,1,0:T(8,128)(2,1)S(1)} %convert_element_type.38), channel_id=1, source_target_pairs={{0,256},{4,0},{256,260},{260,4},{1,257},{5,1},{257,261},{261,5},{2... | collective-permute-start | bytes 1572872 | tf_op jit(solution)/shard_map/ppermute | solution.py:186
  70.7 13.9 %collective-permute-done.12 = bf16[4,256,256]{2,1,0:T(8,128)(2,1)S(1)} collective-permute-done((bf16[4,256,256]{2,1,0:T(8,128)(2,1)S(1)}, bf16[4,256,256]{2,1,0:T(8,128)(2,1)S(1)}, u32[]{:S(2)}, u32[]{:S(2)}) %collective-permute-start.12) | collective-permute-done | bytes 524320 | tf_op jit(solution)/shard_map/ppermute | solution.py:186
  84.6 1.1 pad_maximum_fusion
  85.7 10.7 %all-to-all-start.3 = ((bf16[4,2,256,256]{3,2,1,0:T(8,128)(2,1)}), bf16[4,2,256,256]{3,2,1,0:T(8,128)(2,1)S(1)}, u32[]{:S(2)}, u32[]{:S(2)}) async-start(bf16[4,2,256,256]{3,2,1,0:T(8,128)(2,1)} %pad_maximum_fusion), calls=%async_computation.3 | async-start | bytes 2097152 | tf_op jit(solution)/shard_map/all_to_all | solution.py:151
  96.4 0.7 collective-permute-start.3
  97.1 3.5 %collective-permute-start.4 = (bf16[512,256]{1,0:T(8,128)(2,1)S(1)}, bf16[512,256]{1,0:T(8,128)(2,1)S(1)}, u32[]{:S(2)}, u32[]{:S(2)}) collective-permute-start(bf16[512,256]{1,0:T(8,128)(2,1)S(1)} %bitcast.72), channel_id=1, source_target_pairs={{0,64},{4,192},{64,0},{68,128},{128,320},{132,448},{192,256},{196,... | collective-permute-start | bytes 786440 | tf_op jit(solution)/shard_map/ppermute | solution.py:178
  100.5 14.9 %collective-permute-start.5 = (bf16[512,256]{1,0:T(8,128)(2,1)S(1)}, bf16[512,256]{1,0:T(8,128)(2,1)S(1)}, u32[]{:S(2)}, u32[]{:S(2)}) collective-permute-start(bf16[512,256]{1,0:T(8,128)(2,1)S(1)} %bitcast.75), channel_id=1, source_target_pairs={{0,256},{4,384},{64,320},{68,448},{128,0},{132,128},{192,64},{196,... | collective-permute-start | bytes 786440 | tf_op jit(solution)/shard_map/ppermute | solution.py:178
  115.4 4.9 %collective-permute-start.6 = (bf16[512,256]{1,0:T(8,128)(2,1)S(1)}, bf16[512,256]{1,0:T(8,128)(2,1)}, u32[]{:S(2)}, u32[]{:S(2)}) collective-permute-start(bf16[512,256]{1,0:T(8,128)(2,1)S(1)} %bitcast.73), channel_id=1, source_target_pairs={{0,320},{4,448},{64,256},{68,384},{128,64},{132,192},{192,0},{196,... | collective-permute-start | bytes 786440 | tf_op jit(solution)/shard_map/ppermute | solution.py:178
  120.3 0.1 constant_dynamic-slice_fusion
  120.4 1.9 collective-permute-start.10
  122.3 0.0 copy-start.7
  122.3 3.1 %collective-permute-start.8 = (bf16[512,256]{1,0:T(8,128)(2,1)S(1)}, bf16[512,256]{1,0:T(8,128)(2,1)S(1)}, u32[]{:S(2)}, u32[]{:S(2)}) collective-permute-start(bf16[512,256]{1,0:T(8,128)(2,1)S(1)} %bitcast.79), channel_id=1, source_target_pairs={{0,64},{4,192},{64,0},{68,128},{128,320},{132,448},{192,256},{196,... | collective-permute-start | bytes 786440 | tf_op jit(solution)/shard_map/ppermute | solution.py:178
  125.4 1.4 collective-permute-start.7
  126.8 37.4 %collective-permute-done.5.refs_2_ = bf16[512,256]{1,0:T(8,128)(2,1)S(1)} collective-permute-done((bf16[512,256]{1,0:T(8,128)(2,1)S(1)}, bf16[512,256]{1,0:T(8,128)(2,1)S(1)}, u32[]{:S(2)}, u32[]{:S(2)}) %collective-permute-start.5) | collective-permute-done | bytes 262176 | tf_op jit(solution)/shard_map/ppermute | solution.py:178
  164.2 0.7 copy-done.10
  164.9 1.9 collective-permute-start.9
  166.9 2.2 place.2
  169.1 1.0 copy-done.1
  170.1 5.2 %place_cols.1 = bf16[256,2048]{1,0:T(8,128)(2,1)} custom-call(s32[1]{0:T(128)} %bitcast.19.at_ref, bf16[4,2,256,256]{3,2,1,0:T(8,128)(2,1)} %copy-done.1), custom_call_target="tpu_custom_call" | custom-call | tf_op jit(solution)/shard_map/place_cols/pallas_call | solution.py:137
  175.3 5.9 %collective-permute-done.9.refs_2_ = bf16[512,256]{1,0:T(8,128)(2,1)} collective-permute-done((bf16[512,256]{1,0:T(8,128)(2,1)S(1)}, bf16[512,256]{1,0:T(8,128)(2,1)}, u32[]{:S(2)}, u32[]{:S(2)}) %collective-permute-start.9) | collective-permute-done | bytes 262176 | tf_op jit(solution)/shard_map/ppermute | solution.py:178
  181.2 2.2 place.3
  183.4 3.6 %fusion.9 = f32[1024,256]{1,0:T(8,128)S(1)} fusion(bf16[1024,2048]{1,0:T(8,128)(2,1)} %bitcast.87, bf16[2048,256]{1,0:T(8,128)(2,1)S(1)} %bitcast.62), kind=kOutput, calls=%fused_computation.25 | convolution fusion | flops 1073741824 | bytes 6291456 | tf_op jit(solution)/shard_map/dot_general | solution.py:214
  187.0 0.2 copy-done.14
  187.2 1.3 multiply_convert_fusion
  188.5 2.5 convolution_convert_fusion
  191.0 0.0 reduce-scatter.2.cloned.1.call-update
  191.1 0.3 convolution_convert_fusion.3
  191.4 1.9 collective-permute-start.13
  193.3 0.3 convolution_convert_fusion.2
  193.6 1.9 collective-permute-start.14
  195.5 0.3 convolution_convert_fusion.1
  195.8 3.4 %collective-permute-start.15 = (bf16[256,640]{1,0:T(8,128)(2,1)S(1)}, bf16[256,640]{1,0:T(8,128)(2,1)S(1)}, u32[]{:S(2)}, u32[]{:S(2)}) collective-permute-start(bf16[256,640]{1,0:T(8,128)(2,1)S(1)} %convolution_convert_fusion.1), channel_id=1, source_target_pairs={{0,64},{64,128},{128,192},{192,0},{1,65},{65,129},{129,193},{193,1... | collective-permute-start | bytes 983048 | tf_op jit(solution)/shard_map/ppermute | solution.py:157
  199.2 4.0 %collective-permute-done.13 = bf16[256,640]{1,0:T(8,128)(2,1)S(1)} collective-permute-done((bf16[256,640]{1,0:T(8,128)(2,1)S(1)}, bf16[256,640]{1,0:T(8,128)(2,1)S(1)}, u32[]{:S(2)}, u32[]{:S(2)}) %collective-permute-start.13) | collective-permute-done | bytes 327712 | tf_op jit(solution)/shard_map/ppermute | solution.py:157
  203.1 18.0 %collective-permute-done.14 = bf16[256,640]{1,0:T(8,128)(2,1)S(1)} collective-permute-done((bf16[256,640]{1,0:T(8,128)(2,1)S(1)}, bf16[256,640]{1,0:T(8,128)(2,1)S(1)}, u32[]{:S(2)}, u32[]{:S(2)}) %collective-permute-start.14) | collective-permute-done | bytes 327712 | tf_op jit(solution)/shard_map/ppermute | solution.py:157
  221.1 1.0 add_convert_fusion
  222.2 6.0 %all-to-all-start.4 = ((bf16[8,32,640]{2,1,0:T(8,128)(2,1)}), bf16[8,32,640]{2,1,0:T(8,128)(2,1)S(1)}, u32[]{:S(2)}, u32[]{:S(2)}) async-start(bf16[8,32,640]{2,1,0:T(8,128)(2,1)} %bitcast.33), calls=%async_computation.4 | async-start | bytes 655360 | tf_op jit(solution)/shard_map/all_to_all | solution.py:151
  228.2 3.7 %reduce-scatter.2.cloned.1.call-done = bf16[4,32,1408]{2,1,0:T(8,128)(2,1)} async-done(((bf16[32,32,1408]{2,1,0:T(8,128)(2,1)}), bf16[4,32,1408]{2,1,0:T(8,128)(2,1)}) %reduce-scatter.2.cloned.1.call-update) | async-done | bytes 360464 | tf_op jit(solution)/shard_map/reduce_scatter | solution.py:220
  231.9 1.7 slice_bitcast_fusion.1
  233.6 12.3 %collective-permute-start.16 = (bf16[32,1408]{1,0:T(8,128)(2,1)S(1)}, bf16[32,1408]{1,0:T(8,128)(2,1)S(1)}, u32[]{:S(2)}, u32[]{:S(2)}) collective-permute-start(bf16[32,1408]{1,0:T(8,128)(2,1)S(1)} %get-tuple-element.24), channel_id=1, source_target_pairs={{0,192},{64,0},{128,64},{192,128},{1,193},{65,1},{129,65},{193,129... | collective-permute-start | bytes 270344 | tf_op jit(solution)/shard_map/ppermute | solution.py:157
  246.0 1.9 collective-permute-start.17
  247.9 2.2 collective-permute-start.18
  250.1 2.0 collective-permute-done.17.refs_2_
  252.1 3.1 %collective-permute-done.18.refs_3_ = bf16[32,1408]{1,0:T(8,128)(2,1)S(1)} collective-permute-done((bf16[32,1408]{1,0:T(8,128)(2,1)S(1)}, bf16[32,1408]{1,0:T(8,128)(2,1)S(1)}, u32[]{:S(2)}, u32[]{:S(2)}) %collective-permute-start.18) | collective-permute-done | bytes 90144 | tf_op jit(solution)/shard_map/ppermute | solution.py:157
  255.2 0.6 copy-done.13
  255.9 2.4 combine.1
  258.3 18.7 %all_to_all.31 = bf16[8,16,2048]{2,1,0:T(8,128)(2,1)S(1)} all-to-all(bf16[8,16,2048]{2,1,0:T(8,128)(2,1)} %bitcast.60), channel_id=1, replica_groups=mesh['gr'=2,'zl'=4,'y'=8,'xh'=2,'xl'=2,'c'=2] {'xh','xl','c'}, dimensions={0} | all-to-all | bytes 1048576 | tf_op jit(solution)/shard_map/all_to_all | solution.py:151
  277.0 0.7 reduce_sum.12
  (43 shorter events, 0.2 us)
Async XLA Ops:
  24.4 34.9 %copy-start.5 = (f32[4,256,256]{2,1,0:T(8,128)S(1)}, f32[4,256,256]{2,1,0:T(8,128)}, u32[]{:S(2)}) copy-start(f32[4,256,256]{2,1,0:T(8,128)} %param.12) | copy-start | bytes 3145732
  25.4 26.2 %all-to-all-start.1 = ((bf16[16,64,256]{2,1,0:T(8,128)(2,1)}), bf16[16,64,256]{2,1,0:T(8,128)(2,1)S(1)}, u32[]{:S(2)}, u32[]{:S(2)}) async-start(bf16[16,64,256]{2,1,0:T(8,128)(2,1)} %bitcast.2), calls=%async_computation.1 | async-start | bytes 1048576 | tf_op jit(solution)/shard_map/all_to_all | solution.py:151
  29.0 154.4 %all-gather.2.cloned.1.call-start = ((), (), s32[]{:S(2)}) async-start(), calls=%async_computation.7 | async-start | bytes 4718592 | tf_op jit(solution)/shard_map/all_gather | solution.py:213
  31.2 10.9 %collective-permute-start = (bf16[32,2048]{1,0:T(8,128)(2,1)}, bf16[32,2048]{1,0:T(8,128)(2,1)S(1)}, u32[]{:S(2)}, u32[]{:S(2)}) collective-permute-start(bf16[32,2048]{1,0:T(8,128)(2,1)} %dispatch.1), channel_id=1, source_target_pairs={{0,64},{64,128},{128,192},{192,0},{1,65},{65,129},{129,193},{193,1... | collective-permute-start | bytes 393224 | tf_op jit(solution)/shard_map/ppermute | solution.py:157
  34.1 13.4 %collective-permute-start.1 = (bf16[32,2048]{1,0:T(8,128)(2,1)}, bf16[32,2048]{1,0:T(8,128)(2,1)S(1)}, u32[]{:S(2)}, u32[]{:S(2)}) collective-permute-start(bf16[32,2048]{1,0:T(8,128)(2,1)} %dispatch.1), channel_id=1, source_target_pairs={{0,128},{64,192},{128,0},{192,64},{1,129},{65,193},{129,1},{193,65... | collective-permute-start | bytes 393224 | tf_op jit(solution)/shard_map/ppermute | solution.py:157
  39.9 9.9 %collective-permute-start.2 = (bf16[32,2048]{1,0:T(8,128)(2,1)}, bf16[32,2048]{1,0:T(8,128)(2,1)S(1)}, u32[]{:S(2)}, u32[]{:S(2)}) collective-permute-start(bf16[32,2048]{1,0:T(8,128)(2,1)} %dispatch.1), channel_id=1, source_target_pairs={{0,192},{64,0},{128,64},{192,128},{1,193},{65,1},{129,65},{193,129... | collective-permute-start | bytes 393224 | tf_op jit(solution)/shard_map/ppermute | solution.py:157
  51.7 34.0 %all-to-all-start.2 = ((bf16[16,64,256]{2,1,0:T(8,128)(2,1)}), bf16[16,64,256]{2,1,0:T(8,128)(2,1)S(1)}, u32[]{:S(2)}, u32[]{:S(2)}) async-start(bf16[16,64,256]{2,1,0:T(8,128)(2,1)} %bitcast.14), calls=%async_computation.2 | async-start | bytes 1048576 | tf_op jit(solution)/shard_map/all_to_all | solution.py:151
  59.3 11.4 %collective-permute-start.11 = (bf16[4,256,256]{2,1,0:T(8,128)(2,1)S(1)}, bf16[4,256,256]{2,1,0:T(8,128)(2,1)S(1)}, u32[]{:S(2)}, u32[]{:S(2)}) collective-permute-start(bf16[4,256,256]{2,1,0:T(8,128)(2,1)S(1)} %convert_element_type.38), channel_id=1, source_target_pairs={{0,0},{4,256},{256,4},{260,260},{1,1},{5,257},{257,5},{261,261},{2... | collective-permute-start | bytes 1572872 | tf_op jit(solution)/shard_map/ppermute | solution.py:186
  60.0 24.6 %collective-permute-start.12 = (bf16[4,256,256]{2,1,0:T(8,128)(2,1)S(1)}, bf16[4,256,256]{2,1,0:T(8,128)(2,1)S(1)}, u32[]{:S(2)}, u32[]{:S(2)}) collective-permute-start(bf16[4,256,256]{2,1,0:T(8,128)(2,1)S(1)} %convert_element_type.38), channel_id=1, source_target_pairs={{0,256},{4,0},{256,260},{260,4},{1,257},{5,1},{257,261},{261,5},{2... | collective-permute-start | bytes 1572872 | tf_op jit(solution)/shard_map/ppermute | solution.py:186
  85.7 83.4 %all-to-all-start.3 = ((bf16[4,2,256,256]{3,2,1,0:T(8,128)(2,1)}), bf16[4,2,256,256]{3,2,1,0:T(8,128)(2,1)S(1)}, u32[]{:S(2)}, u32[]{:S(2)}) async-start(bf16[4,2,256,256]{3,2,1,0:T(8,128)(2,1)} %pad_maximum_fusion), calls=%async_computation.3 | async-start | bytes 2097152 | tf_op jit(solution)/shard_map/all_to_all | solution.py:151
  96.4 135.5 %reduce-scatter.2.cloned.1.call-start = ((), (), s32[]{:S(2)}) async-start(), calls=%async_computation.8 | async-start | bytes 3244032 | tf_op jit(solution)/shard_map/reduce_scatter | solution.py:220
  96.4 25.9 %collective-permute-start.3 = (bf16[512,256]{1,0:T(8,128)(2,1)S(1)}, bf16[512,256]{1,0:T(8,128)(2,1)S(1)}, u32[]{:S(2)}, u32[]{:S(2)}) collective-permute-start(bf16[512,256]{1,0:T(8,128)(2,1)S(1)} %bitcast.74), channel_id=1, source_target_pairs={{0,0},{4,128},{64,64},{68,192},{128,256},{132,384},{192,320},{196,... | collective-permute-start | bytes 786440 | tf_op jit(solution)/shard_map/ppermute | solution.py:178
  97.1 28.4 %collective-permute-start.4 = (bf16[512,256]{1,0:T(8,128)(2,1)S(1)}, bf16[512,256]{1,0:T(8,128)(2,1)S(1)}, u32[]{:S(2)}, u32[]{:S(2)}) collective-permute-start(bf16[512,256]{1,0:T(8,128)(2,1)S(1)} %bitcast.72), channel_id=1, source_target_pairs={{0,64},{4,192},{64,0},{68,128},{128,320},{132,448},{192,256},{196,... | collective-permute-start | bytes 786440 | tf_op jit(solution)/shard_map/ppermute | solution.py:178
  100.5 63.7 %collective-permute-start.5 = (bf16[512,256]{1,0:T(8,128)(2,1)S(1)}, bf16[512,256]{1,0:T(8,128)(2,1)S(1)}, u32[]{:S(2)}, u32[]{:S(2)}) collective-permute-start(bf16[512,256]{1,0:T(8,128)(2,1)S(1)} %bitcast.75), channel_id=1, source_target_pairs={{0,256},{4,384},{64,320},{68,448},{128,0},{132,128},{192,64},{196,... | collective-permute-start | bytes 786440 | tf_op jit(solution)/shard_map/ppermute | solution.py:178
  115.4 51.4 %collective-permute-start.6 = (bf16[512,256]{1,0:T(8,128)(2,1)S(1)}, bf16[512,256]{1,0:T(8,128)(2,1)}, u32[]{:S(2)}, u32[]{:S(2)}) collective-permute-start(bf16[512,256]{1,0:T(8,128)(2,1)S(1)} %bitcast.73), channel_id=1, source_target_pairs={{0,320},{4,448},{64,256},{68,384},{128,64},{132,192},{192,0},{196,... | collective-permute-start | bytes 786440 | tf_op jit(solution)/shard_map/ppermute | solution.py:178
  120.4 54.9 %collective-permute-start.10 = (bf16[512,256]{1,0:T(8,128)(2,1)S(1)}, bf16[512,256]{1,0:T(8,128)(2,1)S(1)}, u32[]{:S(2)}, u32[]{:S(2)}) collective-permute-start(bf16[512,256]{1,0:T(8,128)(2,1)S(1)} %bitcast.78), channel_id=1, source_target_pairs={{0,320},{4,448},{64,256},{68,384},{128,64},{132,192},{192,0},{196,... | collective-permute-start | bytes 786440 | tf_op jit(solution)/shard_map/ppermute | solution.py:178
  122.3 44.6 %copy-start.7 = (bf16[512,256]{1,0:T(8,128)(2,1)}, bf16[512,256]{1,0:T(8,128)(2,1)S(1)}, u32[]{:S(2)}) copy-start(bf16[512,256]{1,0:T(8,128)(2,1)S(1)} %collective-permute-done.3.refs_0_) | copy-start | bytes 786436
  122.3 53.0 %collective-permute-start.8 = (bf16[512,256]{1,0:T(8,128)(2,1)S(1)}, bf16[512,256]{1,0:T(8,128)(2,1)S(1)}, u32[]{:S(2)}, u32[]{:S(2)}) collective-permute-start(bf16[512,256]{1,0:T(8,128)(2,1)S(1)} %bitcast.79), channel_id=1, source_target_pairs={{0,64},{4,192},{64,0},{68,128},{128,320},{132,448},{192,256},{196,... | collective-permute-start | bytes 786440 | tf_op jit(solution)/shard_map/ppermute | solution.py:178
  125.4 38.8 %copy-start.9 = (bf16[512,256]{1,0:T(8,128)(2,1)}, bf16[512,256]{1,0:T(8,128)(2,1)S(1)}, u32[]{:S(2)}) copy-start(bf16[512,256]{1,0:T(8,128)(2,1)S(1)} %collective-permute-done.4.refs_1_) | copy-start | bytes 786436
  125.4 49.9 %collective-permute-start.7 = (bf16[512,256]{1,0:T(8,128)(2,1)S(1)}, bf16[512,256]{1,0:T(8,128)(2,1)}, u32[]{:S(2)}, u32[]{:S(2)}) collective-permute-start(bf16[512,256]{1,0:T(8,128)(2,1)S(1)} %bitcast.76), channel_id=1, source_target_pairs={{0,0},{4,128},{64,64},{68,192},{128,256},{132,384},{192,320},{196,... | collective-permute-start | bytes 786440 | tf_op jit(solution)/shard_map/ppermute | solution.py:178
  164.2 0.7 copy-start.10
  164.9 16.3 %collective-permute-start.9 = (bf16[512,256]{1,0:T(8,128)(2,1)S(1)}, bf16[512,256]{1,0:T(8,128)(2,1)}, u32[]{:S(2)}, u32[]{:S(2)}) collective-permute-start(bf16[512,256]{1,0:T(8,128)(2,1)S(1)} %bitcast.77), channel_id=1, source_target_pairs={{0,256},{4,384},{64,320},{68,448},{128,0},{132,128},{192,64},{196,... | collective-permute-start | bytes 786440 | tf_op jit(solution)/shard_map/ppermute | solution.py:178
  169.1 14.3 %copy-start.3 = (bf16[4,512,256]{2,1,0:T(8,128)(2,1)S(1)}, bf16[4,512,256]{2,1,0:T(8,128)(2,1)}, u32[]{:S(2)}) copy-start(bf16[4,512,256]{2,1,0:T(8,128)(2,1)} %place.2) | copy-start | bytes 3145732
  169.1 1.0 copy-start.1
  175.3 5.9 %copy-start.6 = (bf16[512,256]{1,0:T(8,128)(2,1)}, bf16[512,256]{1,0:T(8,128)(2,1)S(1)}, u32[]{:S(2)}) copy-start(bf16[512,256]{1,0:T(8,128)(2,1)S(1)} %collective-permute-done.10.refs_3_) | copy-start | bytes 786436
  175.3 5.9 %copy-start.8 = (bf16[512,256]{1,0:T(8,128)(2,1)}, bf16[512,256]{1,0:T(8,128)(2,1)S(1)}, u32[]{:S(2)}) copy-start(bf16[512,256]{1,0:T(8,128)(2,1)S(1)} %collective-permute-done.8.refs_1_) | copy-start | bytes 786436
  183.4 3.6 %copy-start.4 = (bf16[4,512,256]{2,1,0:T(8,128)(2,1)S(1)}, bf16[4,512,256]{2,1,0:T(8,128)(2,1)}, u32[]{:S(2)}) copy-start(bf16[4,512,256]{2,1,0:T(8,128)(2,1)} %place.3) | copy-start | bytes 3145732
  183.4 3.8 %copy-start.14 = (bf16[32,32,2048]{2,1,0:T(8,128)(2,1)S(1)}, bf16[32,32,2048]{2,1,0:T(8,128)(2,1)}, u32[]{:S(2)}) copy-start(bf16[32,32,2048]{2,1,0:T(8,128)(2,1)} %all-gather.2.cloned.1.call-done) | copy-start | bytes 12582916
  187.2 1.3 copy-start
  191.4 11.7 %collective-permute-start.13 = (bf16[256,640]{1,0:T(8,128)(2,1)S(1)}, bf16[256,640]{1,0:T(8,128)(2,1)S(1)}, u32[]{:S(2)}, u32[]{:S(2)}) collective-permute-start(bf16[256,640]{1,0:T(8,128)(2,1)S(1)} %convolution_convert_fusion.3), channel_id=1, source_target_pairs={{0,192},{64,0},{128,64},{192,128},{1,193},{65,1},{129,65},{193,129... | collective-permute-start | bytes 983048 | tf_op jit(solution)/shard_map/ppermute | solution.py:157
  193.6 27.5 %collective-permute-start.14 = (bf16[256,640]{1,0:T(8,128)(2,1)S(1)}, bf16[256,640]{1,0:T(8,128)(2,1)S(1)}, u32[]{:S(2)}, u32[]{:S(2)}) collective-permute-start(bf16[256,640]{1,0:T(8,128)(2,1)S(1)} %convolution_convert_fusion.2), channel_id=1, source_target_pairs={{0,128},{64,192},{128,0},{192,64},{1,129},{65,193},{129,1},{193,65... | collective-permute-start | bytes 983048 | tf_op jit(solution)/shard_map/ppermute | solution.py:157
  195.8 25.3 %collective-permute-start.15 = (bf16[256,640]{1,0:T(8,128)(2,1)S(1)}, bf16[256,640]{1,0:T(8,128)(2,1)S(1)}, u32[]{:S(2)}, u32[]{:S(2)}) collective-permute-start(bf16[256,640]{1,0:T(8,128)(2,1)S(1)} %convolution_convert_fusion.1), channel_id=1, source_target_pairs={{0,64},{64,128},{128,192},{192,0},{1,65},{65,129},{129,193},{193,1... | collective-permute-start | bytes 983048 | tf_op jit(solution)/shard_map/ppermute | solution.py:157
  222.2 27.9 %all-to-all-start.4 = ((bf16[8,32,640]{2,1,0:T(8,128)(2,1)}), bf16[8,32,640]{2,1,0:T(8,128)(2,1)S(1)}, u32[]{:S(2)}, u32[]{:S(2)}) async-start(bf16[8,32,640]{2,1,0:T(8,128)(2,1)} %bitcast.33), calls=%async_computation.4 | async-start | bytes 655360 | tf_op jit(solution)/shard_map/all_to_all | solution.py:151
  233.6 16.5 %collective-permute-start.16 = (bf16[32,1408]{1,0:T(8,128)(2,1)S(1)}, bf16[32,1408]{1,0:T(8,128)(2,1)S(1)}, u32[]{:S(2)}, u32[]{:S(2)}) collective-permute-start(bf16[32,1408]{1,0:T(8,128)(2,1)S(1)} %get-tuple-element.24), channel_id=1, source_target_pairs={{0,192},{64,0},{128,64},{192,128},{1,193},{65,1},{129,65},{193,129... | collective-permute-start | bytes 270344 | tf_op jit(solution)/shard_map/ppermute | solution.py:157
  246.0 6.2 %collective-permute-start.17 = (bf16[32,1408]{1,0:T(8,128)(2,1)S(1)}, bf16[32,1408]{1,0:T(8,128)(2,1)S(1)}, u32[]{:S(2)}, u32[]{:S(2)}) collective-permute-start(bf16[32,1408]{1,0:T(8,128)(2,1)S(1)} %get-tuple-element.23), channel_id=1, source_target_pairs={{0,128},{64,192},{128,0},{192,64},{1,129},{65,193},{129,1},{193,65... | collective-permute-start | bytes 270344 | tf_op jit(solution)/shard_map/ppermute | solution.py:157
  247.9 7.3 %collective-permute-start.18 = (bf16[32,1408]{1,0:T(8,128)(2,1)S(1)}, bf16[32,1408]{1,0:T(8,128)(2,1)S(1)}, u32[]{:S(2)}, u32[]{:S(2)}) collective-permute-start(bf16[32,1408]{1,0:T(8,128)(2,1)S(1)} %get-tuple-element.22), channel_id=1, source_target_pairs={{0,64},{64,128},{128,192},{192,0},{1,65},{65,129},{129,193},{193,1... | collective-permute-start | bytes 270344 | tf_op jit(solution)/shard_map/ppermute | solution.py:157
  250.1 5.1 %copy-start.2 = (bf16[8,32,640]{2,1,0:T(8,128)(2,1)}, bf16[8,32,640]{2,1,0:T(8,128)(2,1)S(1)}, u32[]{:S(2)}) copy-start(bf16[8,32,640]{2,1,0:T(8,128)(2,1)S(1)} %all-to-all-done.4.far_ref) | copy-start | bytes 983044
  250.1 5.1 %copy-start.11 = (bf16[32,1408]{1,0:T(8,128)(2,1)}, bf16[32,1408]{1,0:T(8,128)(2,1)S(1)}, u32[]{:S(2)}) copy-start(bf16[32,1408]{1,0:T(8,128)(2,1)S(1)} %collective-permute-done.16.refs_1_) | copy-start | bytes 270340
  252.1 3.1 %copy-start.12 = (bf16[32,1408]{1,0:T(8,128)(2,1)}, bf16[32,1408]{1,0:T(8,128)(2,1)S(1)}, u32[]{:S(2)}) copy-start(bf16[32,1408]{1,0:T(8,128)(2,1)S(1)} %collective-permute-done.17.refs_2_) | copy-start | bytes 270340
  255.2 0.6 copy-start.13
Sparse Core Ops, SparseCore 0:
  51.8 62.4 all-gather.1
  191.2 40.6 reduce-scatter.1

commit v2 on v0

v2 whole, which is shorter than its diff:
```python
import jax
import jax.numpy as jnp
from jax import lax
from jax.experimental import pallas as pl
from jax.experimental.pallas import tpu as pltpu
from jax.sharding import Mesh
from jax.sharding import PartitionSpec as P


SLOTS = 32
NEAR = 1408
NORM_EPS = 1e-06
FS = ("zl", "y")
TP = ("xh", "xl", "c")


def cut_kernel(gain_ref, gate_ref, up_ref, out_ref):
    rows, width = out_ref.shape[-2:]
    diagonal = lax.broadcasted_iota(jnp.int32, (rows, rows), 0) == lax.broadcasted_iota(
        jnp.int32, (rows, rows), 1
    )
    gain = jnp.sum(jnp.where(diagonal, gain_ref[...], 0.0), axis=1, keepdims=True)
    for i, w_ref in enumerate((gate_ref, up_ref)):
        for j in range(out_ref.shape[1]):
            cols = w_ref[0, :, j * width : (j + 1) * width]
            out_ref[0, j, 0, i] = (cols * gain).astype(jnp.bfloat16)


def cut(gate, up, gain):
    _, rows, width = gate.shape
    cols = width // 4
    weights = pl.BlockSpec((1, rows, width), lambda e: (e, 0, 0))
    return pl.pallas_call(
        cut_kernel,
        grid=(4,),
        in_specs=[pl.BlockSpec((1, rows), lambda e: (0, 0)), weights, weights],
        out_specs=pl.BlockSpec((1, 4, 1, 2, rows, cols), lambda e: (e % 2, 0, e // 2, 0, 0, 0)),
        out_shape=jax.ShapeDtypeStruct((2, 4, 2, 2, rows, cols), jnp.bfloat16),
        name="cut",
    )(gain, gate, up)


def slots_of(ids, expert):
    tokens = ids.shape[1]
    chosen = (ids[0:1] == expert) | (ids[1:2] == expert)
    before = lax.broadcasted_iota(jnp.int32, (tokens, tokens), 0) < lax.broadcasted_iota(
        jnp.int32, (tokens, tokens), 1
    )
    place = jnp.dot(
        chosen.astype(jnp.float32), before.astype(jnp.float32), preferred_element_type=jnp.float32
    ).astype(jnp.int32)
    slot = lax.broadcasted_iota(jnp.int32, (SLOTS, tokens), 0)
    return (place == slot) & chosen


def dispatch_kernel(expert_ref, ids_ref, prompt_ref, out_ref):
    x = prompt_ref[...].astype(jnp.float32)
    scale = lax.rsqrt(jnp.mean(x * x, axis=1, keepdims=True) + NORM_EPS)
    normed = (x * scale).astype(jnp.bfloat16)
    pick = slots_of(ids_ref[...], expert_ref[0]).astype(jnp.bfloat16)
    out_ref[...] = jnp.dot(pick, normed, preferred_element_type=jnp.float32).astype(jnp.bfloat16)


def dispatch(expert, ids, prompt):
    return pl.pallas_call(
        dispatch_kernel,
        in_specs=[
            pl.BlockSpec(memory_space=pltpu.SMEM),
            pl.BlockSpec(memory_space=pltpu.VMEM),
            pl.BlockSpec(memory_space=pltpu.VMEM),
        ],
        out_specs=pl.BlockSpec(memory_space=pltpu.VMEM),
        out_shape=jax.ShapeDtypeStruct((SLOTS, prompt.shape[1]), jnp.bfloat16),
        name="dispatch",
    )(expert, ids, prompt)


def summed(parts):
    total = parts[0].astype(jnp.float32)
    for i in range(1, parts.shape[0]):
        total = total + parts[i].astype(jnp.float32)
    return total


def combine_kernel(expert_ref, ids_ref, weights_ref, parts_ref, out_ref):
    pick = slots_of(ids_ref[...], expert_ref[0])
    w = jnp.where(ids_ref[0:1] == expert_ref[0], weights_ref[0:1], weights_ref[1:2])
    slot_weight = jnp.sum(jnp.where(pick, w, 0.0), axis=1, keepdims=True)
    out_ref[...] = lax.dot_general(
        pick.astype(jnp.bfloat16),
        (summed(parts_ref) * slot_weight).astype(jnp.bfloat16),
        (((0,), (0,)), ((), ())),
        preferred_element_type=jnp.float32,
    ).astype(jnp.bfloat16)


def combine(expert, ids, weights, parts):
    vmem = pl.BlockSpec(memory_space=pltpu.VMEM)
    return pl.pallas_call(
        combine_kernel,
        in_specs=[pl.BlockSpec(memory_space=pltpu.SMEM), vmem, vmem, vmem],
        out_specs=vmem,
        out_shape=jax.ShapeDtypeStruct((ids.shape[1], parts.shape[2]), jnp.bfloat16),
        name="combine",
    )(expert, ids, weights, parts)


def place_kernel(at_ref, *refs):
    *pieces, gate_ref, up_ref = refs
    rows = gate_ref.shape[2]
    for k, piece in enumerate(pieces):
        gate_ref[k ^ at_ref[0]] = piece[:, :rows]
        up_ref[k ^ at_ref[0]] = piece[:, rows:]


def place(at, pieces):
    vmem = pl.BlockSpec(memory_space=pltpu.VMEM)
    ys, rows, cols = pieces[0].shape
    out = jax.ShapeDtypeStruct((len(pieces), ys, rows // 2, cols), jnp.bfloat16)
    return pl.pallas_call(
        place_kernel,
        in_specs=[pl.BlockSpec(memory_space=pltpu.SMEM)] + [vmem] * len(pieces),
        out_specs=[vmem, vmem],
        out_shape=[out, out],
        name="place",
    )(at, *pieces)


def place_cols_kernel(at_ref, blocks_ref, out_ref):
    out_ref[...] = blocks_ref[0, 0]


def place_cols(at, blocks):
    parts, pieces, rows, width = blocks.shape
    return pl.pallas_call(
        place_cols_kernel,
        grid_spec=pltpu.PrefetchScalarGridSpec(
            num_scalar_prefetch=1,
            grid=(pieces, parts),
            in_specs=[pl.BlockSpec((1, 1, rows, width), lambda k, i, at: (i, k, 0, 0))],
            out_specs=pl.BlockSpec((rows, width), lambda k, i, at: (0, (k ^ at[0]) * parts + i)),
        ),
        out_shape=jax.ShapeDtypeStruct((rows, pieces * parts * width), jnp.bfloat16),
        name="place_cols",
    )(at, blocks)


def exchange(value, axes):
    return lax.all_to_all(value, axes, split_axis=0, concat_axis=0, tiled=True)


def rows_of_line(rows, zl):
    count = lax.axis_size("zl")
    behind = [rows]
    for step in range(1, count):
        pairs = [(z, (z - step) % count) for z in range(count)]
        behind.append(lax.ppermute(rows, "zl", pairs))
    twice = jnp.stack(behind + behind)
    return lax.dynamic_slice_in_dim(twice, (count - zl) % count, count, 0)


def by_half(by_core, zl):
    rows, cols = by_core.shape[-2:]
    by_y = exchange(by_core.reshape(16, rows, cols), ("y", "xl"))
    by_y = by_y.reshape(8, 2, rows, cols)
    own = lax.dynamic_index_in_dim(by_y, zl & 1, 1, keepdims=False)
    other = lax.dynamic_index_in_dim(by_y, 1 - (zl & 1), 1, keepdims=False)
    return own, other


def to_servers(own, other, zl, gr):
    pieces = []
    for k in range(4):
        pairs = []
        for g in range(2):
            for a in range(4):
                for p in range(2):
                    r, low = (k ^ a) >> 1, (k ^ a) & 1
                    pairs.append((g * 8 + a * 2 + p, r * 8 + (2 * p + low) * 2 + g))
        pieces.append(lax.ppermute(other if k & 1 else own, ("gr", "zl", "xh"), pairs))
    return place((2 * gr + (zl & 1)).reshape(1), pieces)


def down_to_servers(down, gr):
    pieces = []
    for k in range(2):
        pairs = [(g * 2 + p, (k ^ p) * 2 + g) for g in range(2) for p in range(2)]
        pieces.append(lax.ppermute(down, ("gr", "xh"), pairs))
    blocks = jnp.stack(pieces, axis=1)
    blocks = exchange(blocks, ("xl", "c"))
    return place_cols(gr.reshape(1), blocks)


def body(prompt, expert_ids, route_weights, gate_master, up_master, down_master, ffn_gain):
    gr, zl = lax.axis_index("gr"), lax.axis_index("zl")
    depth, servers = lax.axis_size("zl"), lax.axis_size(TP)
    expert = lax.axis_index(TP).reshape(1)
    ids, weights = expert_ids.T, route_weights.T
    width = prompt.shape[1]

    down_serving = down_to_servers(down_master.astype(jnp.bfloat16), gr)
    blocks = cut(gate_master, up_master, ffn_gain[None, :])
    by_core = exchange(blocks.reshape(2, 4, 2, -1, blocks.shape[-1]), "c")
    own_rows = dispatch(expert, ids, prompt)
    own, other = by_half(by_core, zl)
    own, other, rows = lax.optimization_barrier((own, other, rows_of_line(own_rows, zl)))
    gate, up = to_servers(own, other, zl, gr)
    gate_serving = gate.reshape(-1, gate.shape[-1])
    up_serving = up.reshape(-1, up.shape[-1])

    rows = lax.all_gather(rows, "y", axis=0, tiled=True).reshape(-1, width)
    gate_part = jnp.dot(rows, gate_serving, preferred_element_type=jnp.float32)
    up_part = jnp.dot(rows, up_serving, preferred_element_type=jnp.float32)
    hidden = (jax.nn.silu(gate_part) * up_part).astype(jnp.bfloat16)
    near = jnp.dot(hidden, down_serving[:, :NEAR], preferred_element_type=jnp.float32)
    near = near.astype(jnp.bfloat16).reshape(-1, SLOTS, NEAR)
    near = lax.psum_scatter(near, "y", scatter_dimension=0, tiled=True)
    by_depth = hidden.reshape(-1, depth, SLOTS, hidden.shape[1]).transpose(1, 0, 2, 3)
    by_depth = by_depth.reshape(hidden.shape)
    far = jnp.dot(by_depth, down_serving[:, NEAR:], preferred_element_type=jnp.float32)
    far = exchange(far.astype(jnp.bfloat16).reshape(depth, -1, width - NEAR), "zl")
    far = summed(far).astype(jnp.bfloat16).reshape(-1, SLOTS, width - NEAR)
    far = exchange(far, "y")
    far = combine(expert, ids, weights, far)
    far = exchange(far.reshape(servers, -1, width - NEAR), TP)
    near = combine(expert, ids, weights, exchange(near, "zl"))
    near = exchange(near.reshape(servers, -1, NEAR), TP)
    mixed = jnp.concatenate([summed(near), summed(far)], axis=1).astype(jnp.bfloat16)
    return (gate_serving[None], up_serving[None], down_serving[None], mixed)


def solution(mesh):
    split = Mesh(
        mesh.devices.reshape(2, 4, 8, 2, 2, 2), ("gr", "zl", "y", "xh", "xl", "c")
    )
    placed = (
        P(("gr", *FS), None),
        P(("gr", *FS), None),
        P(("gr", *FS), None),
        P("gr", FS, TP),
        P("gr", FS, TP),
        P("gr", FS, TP),
        P(FS),
    )
    return jax.shard_map(
        body,
        mesh=split,
        in_specs=placed,
        out_specs=(P(TP, None, FS), P(TP, None, FS), P(TP, FS, None), P(("gr", *FS, *TP), None)),
        check_vma=False,
    )
```

time: 318 us -> 300 us (0.943)
  waiting for transfers between devices: 116 us -> 90.9 us
  local copies, waits for them, and re-layouts: 4.18 us -> 10.4 us
  blocking collectives: 62.7 us -> 68.5 us
  matrix products: 13.5 us -> 8.3 us
    reduce_scatter x1, waiting for transfers between devices: 66.1 us -> 0.01 us  [body(): near = lax.psum_scatter(near, 'y', scatter_dimension=0, tiled=True)]
    ppermute x8 -> x4, waiting for transfers between devices: 4.61 us -> 45.1 us  [to_servers(): lax.ppermute(other if k & 1 else own, ('gr', 'zl', 'xh'), pairs)]
    ppermute x8 -> x4, starting transfers between devices: 60 us -> 20.9 us  [to_servers(): lax.ppermute(other if k & 1 else own, ('gr', 'zl', 'xh'), pairs)]
    all_to_all x3 -> x5, starting transfers between devices: 17.6 us -> 40.7 us  [exchange(): return lax.all_to_all(value, axes, split_axis=0, concat_axis=0, tiled=True)]
    all_to_all x3 -> x5, waiting for transfers between devices: 22.5 us -> 36.1 us  [exchange(): return lax.all_to_all(value, axes, split_axis=0, concat_axis=0, tiled=True)]
    ppermute x2, waiting for transfers between devices: 22.5 us -> 9.7 us  [down_to_servers(): pieces.append(lax.ppermute(down, ('gr', 'xh'), pairs))]
    ppermute x0 -> x3, starting transfers between devices: none -> 12.7 us  [rows_of_line(): behind.append(lax.ppermute(rows, 'zl', pairs))]
    all_to_all x4 -> x3, blocking collectives: 62.7 us -> 68.5 us  [exchange(): return lax.all_to_all(value, axes, split_axis=0, concat_axis=0, tiled=True)]
  transfers between devices with their start and end apart: 15 -> 16, of which waited for: 4 -> 6; matrix products, arithmetic and copies ran while one was open for 1% -> 3% of each run, Pallas kernels for 4% -> 5%
where the time goes in v2:
time: 300 us; the launch traced here: 298 us
  waiting for transfers between devices  90.9 us (30%)
  starting transfers between devices  85.7 us (29%)
  blocking collectives  68.5 us (23%)
  Pallas kernels  18.3 us (6%)
  between operations  14.3 us (5%)
  local copies, waits for them, and re-layouts  10.4 us (3%)
  matrix products  8.3 us (3%)
    all_to_all x3, blocking collectives, exchange(): return lax.all_to_all(value, axes, split_axis=0, concat_axis=0, tiled=True)  68.5 us
    ppermute x4, waiting for transfers between devices, to_servers(): lax.ppermute(other if k & 1 else own, ('gr', 'zl', 'xh'), pairs)  45.1 us
    all_to_all x5, starting transfers between devices, exchange(): return lax.all_to_all(value, axes, split_axis=0, concat_axis=0, tiled=True)  40.7 us
    all_to_all x5, waiting for transfers between devices, exchange(): return lax.all_to_all(value, axes, split_axis=0, concat_axis=0, tiled=True)  36.1 us
    ppermute x4, starting transfers between devices, to_servers(): lax.ppermute(other if k & 1 else own, ('gr', 'zl', 'xh'), pairs)  20.9 us
    ppermute x3, starting transfers between devices, rows_of_line(): behind.append(lax.ppermute(rows, 'zl', pairs))  12.7 us
    ppermute x2, starting transfers between devices, down_to_servers(): pieces.append(lax.ppermute(down, ('gr', 'xh'), pairs))  11.4 us
    ppermute x2, waiting for transfers between devices, down_to_servers(): pieces.append(lax.ppermute(down, ('gr', 'xh'), pairs))  9.7 us
  transfers between devices with their start and end apart: 16, of which 6 were waited for; matrix products, arithmetic and copies ran while one was open for 3% of the time, Pallas kernels for 5%

profile of v2, /device:TPU:1, one launch (start us, length us, event | category | flops | bytes accessed | tf_op | source)
XLA Modules:
  0.0 298.4 jit_solution(599295711436663739)
XLA Ops:
  7.2 2.1 dispatch.1
  9.3 8.6 %collective-permute-start = (bf16[32,2048]{1,0:T(8,128)(2,1)}, bf16[32,2048]{1,0:T(8,128)(2,1)S(1)}, u32[]{:S(2)}, u32[]{:S(2)}) collective-permute-start(bf16[32,2048]{1,0:T(8,128)(2,1)} %dispatch.1), channel_id=1, source_target_pairs={{0,192},{64,0},{128,64},{192,128},{1,193},{65,1},{129,65},{193,129... | collective-permute-start | bytes 393224 | tf_op jit(solution)/shard_map/ppermute | solution.py:157
  17.9 1.9 collective-permute-start.1
  19.8 2.2 collective-permute-start.2
  22.0 3.8 %cut.1 = bf16[2,4,2,2,64,256]{5,4,3,2,1,0:T(8,128)(2,1)} custom-call(f32[1,64]{1,0:T(1,128)} %bitcast.71, f32[4,64,1024]{2,1,0:T(8,128)} %gate_ref.1, f32[4,64,1024]{2,1,0:T(8,128)} %up_ref.1), custom_call_target="tpu_custom_call" | custom-call | tf_op jit(solution)/shard_map/cut/pallas_call | solution.py:33
  25.8 8.2 %all_to_all.40 = bf16[2,4,2,128,256]{4,3,2,1,0:T(8,128)(2,1)} all-to-all(bf16[2,4,2,128,256]{4,3,2,1,0:T(8,128)(2,1)} %bitcast.57), channel_id=1, replica_groups=mesh['gr'=2,'zl'=4,'y'=8,'xh'=2,'xl'=2,'c'=2] {'c'}, dimensions={0} | all-to-all | bytes 2097152 | tf_op jit(solution)/shard_map/all_to_all | solution.py:149
  34.0 7.2 %all-to-all-start.1 = ((bf16[16,128,256]{2,1,0:T(8,128)(2,1)}), bf16[16,128,256]{2,1,0:T(8,128)(2,1)S(1)}, u32[]{:S(2)}, u32[]{:S(2)}) async-start(bf16[16,128,256]{2,1,0:T(8,128)(2,1)} %bitcast.3), calls=%async_computation.1 | async-start | bytes 2097152 | tf_op jit(solution)/shard_map/all_to_all | solution.py:149
  41.2 0.0 all-gather.2.cloned.1.call-start
  41.2 0.7 bitcast_dynamic-update-slice_fusion.6
  41.9 0.0 collective-permute-done
  41.9 0.7 bitcast_dynamic-update-slice_fusion.4
  42.6 0.0 collective-permute-done.1
  42.6 0.7 bitcast_dynamic-update-slice_fusion.2
  43.2 0.0 collective-permute-done.2
  43.2 0.7 bitcast_dynamic-update-slice_fusion
  43.9 0.7 bitcast_dynamic-update-slice_fusion.7
  44.6 0.7 bitcast_dynamic-update-slice_fusion.5
  45.2 0.7 bitcast_dynamic-update-slice_fusion.3
  45.9 0.7 bitcast_dynamic-update-slice_fusion.1
  46.6 1.9 constant_dynamic-slice_fusion
  48.5 18.4 %all-to-all-done.1 = bf16[16,128,256]{2,1,0:T(8,128)(2,1)S(1)} async-done(((bf16[16,128,256]{2,1,0:T(8,128)(2,1)}), bf16[16,128,256]{2,1,0:T(8,128)(2,1)S(1)}, u32[]{:S(2)}, u32[]{:S(2)}) %all-to-all-start.1) | async-done | bytes 1048608 | tf_op jit(solution)/shard_map/all_to_all | solution.py:149
  66.8 1.0 dynamic-slice_bitcast_fusion
  67.9 0.0 all-gather.2.cloned.1.call-update
  67.9 0.1 convert_element_type.115
  68.0 0.7 collective-permute-start.7
  68.7 10.7 %collective-permute-start.8 = (bf16[4,256,256]{2,1,0:T(8,128)(2,1)S(1)}, bf16[4,256,256]{2,1,0:T(8,128)(2,1)S(1)}, u32[]{:S(2)}, u32[]{:S(2)}) collective-permute-start(bf16[4,256,256]{2,1,0:T(8,128)(2,1)S(1)} %convert_element_type.115), channel_id=1, source_target_pairs={{0,256},{4,0},{256,260},{260,4},{1,257},{5,1},{257,261},{261,5},{2... | collective-permute-start | bytes 1572872 | tf_op jit(solution)/shard_map/ppermute | solution.py:188
  79.4 0.0 collective-permute-done.7
  79.4 9.7 %collective-permute-done.8 = bf16[4,256,256]{2,1,0:T(8,128)(2,1)S(1)} collective-permute-done((bf16[4,256,256]{2,1,0:T(8,128)(2,1)S(1)}, bf16[4,256,256]{2,1,0:T(8,128)(2,1)S(1)}, u32[]{:S(2)}, u32[]{:S(2)}) %collective-permute-start.8) | collective-permute-done | bytes 524320 | tf_op jit(solution)/shard_map/ppermute | solution.py:188
  89.1 1.1 pad_maximum_fusion
  90.1 17.0 %all-to-all-start.2 = ((bf16[4,2,256,256]{3,2,1,0:T(8,128)(2,1)}), bf16[4,2,256,256]{3,2,1,0:T(8,128)(2,1)S(1)}, u32[]{:S(2)}, u32[]{:S(2)}) async-start(bf16[4,2,256,256]{3,2,1,0:T(8,128)(2,1)} %pad_maximum_fusion), calls=%async_computation.2 | async-start | bytes 2097152 | tf_op jit(solution)/shard_map/all_to_all | solution.py:149
  107.2 1.7 collective-permute-start.3
  108.9 2.6 collective-permute-start.4
  111.5 13.9 %collective-permute-start.5 = (bf16[8,128,256]{2,1,0:T(8,128)(2,1)}, bf16[8,128,256]{2,1,0:T(8,128)(2,1)S(1)}, u32[]{:S(2)}, u32[]{:S(2)}) collective-permute-start(bf16[8,128,256]{2,1,0:T(8,128)(2,1)} %get-tuple-element.9), channel_id=1, source_target_pairs={{0,256},{4,384},{64,320},{68,448},{128,0},{132,128},{192,64},{196,... | collective-permute-start | bytes 1572872 | tf_op jit(solution)/shard_map/ppermute | solution.py:180
  125.4 2.7 collective-permute-start.6
  128.1 0.0 all-to-all-done.2.blocks_ref
  128.1 0.0 copy-start.1
  128.2 1.0 copy-done.1
  129.1 5.2 %place_cols.1 = bf16[256,2048]{1,0:T(8,128)(2,1)} custom-call(s32[1]{0:T(128)} %bitcast.15.at_ref, bf16[4,2,256,256]{3,2,1,0:T(8,128)(2,1)} %copy-done.1), custom_call_target="tpu_custom_call" | custom-call | tf_op jit(solution)/shard_map/place_cols/pallas_call | solution.py:135
  134.3 0.0 collective-permute-done.3.refs_0_
  134.3 0.0 collective-permute-done.4.refs_1_
  134.3 45.1 %collective-permute-done.5.refs_2_ = bf16[8,128,256]{2,1,0:T(8,128)(2,1)S(1)} collective-permute-done((bf16[8,128,256]{2,1,0:T(8,128)(2,1)}, bf16[8,128,256]{2,1,0:T(8,128)(2,1)S(1)}, u32[]{:S(2)}, u32[]{:S(2)}) %collective-permute-start.5) | collective-permute-done | bytes 524320 | tf_op jit(solution)/shard_map/ppermute | solution.py:180
  179.4 0.0 collective-permute-done.6.refs_3_
  179.5 0.8 copy-done.7
  180.2 0.2 copy-done.8
  180.4 3.0 place.1
  183.4 3.9 %fusion.4 = f32[1024,256]{1,0:T(8,128)S(1)} fusion(bf16[1024,2048]{1,0:T(8,128)(2,1)} %bitcast.72, bf16[2048,256]{1,0:T(8,128)(2,1)} %bitcast.74), kind=kOutput, calls=%fused_computation.23 | convolution fusion | flops 1073741824 | bytes 6291456 | tf_op jit(solution)/shard_map/dot_general | solution.py:212
  187.3 0.2 copy-done.9
  187.5 1.3 multiply_convert_fusion
  188.8 2.5 convolution_convert_fusion
  191.3 0.0 reduce-scatter.2.cloned.1.call-update
  191.4 0.6 convolution_convert_fusion.1
  192.0 43.4 %all_to_all.41 = bf16[4,256,640]{2,1,0:T(8,128)(2,1)S(1)} all-to-all(bf16[4,256,640]{2,1,0:T(8,128)(2,1)S(1)} %bitcast.55), channel_id=1, replica_groups=mesh['gr'=2,'zl'=4,'y'=8,'xh'=2,'xl'=2,'c'=2] {'zl'}, dimensions={0} | all-to-all | bytes 2621440 | tf_op jit(solution)/shard_map/all_to_all | solution.py:149
  235.4 0.2 add_convert_fusion
  235.6 16.8 %all_to_all.42.parts_ref = bf16[8,32,640]{2,1,0:T(8,128)(2,1)} all-to-all(bf16[8,32,640]{2,1,0:T(8,128)(2,1)S(1)} %bitcast.62), channel_id=1, replica_groups=mesh['gr'=2,'zl'=4,'y'=8,'xh'=2,'xl'=2,'c'=2] {'y'}, dimensions={0} | all-to-all | bytes 655360 | tf_op jit(solution)/shard_map/all_to_all | solution.py:149
  252.4 4.9 %all-to-all-start.3 = ((bf16[4,32,1408]{2,1,0:T(8,128)(2,1)}), bf16[4,32,1408]{2,1,0:T(8,128)(2,1)S(1)}, u32[]{:S(2)}, u32[]{:S(2)}) async-start(bf16[4,32,1408]{2,1,0:T(8,128)(2,1)} %reduce-scatter.2.cloned.1.call-done), calls=%async_computation.4 | async-start | bytes 720896 | tf_op jit(solution)/shard_map/all_to_all | solution.py:149
  257.2 2.1 combine.3
  259.3 7.0 %all-to-all-done.3.parts_ref = bf16[4,32,1408]{2,1,0:T(8,128)(2,1)S(1)} async-done(((bf16[4,32,1408]{2,1,0:T(8,128)(2,1)}), bf16[4,32,1408]{2,1,0:T(8,128)(2,1)S(1)}, u32[]{:S(2)}, u32[]{:S(2)}) %all-to-all-start.3) | async-done | bytes 360480 | tf_op jit(solution)/shard_map/all_to_all | solution.py:149
  266.3 7.4 %all-to-all-start.7 = ((bf16[8,16,640]{2,1,0:T(8,128)(2,1)}), bf16[8,16,640]{2,1,0:T(8,128)(2,1)S(1)}, u32[]{:S(2)}, u32[]{:S(2)}) async-start(bf16[8,16,640]{2,1,0:T(8,128)(2,1)} %bitcast.63), calls=%async_computation.8 | async-start | bytes 327680 | tf_op jit(solution)/shard_map/all_to_all | solution.py:149
  273.6 2.2 combine.2
  275.8 3.3 %all-to-all-done.7 = bf16[8,16,640]{2,1,0:T(8,128)(2,1)S(1)} async-done(((bf16[8,16,640]{2,1,0:T(8,128)(2,1)}), bf16[8,16,640]{2,1,0:T(8,128)(2,1)S(1)}, u32[]{:S(2)}, u32[]{:S(2)}) %all-to-all-start.7) | async-done | bytes 163872 | tf_op jit(solution)/shard_map/all_to_all | solution.py:149
  279.2 4.3 %all-to-all-start.4 = ((bf16[8,16,1408]{2,1,0:T(8,128)(2,1)}), bf16[8,16,1408]{2,1,0:T(8,128)(2,1)S(1)}, u32[]{:S(2)}, u32[]{:S(2)}) async-start(bf16[8,16,1408]{2,1,0:T(8,128)(2,1)} %bitcast.61), calls=%async_computation.5 | async-start | bytes 720896 | tf_op jit(solution)/shard_map/all_to_all | solution.py:149
  283.4 7.4 %all-to-all-done.4 = bf16[8,16,1408]{2,1,0:T(8,128)(2,1)S(1)} async-done(((bf16[8,16,1408]{2,1,0:T(8,128)(2,1)}), bf16[8,16,1408]{2,1,0:T(8,128)(2,1)S(1)}, u32[]{:S(2)}, u32[]{:S(2)}) %all-to-all-start.4) | async-done | bytes 360480 | tf_op jit(solution)/shard_map/all_to_all | solution.py:149
  290.8 0.1 fusion.2
  290.9 0.6 pad_maximum_fusion.1
  (22 shorter events, 0.1 us)
Async XLA Ops:
  9.3 31.9 %copy-start.3 = (bf16[32,2048]{1,0:T(8,128)(2,1)S(1)}, bf16[32,2048]{1,0:T(8,128)(2,1)}, u32[]{:S(2)}) copy-start(bf16[32,2048]{1,0:T(8,128)(2,1)} %dispatch.1) | copy-start | bytes 393220
  9.3 32.6 %collective-permute-start = (bf16[32,2048]{1,0:T(8,128)(2,1)}, bf16[32,2048]{1,0:T(8,128)(2,1)S(1)}, u32[]{:S(2)}, u32[]{:S(2)}) collective-permute-start(bf16[32,2048]{1,0:T(8,128)(2,1)} %dispatch.1), channel_id=1, source_target_pairs={{0,192},{64,0},{128,64},{192,128},{1,193},{65,1},{129,65},{193,129... | collective-permute-start | bytes 393224 | tf_op jit(solution)/shard_map/ppermute | solution.py:157
  17.9 24.7 %collective-permute-start.1 = (bf16[32,2048]{1,0:T(8,128)(2,1)}, bf16[32,2048]{1,0:T(8,128)(2,1)S(1)}, u32[]{:S(2)}, u32[]{:S(2)}) collective-permute-start(bf16[32,2048]{1,0:T(8,128)(2,1)} %dispatch.1), channel_id=1, source_target_pairs={{0,128},{64,192},{128,0},{192,64},{1,129},{65,193},{129,1},{193,65... | collective-permute-start | bytes 393224 | tf_op jit(solution)/shard_map/ppermute | solution.py:157
  19.8 23.5 %collective-permute-start.2 = (bf16[32,2048]{1,0:T(8,128)(2,1)}, bf16[32,2048]{1,0:T(8,128)(2,1)S(1)}, u32[]{:S(2)}, u32[]{:S(2)}) collective-permute-start(bf16[32,2048]{1,0:T(8,128)(2,1)} %dispatch.1), channel_id=1, source_target_pairs={{0,64},{64,128},{128,192},{192,0},{1,65},{65,129},{129,193},{193,1... | collective-permute-start | bytes 393224 | tf_op jit(solution)/shard_map/ppermute | solution.py:157
  34.0 33.9 %copy-start.4 = (f32[4,256,256]{2,1,0:T(8,128)S(1)}, f32[4,256,256]{2,1,0:T(8,128)}, u32[]{:S(2)}) copy-start(f32[4,256,256]{2,1,0:T(8,128)} %param.12) | copy-start | bytes 3145732
  34.0 32.8 %all-to-all-start.1 = ((bf16[16,128,256]{2,1,0:T(8,128)(2,1)}), bf16[16,128,256]{2,1,0:T(8,128)(2,1)S(1)}, u32[]{:S(2)}, u32[]{:S(2)}) async-start(bf16[16,128,256]{2,1,0:T(8,128)(2,1)} %bitcast.3), calls=%async_computation.1 | async-start | bytes 2097152 | tf_op jit(solution)/shard_map/all_to_all | solution.py:149
  41.2 142.2 %all-gather.2.cloned.1.call-start = ((), (), s32[]{:S(2)}) async-start(), calls=%async_computation.9 | async-start | bytes 4718592 | tf_op jit(solution)/shard_map/all_gather | solution.py:211
  68.0 11.4 %collective-permute-start.7 = (bf16[4,256,256]{2,1,0:T(8,128)(2,1)S(1)}, bf16[4,256,256]{2,1,0:T(8,128)(2,1)S(1)}, u32[]{:S(2)}, u32[]{:S(2)}) collective-permute-start(bf16[4,256,256]{2,1,0:T(8,128)(2,1)S(1)} %convert_element_type.115), channel_id=1, source_target_pairs={{0,0},{4,256},{256,4},{260,260},{1,1},{5,257},{257,5},{261,261},{2... | collective-permute-start | bytes 1572872 | tf_op jit(solution)/shard_map/ppermute | solution.py:188
  68.7 20.4 %collective-permute-start.8 = (bf16[4,256,256]{2,1,0:T(8,128)(2,1)S(1)}, bf16[4,256,256]{2,1,0:T(8,128)(2,1)S(1)}, u32[]{:S(2)}, u32[]{:S(2)}) collective-permute-start(bf16[4,256,256]{2,1,0:T(8,128)(2,1)S(1)} %convert_element_type.115), channel_id=1, source_target_pairs={{0,256},{4,0},{256,260},{260,4},{1,257},{5,1},{257,261},{261,5},{2... | collective-permute-start | bytes 1572872 | tf_op jit(solution)/shard_map/ppermute | solution.py:188
  90.1 38.0 %all-to-all-start.2 = ((bf16[4,2,256,256]{3,2,1,0:T(8,128)(2,1)}), bf16[4,2,256,256]{3,2,1,0:T(8,128)(2,1)S(1)}, u32[]{:S(2)}, u32[]{:S(2)}) async-start(bf16[4,2,256,256]{3,2,1,0:T(8,128)(2,1)} %pad_maximum_fusion), calls=%async_computation.2 | async-start | bytes 2097152 | tf_op jit(solution)/shard_map/all_to_all | solution.py:149
  107.2 145.2 %reduce-scatter.2.cloned.1.call-start = ((), (), s32[]{:S(2)}) async-start(), calls=%async_computation.10 | async-start | bytes 3244032 | tf_op jit(solution)/shard_map/reduce_scatter | solution.py:217
  107.2 27.1 %collective-permute-start.3 = (bf16[8,128,256]{2,1,0:T(8,128)(2,1)}, bf16[8,128,256]{2,1,0:T(8,128)(2,1)S(1)}, u32[]{:S(2)}, u32[]{:S(2)}) collective-permute-start(bf16[8,128,256]{2,1,0:T(8,128)(2,1)} %get-tuple-element.9), channel_id=1, source_target_pairs={{0,0},{4,128},{64,64},{68,192},{128,256},{132,384},{192,320},{196,... | collective-permute-start | bytes 1572872 | tf_op jit(solution)/shard_map/ppermute | solution.py:180
  108.9 25.4 %collective-permute-start.4 = (bf16[8,128,256]{2,1,0:T(8,128)(2,1)}, bf16[8,128,256]{2,1,0:T(8,128)(2,1)S(1)}, u32[]{:S(2)}, u32[]{:S(2)}) collective-permute-start(bf16[8,128,256]{2,1,0:T(8,128)(2,1)} %get-tuple-element.10), channel_id=1, source_target_pairs={{0,64},{4,192},{64,0},{68,128},{128,320},{132,448},{192,256},{196,... | collective-permute-start | bytes 1572872 | tf_op jit(solution)/shard_map/ppermute | solution.py:180
  111.5 67.9 %collective-permute-start.5 = (bf16[8,128,256]{2,1,0:T(8,128)(2,1)}, bf16[8,128,256]{2,1,0:T(8,128)(2,1)S(1)}, u32[]{:S(2)}, u32[]{:S(2)}) collective-permute-start(bf16[8,128,256]{2,1,0:T(8,128)(2,1)} %get-tuple-element.9), channel_id=1, source_target_pairs={{0,256},{4,384},{64,320},{68,448},{128,0},{132,128},{192,64},{196,... | collective-permute-start | bytes 1572872 | tf_op jit(solution)/shard_map/ppermute | solution.py:180
  125.4 54.0 %collective-permute-start.6 = (bf16[8,128,256]{2,1,0:T(8,128)(2,1)}, bf16[8,128,256]{2,1,0:T(8,128)(2,1)S(1)}, u32[]{:S(2)}, u32[]{:S(2)}) collective-permute-start(bf16[8,128,256]{2,1,0:T(8,128)(2,1)} %get-tuple-element.10), channel_id=1, source_target_pairs={{0,320},{4,448},{64,256},{68,384},{128,64},{132,192},{192,0},{196,... | collective-permute-start | bytes 1572872 | tf_op jit(solution)/shard_map/ppermute | solution.py:180
  128.1 1.0 copy-start.1
  134.3 45.1 %copy-start.5 = (bf16[8,128,256]{2,1,0:T(8,128)(2,1)}, bf16[8,128,256]{2,1,0:T(8,128)(2,1)S(1)}, u32[]{:S(2)}) copy-start(bf16[8,128,256]{2,1,0:T(8,128)(2,1)S(1)} %collective-permute-done.3.refs_0_) | copy-start | bytes 1572868
  134.3 45.1 %copy-start.6 = (bf16[8,128,256]{2,1,0:T(8,128)(2,1)}, bf16[8,128,256]{2,1,0:T(8,128)(2,1)S(1)}, u32[]{:S(2)}) copy-start(bf16[8,128,256]{2,1,0:T(8,128)(2,1)S(1)} %collective-permute-done.4.refs_1_) | copy-start | bytes 1572868
  179.4 0.8 copy-start.7
  179.4 1.0 copy-start.8
  183.4 3.9 %copy-start.10 = (bf16[4,8,64,256]{3,2,1,0:T(8,128)(2,1)S(1)}, bf16[4,8,64,256]{3,2,1,0:T(8,128)(2,1)}, u32[]{:S(2)}) copy-start(bf16[4,8,64,256]{3,2,1,0:T(8,128)(2,1)} %get-tuple-element.12) | copy-start | bytes 3145732
  183.4 4.1 %copy-start.9 = (bf16[32,32,2048]{2,1,0:T(8,128)(2,1)S(1)}, bf16[32,32,2048]{2,1,0:T(8,128)(2,1)}, u32[]{:S(2)}) copy-start(bf16[32,32,2048]{2,1,0:T(8,128)(2,1)} %all-gather.2.cloned.1.call-done) | copy-start | bytes 12582916
  187.5 1.3 copy-start
  252.4 13.9 %all-to-all-start.3 = ((bf16[4,32,1408]{2,1,0:T(8,128)(2,1)}), bf16[4,32,1408]{2,1,0:T(8,128)(2,1)S(1)}, u32[]{:S(2)}, u32[]{:S(2)}) async-start(bf16[4,32,1408]{2,1,0:T(8,128)(2,1)} %reduce-scatter.2.cloned.1.call-done), calls=%async_computation.4 | async-start | bytes 720896 | tf_op jit(solution)/shard_map/all_to_all | solution.py:149
  266.3 7.4 %copy-start.2 = (bf16[4,32,1408]{2,1,0:T(8,128)(2,1)}, bf16[4,32,1408]{2,1,0:T(8,128)(2,1)S(1)}, u32[]{:S(2)}) copy-start(bf16[4,32,1408]{2,1,0:T(8,128)(2,1)S(1)} %all-to-all-done.3.parts_ref) | copy-start | bytes 1081348
  266.3 12.9 %all-to-all-start.7 = ((bf16[8,16,640]{2,1,0:T(8,128)(2,1)}), bf16[8,16,640]{2,1,0:T(8,128)(2,1)S(1)}, u32[]{:S(2)}, u32[]{:S(2)}) async-start(bf16[8,16,640]{2,1,0:T(8,128)(2,1)} %bitcast.63), calls=%async_computation.8 | async-start | bytes 327680 | tf_op jit(solution)/shard_map/all_to_all | solution.py:149
  279.2 11.7 %all-to-all-start.4 = ((bf16[8,16,1408]{2,1,0:T(8,128)(2,1)}), bf16[8,16,1408]{2,1,0:T(8,128)(2,1)S(1)}, u32[]{:S(2)}, u32[]{:S(2)}) async-start(bf16[8,16,1408]{2,1,0:T(8,128)(2,1)} %bitcast.61), calls=%async_computation.5 | async-start | bytes 720896 | tf_op jit(solution)/shard_map/all_to_all | solution.py:149
Sparse Core Ops, SparseCore 0:
  68.0 58.8 all-gather.1
  191.5 49.7 reduce-scatter.1

commit v3 on v2

--- a/solution.py
+++ b/solution.py
@@ -1,3 +1,5 @@
+import itertools
+
 import jax
 import jax.numpy as jnp
 from jax import lax
@@ -8,7 +10,7 @@
 
 
 SLOTS = 32
-NEAR = 1408
+NEAR = 1664
 NORM_EPS = 1e-06
 FS = ("zl", "y")
 TP = ("xh", "xl", "c")
@@ -161,7 +163,7 @@
 
 def by_half(by_core, zl):
     rows, cols = by_core.shape[-2:]
-    by_y = exchange(by_core.reshape(16, rows, cols), ("y", "xl"))
+    by_y = exchange(by_core.reshape(16, rows, cols), ("y", "xh"))
     by_y = by_y.reshape(8, 2, rows, cols)
     own = lax.dynamic_index_in_dim(by_y, zl & 1, 1, keepdims=False)
     other = lax.dynamic_index_in_dim(by_y, 1 - (zl & 1), 1, keepdims=False)
@@ -172,13 +174,12 @@
     pieces = []
     for k in range(4):
         pairs = []
-        for g in range(2):
-            for a in range(4):
-                for p in range(2):
-                    r, low = (k ^ a) >> 1, (k ^ a) & 1
-                    pairs.append((g * 8 + a * 2 + p, r * 8 + (2 * p + low) * 2 + g))
-        pieces.append(lax.ppermute(other if k & 1 else own, ("gr", "zl", "xh"), pairs))
-    return place((2 * gr + (zl & 1)).reshape(1), pieces)
+        for g, a, e, p in itertools.product(range(2), range(4), range(2), range(2)):
+            r, high = (k ^ a) >> 1, (k ^ a) & 1
+            pairs.append((((g * 4 + a) * 2 + e) * 2 + p, ((r * 4 + 2 * high + p) * 2 + g) * 2 + e))
+        piece = other if k & 1 else own
+        pieces.append(lax.ppermute(piece, ("gr", "zl", "xh", "xl"), pairs))
+    return place((2 * gr + (zl >> 1)).reshape(1), pieces)
 
 
 def down_to_servers(down, gr):

time: 300 us -> 306 us (1.020)
  waiting for transfers between devices: 90.9 us -> 102 us
  blocking collectives: 68.5 us -> 64.2 us
    reduce_scatter x1, waiting for transfers between devices: 0.01 us -> 16.3 us  [body(): near = lax.psum_scatter(near, 'y', scatter_dimension=0, tiled=True)]
    ppermute x4, waiting for transfers between devices: 45.1 us -> 34.7 us  [to_servers(): pieces.append(lax.ppermute(piece, ('gr', 'zl', 'xh', 'xl'), pairs))]
    all_to_all x5, waiting for transfers between devices: 36.1 us -> 40.6 us  [exchange(): return lax.all_to_all(value, axes, split_axis=0, concat_axis=0, tiled=True)]
    all_to_all x3, blocking collectives: 68.5 us -> 64.2 us  [exchange(): return lax.all_to_all(value, axes, split_axis=0, concat_axis=0, tiled=True)]
  transfers between devices with their start and end apart: 16 -> 16, of which waited for: 6 -> 8; matrix products, arithmetic and copies ran while one was open for 3% -> 3% of each run, Pallas kernels for 5% -> 5%
where the time goes in v3:
time: 306 us; the launch traced here: 305 us
  waiting for transfers between devices  102 us (33%)
  starting transfers between devices  85 us (28%)
  blocking collectives  64.2 us (21%)
  Pallas kernels  18.3 us (6%)
  between operations  14.3 us (5%)
  local copies, waits for them, and re-layouts  10.3 us (3%)
  matrix products  8.44 us (3%)
    all_to_all x3, blocking collectives, exchange(): return lax.all_to_all(value, axes, split_axis=0, concat_axis=0, tiled=True)  64.2 us
    all_to_all x5, waiting for transfers between devices, exchange(): return lax.all_to_all(value, axes, split_axis=0, concat_axis=0, tiled=True)  40.6 us
    all_to_all x5, starting transfers between devices, exchange(): return lax.all_to_all(value, axes, split_axis=0, concat_axis=0, tiled=True)  38.9 us
    ppermute x4, waiting for transfers between devices, to_servers(): pieces.append(lax.ppermute(piece, ('gr', 'zl', 'xh', 'xl'), pairs))  34.7 us
    ppermute x4, starting transfers between devices, to_servers(): pieces.append(lax.ppermute(piece, ('gr', 'zl', 'xh', 'xl'), pairs))  23 us
    reduce_scatter x1, waiting for transfers between devices, body(): near = lax.psum_scatter(near, 'y', scatter_dimension=0, tiled=True)  16.3 us
    ppermute x3, starting transfers between devices, rows_of_line(): behind.append(lax.ppermute(rows, 'zl', pairs))  12.7 us
    ppermute x2, waiting for transfers between devices, down_to_servers(): pieces.append(lax.ppermute(down, ('gr', 'xh'), pairs))  10.7 us
  transfers between devices with their start and end apart: 16, of which 8 were waited for; matrix products, arithmetic and copies ran while one was open for 3% of the time, Pallas kernels for 5%

profile of v3, /device:TPU:1, one launch (start us, length us, event | category | flops | bytes accessed | tf_op | source)
XLA Modules:
  0.0 304.7 jit_solution(7223026881581609371)
XLA Ops:
  7.2 2.1 dispatch.1
  9.3 8.6 %collective-permute-start = (bf16[32,2048]{1,0:T(8,128)(2,1)}, bf16[32,2048]{1,0:T(8,128)(2,1)S(1)}, u32[]{:S(2)}, u32[]{:S(2)}) collective-permute-start(bf16[32,2048]{1,0:T(8,128)(2,1)} %dispatch.1), channel_id=1, source_target_pairs={{0,192},{64,0},{128,64},{192,128},{1,193},{65,1},{129,65},{193,129... | collective-permute-start | bytes 393224 | tf_op jit(solution)/shard_map/ppermute | solution.py:159
  17.9 1.9 collective-permute-start.1
  19.8 2.2 collective-permute-start.2
  22.0 3.8 %cut.1 = bf16[2,4,2,2,64,256]{5,4,3,2,1,0:T(8,128)(2,1)} custom-call(f32[1,64]{1,0:T(1,128)} %bitcast.71, f32[4,64,1024]{2,1,0:T(8,128)} %gate_ref.1, f32[4,64,1024]{2,1,0:T(8,128)} %up_ref.1), custom_call_target="tpu_custom_call" | custom-call | tf_op jit(solution)/shard_map/cut/pallas_call | solution.py:35
  25.8 8.2 %all_to_all.40 = bf16[2,4,2,128,256]{4,3,2,1,0:T(8,128)(2,1)} all-to-all(bf16[2,4,2,128,256]{4,3,2,1,0:T(8,128)(2,1)} %bitcast.55), channel_id=1, replica_groups=mesh['gr'=2,'zl'=4,'y'=8,'xh'=2,'xl'=2,'c'=2] {'c'}, dimensions={0} | all-to-all | bytes 2097152 | tf_op jit(solution)/shard_map/all_to_all | solution.py:151
  34.0 8.7 %all-to-all-start.1 = ((bf16[16,128,256]{2,1,0:T(8,128)(2,1)}), bf16[16,128,256]{2,1,0:T(8,128)(2,1)S(1)}, u32[]{:S(2)}, u32[]{:S(2)}) async-start(bf16[16,128,256]{2,1,0:T(8,128)(2,1)} %bitcast.3), calls=%async_computation.1 | async-start | bytes 2097152 | tf_op jit(solution)/shard_map/all_to_all | solution.py:151
  42.7 0.0 all-gather.2.cloned.1.call-start
  42.8 0.7 bitcast_dynamic-update-slice_fusion.6
  43.4 0.0 collective-permute-done
  43.4 0.7 bitcast_dynamic-update-slice_fusion.4
  44.1 0.0 collective-permute-done.1
  44.1 0.7 bitcast_dynamic-update-slice_fusion.2
  44.8 0.0 collective-permute-done.2
  44.8 0.7 bitcast_dynamic-update-slice_fusion
  45.4 0.7 bitcast_dynamic-update-slice_fusion.7
  46.1 0.7 bitcast_dynamic-update-slice_fusion.5
  46.8 0.7 bitcast_dynamic-update-slice_fusion.3
  47.4 0.7 bitcast_dynamic-update-slice_fusion.1
  48.1 1.9 constant_dynamic-slice_fusion
  50.0 19.9 %all-to-all-done.1 = bf16[16,128,256]{2,1,0:T(8,128)(2,1)S(1)} async-done(((bf16[16,128,256]{2,1,0:T(8,128)(2,1)}), bf16[16,128,256]{2,1,0:T(8,128)(2,1)S(1)}, u32[]{:S(2)}, u32[]{:S(2)}) %all-to-all-start.1) | async-done | bytes 1048608 | tf_op jit(solution)/shard_map/all_to_all | solution.py:151
  69.9 1.0 dynamic-slice_bitcast_fusion
  70.9 0.0 all-gather.2.cloned.1.call-update
  71.0 0.1 convert_element_type.115
  71.0 0.7 collective-permute-start.7
  71.7 9.7 %collective-permute-start.8 = (bf16[4,256,256]{2,1,0:T(8,128)(2,1)S(1)}, bf16[4,256,256]{2,1,0:T(8,128)(2,1)S(1)}, u32[]{:S(2)}, u32[]{:S(2)}) collective-permute-start(bf16[4,256,256]{2,1,0:T(8,128)(2,1)S(1)} %convert_element_type.115), channel_id=1, source_target_pairs={{0,256},{4,0},{256,260},{260,4},{1,257},{5,1},{257,261},{261,5},{2... | collective-permute-start | bytes 1572872 | tf_op jit(solution)/shard_map/ppermute | solution.py:189
  81.4 0.0 collective-permute-done.7
  81.5 10.7 %collective-permute-done.8 = bf16[4,256,256]{2,1,0:T(8,128)(2,1)S(1)} collective-permute-done((bf16[4,256,256]{2,1,0:T(8,128)(2,1)S(1)}, bf16[4,256,256]{2,1,0:T(8,128)(2,1)S(1)}, u32[]{:S(2)}, u32[]{:S(2)}) %collective-permute-start.8) | collective-permute-done | bytes 524320 | tf_op jit(solution)/shard_map/ppermute | solution.py:189
  92.1 1.1 pad_maximum_fusion
  93.2 15.6 %all-to-all-start.2 = ((bf16[4,2,256,256]{3,2,1,0:T(8,128)(2,1)}), bf16[4,2,256,256]{3,2,1,0:T(8,128)(2,1)S(1)}, u32[]{:S(2)}, u32[]{:S(2)}) async-start(bf16[4,2,256,256]{3,2,1,0:T(8,128)(2,1)} %pad_maximum_fusion), calls=%async_computation.2 | async-start | bytes 2097152 | tf_op jit(solution)/shard_map/all_to_all | solution.py:151
  108.7 1.7 collective-permute-start.3
  110.4 8.6 %collective-permute-start.4 = (bf16[8,128,256]{2,1,0:T(8,128)(2,1)}, bf16[8,128,256]{2,1,0:T(8,128)(2,1)S(1)}, u32[]{:S(2)}, u32[]{:S(2)}) collective-permute-start(bf16[8,128,256]{2,1,0:T(8,128)(2,1)} %get-tuple-element.10), channel_id=1, source_target_pairs={{0,128},{2,192},{4,130},{6,194},{64,0},{66,64},{68,2},{70,66},{128... | collective-permute-start | bytes 1572872 | tf_op jit(solution)/shard_map/ppermute | solution.py:181
  119.0 9.4 %collective-permute-start.5 = (bf16[8,128,256]{2,1,0:T(8,128)(2,1)}, bf16[8,128,256]{2,1,0:T(8,128)(2,1)S(1)}, u32[]{:S(2)}, u32[]{:S(2)}) collective-permute-start(bf16[8,128,256]{2,1,0:T(8,128)(2,1)} %get-tuple-element.9), channel_id=1, source_target_pairs={{0,256},{2,320},{4,258},{6,322},{64,384},{66,448},{68,386},{70,450... | collective-permute-start | bytes 1572872 | tf_op jit(solution)/shard_map/ppermute | solution.py:181
  128.4 3.4 %collective-permute-start.6 = (bf16[8,128,256]{2,1,0:T(8,128)(2,1)}, bf16[8,128,256]{2,1,0:T(8,128)(2,1)S(1)}, u32[]{:S(2)}, u32[]{:S(2)}) collective-permute-start(bf16[8,128,256]{2,1,0:T(8,128)(2,1)} %get-tuple-element.10), channel_id=1, source_target_pairs={{0,384},{2,448},{4,386},{6,450},{64,256},{66,320},{68,258},{70,322... | collective-permute-start | bytes 1572872 | tf_op jit(solution)/shard_map/ppermute | solution.py:181
  131.8 0.0 all-to-all-done.2.blocks_ref
  131.8 0.0 copy-start
  131.8 1.0 copy-done
  132.8 5.2 %place_cols.1 = bf16[256,2048]{1,0:T(8,128)(2,1)} custom-call(s32[1]{0:T(128)} %bitcast.15.at_ref, bf16[4,2,256,256]{3,2,1,0:T(8,128)(2,1)} %copy-done), custom_call_target="tpu_custom_call" | custom-call | tf_op jit(solution)/shard_map/place_cols/pallas_call | solution.py:137
  138.0 0.0 collective-permute-done.3.refs_0_
  138.0 0.0 collective-permute-done.4.refs_1_
  138.0 3.6 %collective-permute-done.5.refs_2_ = bf16[8,128,256]{2,1,0:T(8,128)(2,1)S(1)} collective-permute-done((bf16[8,128,256]{2,1,0:T(8,128)(2,1)}, bf16[8,128,256]{2,1,0:T(8,128)(2,1)S(1)}, u32[]{:S(2)}, u32[]{:S(2)}) %collective-permute-start.5) | collective-permute-done | bytes 524320 | tf_op jit(solution)/shard_map/ppermute | solution.py:181
  141.6 31.1 %collective-permute-done.6.refs_3_ = bf16[8,128,256]{2,1,0:T(8,128)(2,1)S(1)} collective-permute-done((bf16[8,128,256]{2,1,0:T(8,128)(2,1)}, bf16[8,128,256]{2,1,0:T(8,128)(2,1)S(1)}, u32[]{:S(2)}, u32[]{:S(2)}) %collective-permute-start.6) | collective-permute-done | bytes 524320 | tf_op jit(solution)/shard_map/ppermute | solution.py:181
  172.7 0.8 copy-done.8
  173.5 3.0 place.1
  176.5 3.9 %fusion.4 = f32[1024,256]{1,0:T(8,128)S(1)} fusion(bf16[1024,2048]{1,0:T(8,128)(2,1)} %bitcast.72, bf16[2048,256]{1,0:T(8,128)(2,1)} %bitcast.74), kind=kOutput, calls=%fused_computation.23 | convolution fusion | flops 1073741824 | bytes 6291456 | tf_op jit(solution)/shard_map/dot_general | solution.py:213
  180.4 0.2 copy-done.9
  180.5 1.3 multiply_convert_fusion
  181.8 2.8 convolution_convert_fusion
  184.7 0.0 reduce-scatter.2.cloned.1.call-update
  184.7 0.4 convolution_convert_fusion.1
  185.2 37.8 %all_to_all.41 = bf16[4,256,384]{2,1,0:T(8,128)(2,1)S(1)} all-to-all(bf16[4,256,384]{2,1,0:T(8,128)(2,1)S(1)} %bitcast.59), channel_id=1, replica_groups=mesh['gr'=2,'zl'=4,'y'=8,'xh'=2,'xl'=2,'c'=2] {'zl'}, dimensions={0} | all-to-all | bytes 1572864 | tf_op jit(solution)/shard_map/all_to_all | solution.py:151
  223.0 0.1 add_convert_fusion
  223.1 18.1 %all_to_all.42.parts_ref = bf16[8,32,384]{2,1,0:T(8,128)(2,1)} all-to-all(bf16[8,32,384]{2,1,0:T(8,128)(2,1)S(1)} %bitcast.62), channel_id=1, replica_groups=mesh['gr'=2,'zl'=4,'y'=8,'xh'=2,'xl'=2,'c'=2] {'y'}, dimensions={0} | all-to-all | bytes 393216 | tf_op jit(solution)/shard_map/all_to_all | solution.py:151
  241.2 16.3 %reduce-scatter.2.cloned.1.call-done = bf16[4,32,1664]{2,1,0:T(8,128)(2,1)} async-done(((bf16[32,32,1664]{2,1,0:T(8,128)(2,1)}), bf16[4,32,1664]{2,1,0:T(8,128)(2,1)}) %reduce-scatter.2.cloned.1.call-update) | async-done | bytes 426000 | tf_op jit(solution)/shard_map/reduce_scatter | solution.py:218
  257.5 4.8 %all-to-all-start.3 = ((bf16[4,32,1664]{2,1,0:T(8,128)(2,1)}), bf16[4,32,1664]{2,1,0:T(8,128)(2,1)S(1)}, u32[]{:S(2)}, u32[]{:S(2)}) async-start(bf16[4,32,1664]{2,1,0:T(8,128)(2,1)} %reduce-scatter.2.cloned.1.call-done), calls=%async_computation.4 | async-start | bytes 851968 | tf_op jit(solution)/shard_map/all_to_all | solution.py:151
  262.4 2.0 combine.3
  264.3 10.0 %all-to-all-done.3.parts_ref = bf16[4,32,1664]{2,1,0:T(8,128)(2,1)S(1)} async-done(((bf16[4,32,1664]{2,1,0:T(8,128)(2,1)}), bf16[4,32,1664]{2,1,0:T(8,128)(2,1)S(1)}, u32[]{:S(2)}, u32[]{:S(2)}) %all-to-all-start.3) | async-done | bytes 426016 | tf_op jit(solution)/shard_map/all_to_all | solution.py:151
  274.3 5.6 %all-to-all-start.7 = ((bf16[8,16,384]{2,1,0:T(8,128)(2,1)}), bf16[8,16,384]{2,1,0:T(8,128)(2,1)S(1)}, u32[]{:S(2)}, u32[]{:S(2)}) async-start(bf16[8,16,384]{2,1,0:T(8,128)(2,1)} %bitcast.65), calls=%async_computation.8 | async-start | bytes 196608 | tf_op jit(solution)/shard_map/all_to_all | solution.py:151
  279.9 2.3 combine.2
  282.2 2.7 all-to-all-done.7
  284.9 4.2 %all-to-all-start.4 = ((bf16[8,16,1664]{2,1,0:T(8,128)(2,1)}), bf16[8,16,1664]{2,1,0:T(8,128)(2,1)S(1)}, u32[]{:S(2)}, u32[]{:S(2)}) async-start(bf16[8,16,1664]{2,1,0:T(8,128)(2,1)} %bitcast.61), calls=%async_computation.5 | async-start | bytes 851968 | tf_op jit(solution)/shard_map/all_to_all | solution.py:151
  289.1 8.0 %all-to-all-done.4 = bf16[8,16,1664]{2,1,0:T(8,128)(2,1)S(1)} async-done(((bf16[8,16,1664]{2,1,0:T(8,128)(2,1)}), bf16[8,16,1664]{2,1,0:T(8,128)(2,1)S(1)}, u32[]{:S(2)}, u32[]{:S(2)}) %all-to-all-start.4) | async-done | bytes 426016 | tf_op jit(solution)/shard_map/all_to_all | solution.py:151
  297.1 0.1 fusion.2
  297.2 0.6 pad_maximum_fusion.1
  (22 shorter events, 0.1 us)
Async XLA Ops:
  9.3 33.5 %copy-start.3 = (bf16[32,2048]{1,0:T(8,128)(2,1)S(1)}, bf16[32,2048]{1,0:T(8,128)(2,1)}, u32[]{:S(2)}) copy-start(bf16[32,2048]{1,0:T(8,128)(2,1)} %dispatch.1) | copy-start | bytes 393220
  9.3 34.1 %collective-permute-start = (bf16[32,2048]{1,0:T(8,128)(2,1)}, bf16[32,2048]{1,0:T(8,128)(2,1)S(1)}, u32[]{:S(2)}, u32[]{:S(2)}) collective-permute-start(bf16[32,2048]{1,0:T(8,128)(2,1)} %dispatch.1), channel_id=1, source_target_pairs={{0,192},{64,0},{128,64},{192,128},{1,193},{65,1},{129,65},{193,129... | collective-permute-start | bytes 393224 | tf_op jit(solution)/shard_map/ppermute | solution.py:159
  17.9 26.2 %collective-permute-start.1 = (bf16[32,2048]{1,0:T(8,128)(2,1)}, bf16[32,2048]{1,0:T(8,128)(2,1)S(1)}, u32[]{:S(2)}, u32[]{:S(2)}) collective-permute-start(bf16[32,2048]{1,0:T(8,128)(2,1)} %dispatch.1), channel_id=1, source_target_pairs={{0,128},{64,192},{128,0},{192,64},{1,129},{65,193},{129,1},{193,65... | collective-permute-start | bytes 393224 | tf_op jit(solution)/shard_map/ppermute | solution.py:159
  19.8 25.0 %collective-permute-start.2 = (bf16[32,2048]{1,0:T(8,128)(2,1)}, bf16[32,2048]{1,0:T(8,128)(2,1)S(1)}, u32[]{:S(2)}, u32[]{:S(2)}) collective-permute-start(bf16[32,2048]{1,0:T(8,128)(2,1)} %dispatch.1), channel_id=1, source_target_pairs={{0,64},{64,128},{128,192},{192,0},{1,65},{65,129},{129,193},{193,1... | collective-permute-start | bytes 393224 | tf_op jit(solution)/shard_map/ppermute | solution.py:159
  34.0 37.0 %copy-start.4 = (f32[4,256,256]{2,1,0:T(8,128)S(1)}, f32[4,256,256]{2,1,0:T(8,128)}, u32[]{:S(2)}) copy-start(f32[4,256,256]{2,1,0:T(8,128)} %param.12) | copy-start | bytes 3145732
  34.0 35.9 %all-to-all-start.1 = ((bf16[16,128,256]{2,1,0:T(8,128)(2,1)}), bf16[16,128,256]{2,1,0:T(8,128)(2,1)S(1)}, u32[]{:S(2)}, u32[]{:S(2)}) async-start(bf16[16,128,256]{2,1,0:T(8,128)(2,1)} %bitcast.3), calls=%async_computation.1 | async-start | bytes 2097152 | tf_op jit(solution)/shard_map/all_to_all | solution.py:151
  42.7 133.8 %all-gather.2.cloned.1.call-start = ((), (), s32[]{:S(2)}) async-start(), calls=%async_computation.9 | async-start | bytes 4718592 | tf_op jit(solution)/shard_map/all_gather | solution.py:212
  71.0 10.4 %collective-permute-start.7 = (bf16[4,256,256]{2,1,0:T(8,128)(2,1)S(1)}, bf16[4,256,256]{2,1,0:T(8,128)(2,1)S(1)}, u32[]{:S(2)}, u32[]{:S(2)}) collective-permute-start(bf16[4,256,256]{2,1,0:T(8,128)(2,1)S(1)} %convert_element_type.115), channel_id=1, source_target_pairs={{0,0},{4,256},{256,4},{260,260},{1,1},{5,257},{257,5},{261,261},{2... | collective-permute-start | bytes 1572872 | tf_op jit(solution)/shard_map/ppermute | solution.py:189
  71.7 20.4 %collective-permute-start.8 = (bf16[4,256,256]{2,1,0:T(8,128)(2,1)S(1)}, bf16[4,256,256]{2,1,0:T(8,128)(2,1)S(1)}, u32[]{:S(2)}, u32[]{:S(2)}) collective-permute-start(bf16[4,256,256]{2,1,0:T(8,128)(2,1)S(1)} %convert_element_type.115), channel_id=1, source_target_pairs={{0,256},{4,0},{256,260},{260,4},{1,257},{5,1},{257,261},{261,5},{2... | collective-permute-start | bytes 1572872 | tf_op jit(solution)/shard_map/ppermute | solution.py:189
  93.2 38.6 %all-to-all-start.2 = ((bf16[4,2,256,256]{3,2,1,0:T(8,128)(2,1)}), bf16[4,2,256,256]{3,2,1,0:T(8,128)(2,1)S(1)}, u32[]{:S(2)}, u32[]{:S(2)}) async-start(bf16[4,2,256,256]{3,2,1,0:T(8,128)(2,1)} %pad_maximum_fusion), calls=%async_computation.2 | async-start | bytes 2097152 | tf_op jit(solution)/shard_map/all_to_all | solution.py:151
  108.7 148.8 %reduce-scatter.2.cloned.1.call-start = ((), (), s32[]{:S(2)}) async-start(), calls=%async_computation.10 | async-start | bytes 3833856 | tf_op jit(solution)/shard_map/reduce_scatter | solution.py:218
  108.7 29.2 %collective-permute-start.3 = (bf16[8,128,256]{2,1,0:T(8,128)(2,1)}, bf16[8,128,256]{2,1,0:T(8,128)(2,1)S(1)}, u32[]{:S(2)}, u32[]{:S(2)}) collective-permute-start(bf16[8,128,256]{2,1,0:T(8,128)(2,1)} %get-tuple-element.9), channel_id=1, source_target_pairs={{0,0},{2,64},{4,2},{6,66},{64,128},{66,192},{68,130},{70,194},{128... | collective-permute-start | bytes 1572872 | tf_op jit(solution)/shard_map/ppermute | solution.py:181
  110.4 27.5 %collective-permute-start.4 = (bf16[8,128,256]{2,1,0:T(8,128)(2,1)}, bf16[8,128,256]{2,1,0:T(8,128)(2,1)S(1)}, u32[]{:S(2)}, u32[]{:S(2)}) collective-permute-start(bf16[8,128,256]{2,1,0:T(8,128)(2,1)} %get-tuple-element.10), channel_id=1, source_target_pairs={{0,128},{2,192},{4,130},{6,194},{64,0},{66,64},{68,2},{70,66},{128... | collective-permute-start | bytes 1572872 | tf_op jit(solution)/shard_map/ppermute | solution.py:181
  119.0 22.6 %collective-permute-start.5 = (bf16[8,128,256]{2,1,0:T(8,128)(2,1)}, bf16[8,128,256]{2,1,0:T(8,128)(2,1)S(1)}, u32[]{:S(2)}, u32[]{:S(2)}) collective-permute-start(bf16[8,128,256]{2,1,0:T(8,128)(2,1)} %get-tuple-element.9), channel_id=1, source_target_pairs={{0,256},{2,320},{4,258},{6,322},{64,384},{66,448},{68,386},{70,450... | collective-permute-start | bytes 1572872 | tf_op jit(solution)/shard_map/ppermute | solution.py:181
  128.4 44.3 %collective-permute-start.6 = (bf16[8,128,256]{2,1,0:T(8,128)(2,1)}, bf16[8,128,256]{2,1,0:T(8,128)(2,1)S(1)}, u32[]{:S(2)}, u32[]{:S(2)}) collective-permute-start(bf16[8,128,256]{2,1,0:T(8,128)(2,1)} %get-tuple-element.10), channel_id=1, source_target_pairs={{0,384},{2,448},{4,386},{6,450},{64,256},{66,320},{68,258},{70,322... | collective-permute-start | bytes 1572872 | tf_op jit(solution)/shard_map/ppermute | solution.py:181
  131.8 1.0 copy-start
  138.0 34.7 %copy-start.5 = (bf16[8,128,256]{2,1,0:T(8,128)(2,1)}, bf16[8,128,256]{2,1,0:T(8,128)(2,1)S(1)}, u32[]{:S(2)}) copy-start(bf16[8,128,256]{2,1,0:T(8,128)(2,1)S(1)} %collective-permute-done.3.refs_0_) | copy-start | bytes 1572868
  138.0 34.7 %copy-start.6 = (bf16[8,128,256]{2,1,0:T(8,128)(2,1)}, bf16[8,128,256]{2,1,0:T(8,128)(2,1)S(1)}, u32[]{:S(2)}) copy-start(bf16[8,128,256]{2,1,0:T(8,128)(2,1)S(1)} %collective-permute-done.4.refs_1_) | copy-start | bytes 1572868
  141.6 31.1 %copy-start.7 = (bf16[8,128,256]{2,1,0:T(8,128)(2,1)}, bf16[8,128,256]{2,1,0:T(8,128)(2,1)S(1)}, u32[]{:S(2)}) copy-start(bf16[8,128,256]{2,1,0:T(8,128)(2,1)S(1)} %collective-permute-done.5.refs_2_) | copy-start | bytes 1572868
  172.7 0.8 copy-start.8
  176.5 3.9 %copy-start.10 = (bf16[4,8,64,256]{3,2,1,0:T(8,128)(2,1)S(1)}, bf16[4,8,64,256]{3,2,1,0:T(8,128)(2,1)}, u32[]{:S(2)}) copy-start(bf16[4,8,64,256]{3,2,1,0:T(8,128)(2,1)} %get-tuple-element.12) | copy-start | bytes 3145732
  176.5 4.1 %copy-start.9 = (bf16[32,32,2048]{2,1,0:T(8,128)(2,1)S(1)}, bf16[32,32,2048]{2,1,0:T(8,128)(2,1)}, u32[]{:S(2)}) copy-start(bf16[32,32,2048]{2,1,0:T(8,128)(2,1)} %all-gather.2.cloned.1.call-done) | copy-start | bytes 12582916
  180.5 1.3 copy-start.1
  257.5 16.8 %all-to-all-start.3 = ((bf16[4,32,1664]{2,1,0:T(8,128)(2,1)}), bf16[4,32,1664]{2,1,0:T(8,128)(2,1)S(1)}, u32[]{:S(2)}, u32[]{:S(2)}) async-start(bf16[4,32,1664]{2,1,0:T(8,128)(2,1)} %reduce-scatter.2.cloned.1.call-done), calls=%async_computation.4 | async-start | bytes 851968 | tf_op jit(solution)/shard_map/all_to_all | solution.py:151
  274.3 5.6 %copy-start.2 = (bf16[4,32,1664]{2,1,0:T(8,128)(2,1)}, bf16[4,32,1664]{2,1,0:T(8,128)(2,1)S(1)}, u32[]{:S(2)}) copy-start(bf16[4,32,1664]{2,1,0:T(8,128)(2,1)S(1)} %all-to-all-done.3.parts_ref) | copy-start | bytes 1277956
  274.3 10.6 %all-to-all-start.7 = ((bf16[8,16,384]{2,1,0:T(8,128)(2,1)}), bf16[8,16,384]{2,1,0:T(8,128)(2,1)S(1)}, u32[]{:S(2)}, u32[]{:S(2)}) async-start(bf16[8,16,384]{2,1,0:T(8,128)(2,1)} %bitcast.65), calls=%async_computation.8 | async-start | bytes 196608 | tf_op jit(solution)/shard_map/all_to_all | solution.py:151
  284.9 12.2 %all-to-all-start.4 = ((bf16[8,16,1664]{2,1,0:T(8,128)(2,1)}), bf16[8,16,1664]{2,1,0:T(8,128)(2,1)S(1)}, u32[]{:S(2)}, u32[]{:S(2)}) async-start(bf16[8,16,1664]{2,1,0:T(8,128)(2,1)} %bitcast.61), calls=%async_computation.5 | async-start | bytes 851968 | tf_op jit(solution)/shard_map/all_to_all | solution.py:151
Sparse Core Ops, SparseCore 0:
  71.1 56.7 all-gather.1
  184.8 72.6 reduce-scatter.1

commit v4 on v3

--- a/solution.py
+++ b/solution.py
@@ -10,9 +10,10 @@
 
 
 SLOTS = 32
-NEAR = 1664
+NEAR = 1536
 NORM_EPS = 1e-06
 FS = ("zl", "y")
+STEPS = (((4, -1), (0, 3), (2, -3), (-2, 1)), ((4, 1), (0, -3), (-2, 3), (2, -1)))
 TP = ("xh", "xl", "c")
 
 
@@ -84,35 +85,41 @@
     return total
 
 
-def combine_kernel(expert_ref, ids_ref, weights_ref, parts_ref, out_ref):
+def combine_kernel(expert_ref, ids_ref, weights_ref, near_ref, far_ref, out_ref):
     pick = slots_of(ids_ref[...], expert_ref[0])
     w = jnp.where(ids_ref[0:1] == expert_ref[0], weights_ref[0:1], weights_ref[1:2])
     slot_weight = jnp.sum(jnp.where(pick, w, 0.0), axis=1, keepdims=True)
-    out_ref[...] = lax.dot_general(
-        pick.astype(jnp.bfloat16),
-        (summed(parts_ref) * slot_weight).astype(jnp.bfloat16),
-        (((0,), (0,)), ((), ())),
-        preferred_element_type=jnp.float32,
-    ).astype(jnp.bfloat16)
-
-
-def combine(expert, ids, weights, parts):
+    pick = pick.astype(jnp.bfloat16)
+    first = 0
+    for parts_ref in (near_ref, far_ref):
+        width = parts_ref.shape[2]
+        out_ref[:, first : first + width] = lax.dot_general(
+            pick,
+            (summed(parts_ref) * slot_weight).astype(jnp.bfloat16),
+            (((0,), (0,)), ((), ())),
+            preferred_element_type=jnp.float32,
+        ).astype(jnp.bfloat16)
+        first += width
+
+
+def combine(expert, ids, weights, near, far):
     vmem = pl.BlockSpec(memory_space=pltpu.VMEM)
+    width = near.shape[2] + far.shape[2]
     return pl.pallas_call(
         combine_kernel,
-        in_specs=[pl.BlockSpec(memory_space=pltpu.SMEM), vmem, vmem, vmem],
+        in_specs=[pl.BlockSpec(memory_space=pltpu.SMEM)] + [vmem] * 4,
         out_specs=vmem,
-        out_shape=jax.ShapeDtypeStruct((ids.shape[1], parts.shape[2]), jnp.bfloat16),
+        out_shape=jax.ShapeDtypeStruct((ids.shape[1], width), jnp.bfloat16),
         name="combine",
-    )(expert, ids, weights, parts)
+    )(expert, ids, weights, near, far)
 
 
 def place_kernel(at_ref, *refs):
     *pieces, gate_ref, up_ref = refs
     rows = gate_ref.shape[2]
     for k, piece in enumerate(pieces):
-        gate_ref[k ^ at_ref[0]] = piece[:, :rows]
-        up_ref[k ^ at_ref[0]] = piece[:, rows:]
+        gate_ref[at_ref[k]] = piece[:, :rows]
+        up_ref[at_ref[k]] = piece[:, rows:]
 
 
 def place(at, pieces):
@@ -161,25 +168,31 @@
     return lax.dynamic_slice_in_dim(twice, (count - zl) % count, count, 0)
 
 
-def by_half(by_core, zl):
+def halves(by_core, gr, zl, xl):
     rows, cols = by_core.shape[-2:]
     by_y = exchange(by_core.reshape(16, rows, cols), ("y", "xh"))
     by_y = by_y.reshape(8, 2, rows, cols)
-    own = lax.dynamic_index_in_dim(by_y, zl & 1, 1, keepdims=False)
-    other = lax.dynamic_index_in_dim(by_y, 1 - (zl & 1), 1, keepdims=False)
-    return own, other
-
-
-def to_servers(own, other, zl, gr):
-    pieces = []
-    for k in range(4):
+    z = 4 * gr + zl
+    out = []
+    for even, odd in zip(*STEPS):
+        same, other = (jnp.where(xl == 0, e, o) for e, o in zip(even, odd))
+        to = z + jnp.where((z & 1) == xl, same, other)
+        out.append(lax.dynamic_index_in_dim(by_y, (to >> 1) & 1, 1, keepdims=False))
+    return out
+
+
+def to_servers(pieces, gr, zl, xh):
+    arrived, at = [], []
+    for k, piece in enumerate(pieces):
         pairs = []
-        for g, a, e, p in itertools.product(range(2), range(4), range(2), range(2)):
-            r, high = (k ^ a) >> 1, (k ^ a) & 1
-            pairs.append((((g * 4 + a) * 2 + e) * 2 + p, ((r * 4 + 2 * high + p) * 2 + g) * 2 + e))
-        piece = other if k & 1 else own
-        pieces.append(lax.ppermute(piece, ("gr", "zl", "xh", "xl"), pairs))
-    return place((2 * gr + (zl >> 1)).reshape(1), pieces)
+        for z, e, p in itertools.product(range(8), range(2), range(2)):
+            to = (z + STEPS[p][k][(z ^ p) & 1]) % 8
+            pairs.append(((z * 2 + e) * 2 + p, (to * 2 + z // 4) * 2 + e))
+        arrived.append(lax.ppermute(piece, ("gr", "zl", "xh", "xl"), pairs))
+        same, other = (jnp.where((zl & 1) == 0, e, o) for e, o in zip(STEPS[0][k], STEPS[1][k]))
+        z = (4 * gr + zl - same) & 7
+        at.append(jnp.where((z >> 2) == xh, z, 4 * gr + zl - other) & 3)
+    return place(jnp.stack(at), arrived)
 
 
 def down_to_servers(down, gr):
@@ -203,9 +216,9 @@
     blocks = cut(gate_master, up_master, ffn_gain[None, :])
     by_core = exchange(blocks.reshape(2, 4, 2, -1, blocks.shape[-1]), "c")
     own_rows = dispatch(expert, ids, prompt)
-    own, other = by_half(by_core, zl)
-    own, other, rows = lax.optimization_barrier((own, other, rows_of_line(own_rows, zl)))
-    gate, up = to_servers(own, other, zl, gr)
+    pieces = halves(by_core, gr, zl, lax.axis_index("xl"))
+    pieces, rows = lax.optimization_barrier((pieces, rows_of_line(own_rows, zl)))
+    gate, up = to_servers(pieces, gr, zl, lax.axis_index("xh"))
     gate_serving = gate.reshape(-1, gate.shape[-1])
     up_serving = up.reshape(-1, up.shape[-1])
 
@@ -222,11 +235,9 @@
     far = exchange(far.astype(jnp.bfloat16).reshape(depth, -1, width - NEAR), "zl")
     far = summed(far).astype(jnp.bfloat16).reshape(-1, SLOTS, width - NEAR)
     far = exchange(far, "y")
-    far = combine(expert, ids, weights, far)
-    far = exchange(far.reshape(servers, -1, width - NEAR), TP)
-    near = combine(expert, ids, weights, exchange(near, "zl"))
-    near = exchange(near.reshape(servers, -1, NEAR), TP)
-    mixed = jnp.concatenate([summed(near), summed(far)], axis=1).astype(jnp.bfloat16)
+    terms = combine(expert, ids, weights, exchange(near, "zl"), far)
+    arrived = exchange(terms.reshape(servers, -1, width), TP)
+    mixed = summed(arrived).astype(jnp.bfloat16)
     return (gate_serving[None], up_serving[None], down_serving[None], mixed)
 
 

time: 306 us -> 295 us (0.964)
  blocking collectives: 64.2 us -> 117 us
  waiting for transfers between devices: 102 us -> 55.1 us
  starting transfers between devices: 85 us -> 68.1 us
    all_to_all x3 -> x5, blocking collectives: 64.2 us -> 117 us  [exchange(): return lax.all_to_all(value, axes, split_axis=0, concat_axis=0, tiled=True)]
    all_to_all x5 -> x2, waiting for transfers between devices: 40.6 us -> 19.9 us  [exchange(): return lax.all_to_all(value, axes, split_axis=0, concat_axis=0, tiled=True)]
    all_to_all x5 -> x2, starting transfers between devices: 38.9 us -> 24.1 us  [exchange(): return lax.all_to_all(value, axes, split_axis=0, concat_axis=0, tiled=True)]
    ppermute x4, waiting for transfers between devices: 34.7 us -> 20.6 us  [to_servers(): arrived.append(lax.ppermute(piece, ('gr', 'zl', 'xh', 'xl'), pairs))]
    reduce_scatter x1, waiting for transfers between devices: 16.3 us -> 3.94 us  [body(): near = lax.psum_scatter(near, 'y', scatter_dimension=0, tiled=True)]
    unnamed x29 -> x27, local copies, waits for them, and re-layouts: 6.62 us -> 7.42 us
  transfers between devices with their start and end apart: 16 -> 13, of which waited for: 8 -> 4; matrix products, arithmetic and copies ran while one was open for 3% -> 3% of each run, Pallas kernels for 5% -> 4%
where the time goes in v4:
time: 295 us; the launch traced here: 294 us
  blocking collectives  117 us (40%)
  starting transfers between devices  68.1 us (23%)
  waiting for transfers between devices  55.1 us (19%)
  Pallas kernels  16.4 us (6%)
  between operations  14.3 us (5%)
  local copies, waits for them, and re-layouts  11.4 us (4%)
  matrix products  8.23 us (3%)
    all_to_all x5, blocking collectives, exchange(): return lax.all_to_all(value, axes, split_axis=0, concat_axis=0, tiled=True)  117 us
    all_to_all x2, starting transfers between devices, exchange(): return lax.all_to_all(value, axes, split_axis=0, concat_axis=0, tiled=True)  24.1 us
    ppermute x4, starting transfers between devices, to_servers(): arrived.append(lax.ppermute(piece, ('gr', 'zl', 'xh', 'xl'), pairs))  20.8 us
    ppermute x4, waiting for transfers between devices, to_servers(): arrived.append(lax.ppermute(piece, ('gr', 'zl', 'xh', 'xl'), pairs))  20.6 us
    all_to_all x2, waiting for transfers between devices, exchange(): return lax.all_to_all(value, axes, split_axis=0, concat_axis=0, tiled=True)  19.9 us
    ppermute x3, starting transfers between devices, rows_of_line(): behind.append(lax.ppermute(rows, 'zl', pairs))  12.7 us
    ppermute x2, waiting for transfers between devices, down_to_servers(): pieces.append(lax.ppermute(down, ('gr', 'xh'), pairs))  10.7 us
    ppermute x2, starting transfers between devices, down_to_servers(): pieces.append(lax.ppermute(down, ('gr', 'xh'), pairs))  10.4 us
  transfers between devices with their start and end apart: 13, of which 4 were waited for; matrix products, arithmetic and copies ran while one was open for 3% of the time, Pallas kernels for 4%

profile of v4, /device:TPU:1, one launch (start us, length us, event | category | flops | bytes accessed | tf_op | source)
XLA Modules:
  0.0 293.6 jit_solution(12747657824083584477)
XLA Ops:
  7.2 2.1 dispatch.1
  9.3 8.6 %collective-permute-start = (bf16[32,2048]{1,0:T(8,128)(2,1)}, bf16[32,2048]{1,0:T(8,128)(2,1)S(1)}, u32[]{:S(2)}, u32[]{:S(2)}) collective-permute-start(bf16[32,2048]{1,0:T(8,128)(2,1)} %dispatch.1), channel_id=1, source_target_pairs={{0,192},{64,0},{128,64},{192,128},{1,193},{65,1},{129,65},{193,129... | collective-permute-start | bytes 393224 | tf_op jit(solution)/shard_map/ppermute | solution.py:166
  17.9 1.9 collective-permute-start.1
  19.8 2.2 collective-permute-start.2
  22.0 3.8 %cut.1 = bf16[2,4,2,2,64,256]{5,4,3,2,1,0:T(8,128)(2,1)} custom-call(f32[1,64]{1,0:T(1,128)} %bitcast.72, f32[4,64,1024]{2,1,0:T(8,128)} %gate_ref.1, f32[4,64,1024]{2,1,0:T(8,128)} %up_ref.1), custom_call_target="tpu_custom_call" | custom-call | tf_op jit(solution)/shard_map/cut/pallas_call | solution.py:36
  25.8 8.3 %all_to_all.35 = bf16[2,4,2,128,256]{4,3,2,1,0:T(8,128)(2,1)} all-to-all(bf16[2,4,2,128,256]{4,3,2,1,0:T(8,128)(2,1)} %bitcast.62), channel_id=1, replica_groups=mesh['gr'=2,'zl'=4,'y'=8,'xh'=2,'xl'=2,'c'=2] {'c'}, dimensions={0} | all-to-all | bytes 2097152 | tf_op jit(solution)/shard_map/all_to_all | solution.py:158
  34.0 8.6 %all-to-all-start.1 = ((bf16[16,128,256]{2,1,0:T(8,128)(2,1)}), bf16[16,128,256]{2,1,0:T(8,128)(2,1)S(1)}, u32[]{:S(2)}, u32[]{:S(2)}) async-start(bf16[16,128,256]{2,1,0:T(8,128)(2,1)} %bitcast.6), calls=%async_computation.1 | async-start | bytes 2097152 | tf_op jit(solution)/shard_map/all_to_all | solution.py:158
  42.6 0.0 copy-start.3
  42.6 0.0 all-gather.2.cloned.1.call-start
  42.7 0.0 copy-done.2
  42.7 0.7 bitcast_dynamic-update-slice_fusion.6
  43.3 0.0 collective-permute-done
  43.3 0.7 bitcast_dynamic-update-slice_fusion.4
  44.0 0.0 collective-permute-done.1
  44.0 0.7 bitcast_dynamic-update-slice_fusion.2
  44.7 0.0 collective-permute-done.2
  44.7 0.7 bitcast_dynamic-update-slice_fusion
  45.3 0.7 bitcast_dynamic-update-slice_fusion.7
  46.0 0.7 bitcast_dynamic-update-slice_fusion.5
  46.7 0.7 bitcast_dynamic-update-slice_fusion.3
  47.3 0.7 bitcast_dynamic-update-slice_fusion.1
  48.0 1.9 constant_dynamic-slice_fusion
  49.9 19.9 %all-to-all-done.1 = bf16[16,128,256]{2,1,0:T(8,128)(2,1)S(1)} async-done(((bf16[16,128,256]{2,1,0:T(8,128)(2,1)}), bf16[16,128,256]{2,1,0:T(8,128)(2,1)S(1)}, u32[]{:S(2)}, u32[]{:S(2)}) %all-to-all-start.1) | async-done | bytes 1048608 | tf_op jit(solution)/shard_map/all_to_all | solution.py:158
  69.8 1.4 dynamic-slice_bitcast_fusion
  71.2 0.0 all-gather.2.cloned.1.call-update
  71.2 0.1 convert_element_type.77
  71.2 0.7 collective-permute-start.7
  71.9 9.7 %collective-permute-start.8 = (bf16[4,256,256]{2,1,0:T(8,128)(2,1)S(1)}, bf16[4,256,256]{2,1,0:T(8,128)(2,1)S(1)}, u32[]{:S(2)}, u32[]{:S(2)}) collective-permute-start(bf16[4,256,256]{2,1,0:T(8,128)(2,1)S(1)} %convert_element_type.77), channel_id=1, source_target_pairs={{0,256},{4,0},{256,260},{260,4},{1,257},{5,1},{257,261},{261,5},{2... | collective-permute-start | bytes 1572872 | tf_op jit(solution)/shard_map/ppermute | solution.py:202
  81.7 0.0 collective-permute-done.7
  81.7 10.7 %collective-permute-done.8 = bf16[4,256,256]{2,1,0:T(8,128)(2,1)S(1)} collective-permute-done((bf16[4,256,256]{2,1,0:T(8,128)(2,1)S(1)}, bf16[4,256,256]{2,1,0:T(8,128)(2,1)S(1)}, u32[]{:S(2)}, u32[]{:S(2)}) %collective-permute-start.8) | collective-permute-done | bytes 524320 | tf_op jit(solution)/shard_map/ppermute | solution.py:202
  92.3 1.1 pad_maximum_fusion
  93.4 15.6 %all-to-all-start.2 = ((bf16[4,2,256,256]{3,2,1,0:T(8,128)(2,1)}), bf16[4,2,256,256]{3,2,1,0:T(8,128)(2,1)S(1)}, u32[]{:S(2)}, u32[]{:S(2)}) async-start(bf16[4,2,256,256]{3,2,1,0:T(8,128)(2,1)} %pad_maximum_fusion), calls=%async_computation.2 | async-start | bytes 2097152 | tf_op jit(solution)/shard_map/all_to_all | solution.py:158
  109.0 8.1 %collective-permute-start.3 = (bf16[8,128,256]{2,1,0:T(8,128)(2,1)}, bf16[8,128,256]{2,1,0:T(8,128)(2,1)S(1)}, u32[]{:S(2)}, u32[]{:S(2)}) collective-permute-start(bf16[8,128,256]{2,1,0:T(8,128)(2,1)} %get-tuple-element.11), channel_id=1, source_target_pairs={{0,256},{2,64},{4,258},{6,66},{64,0},{66,320},{68,2},{70,322},{128... | collective-permute-start | bytes 1572872 | tf_op jit(solution)/shard_map/ppermute | solution.py:191
  117.0 1.7 collective-permute-start.4
  118.7 4.5 %collective-permute-start.5 = (bf16[8,128,256]{2,1,0:T(8,128)(2,1)}, bf16[8,128,256]{2,1,0:T(8,128)(2,1)S(1)}, u32[]{:S(2)}, u32[]{:S(2)}) collective-permute-start(bf16[8,128,256]{2,1,0:T(8,128)(2,1)} %get-tuple-element.13), channel_id=1, source_target_pairs={{0,128},{2,192},{4,130},{6,194},{64,384},{66,448},{68,386},{70,450... | collective-permute-start | bytes 1572872 | tf_op jit(solution)/shard_map/ppermute | solution.py:191
  123.3 6.5 %collective-permute-start.6 = (bf16[8,128,256]{2,1,0:T(8,128)(2,1)}, bf16[8,128,256]{2,1,0:T(8,128)(2,1)S(1)}, u32[]{:S(2)}, u32[]{:S(2)}) collective-permute-start(bf16[8,128,256]{2,1,0:T(8,128)(2,1)} %get-tuple-element.14), channel_id=1, source_target_pairs={{0,384},{2,448},{4,386},{6,450},{64,128},{66,192},{68,130},{70,194... | collective-permute-start | bytes 1572872 | tf_op jit(solution)/shard_map/ppermute | solution.py:191
  129.9 0.6 pad_add_fusion.at_ref
  130.5 0.0 all-to-all-done.2.blocks_ref
  130.5 1.0 copy-done.1
  131.4 5.2 %place_cols.1 = bf16[256,2048]{1,0:T(8,128)(2,1)} custom-call(s32[1]{0:T(128)} %bitcast.20.at_ref, bf16[4,2,256,256]{3,2,1,0:T(8,128)(2,1)} %copy-done.1), custom_call_target="tpu_custom_call" | custom-call | tf_op jit(solution)/shard_map/place_cols/pallas_call | solution.py:144
  136.6 0.0 collective-permute-done.3.refs_0_
  136.6 0.0 collective-permute-done.4.refs_1_
  136.6 0.0 copy-start.5
  136.6 20.6 %collective-permute-done.5.refs_2_ = bf16[8,128,256]{2,1,0:T(8,128)(2,1)S(1)} collective-permute-done((bf16[8,128,256]{2,1,0:T(8,128)(2,1)}, bf16[8,128,256]{2,1,0:T(8,128)(2,1)S(1)}, u32[]{:S(2)}, u32[]{:S(2)}) %collective-permute-start.5) | collective-permute-done | bytes 524320 | tf_op jit(solution)/shard_map/ppermute | solution.py:191
  157.2 0.0 collective-permute-done.6.refs_3_
  157.3 0.8 copy-done.6
  158.0 0.8 copy-done.7
  158.9 3.0 %place.1 = (bf16[4,8,64,256]{3,2,1,0:T(8,128)(2,1)}, bf16[4,8,64,256]{3,2,1,0:T(8,128)(2,1)}) custom-call(s32[4]{0:T(128)} %pad_add_fusion.at_ref, bf16[8,128,256]{2,1,0:T(8,128)(2,1)} %copy-done.4, bf16[8,128,256]{2,1,0:T(8,128)(2,1)} %copy-done.5, bf16[8,128,256]{2,1,0:T(8,128)(2,1)} %copy-done.6, bf16[8,128,256]{2,1,0:T(8,128)(2,1)} %copy-done.7), custom_call_target="tpu_custom_call" | custom-call | tf_op jit(solution)/shard_map/place/pallas_call | solution.py:129
  161.8 3.9 %fusion.3 = f32[1024,256]{1,0:T(8,128)S(1)} fusion(bf16[1024,2048]{1,0:T(8,128)(2,1)} %bitcast.73, bf16[2048,256]{1,0:T(8,128)(2,1)} %bitcast.75), kind=kOutput, calls=%fused_computation.23 | convolution fusion | flops 1073741824 | bytes 6291456 | tf_op jit(solution)/shard_map/dot_general | solution.py:226
  165.7 0.0 copy-done.9
  165.7 0.2 copy-done.8
  165.9 1.3 multiply_convert_fusion
  167.2 0.0 copy-done
  167.2 2.6 convolution_convert_fusion
  169.8 0.0 reduce-scatter.2.cloned.1.call-update
  169.9 0.4 convolution_convert_fusion.1
  170.4 58.2 %all_to_all.36 = bf16[4,256,512]{2,1,0:T(8,128)(2,1)S(1)} all-to-all(bf16[4,256,512]{2,1,0:T(8,128)(2,1)S(1)} %bitcast.61), channel_id=1, replica_groups=mesh['gr'=2,'zl'=4,'y'=8,'xh'=2,'xl'=2,'c'=2] {'zl'}, dimensions={0} | all-to-all | bytes 2097152 | tf_op jit(solution)/shard_map/all_to_all | solution.py:158
  228.5 0.1 add_convert_fusion
  228.7 19.9 %all_to_all.37.far_ref = bf16[8,32,512]{2,1,0:T(8,128)(2,1)} all-to-all(bf16[8,32,512]{2,1,0:T(8,128)(2,1)S(1)} %bitcast.66), channel_id=1, replica_groups=mesh['gr'=2,'zl'=4,'y'=8,'xh'=2,'xl'=2,'c'=2] {'y'}, dimensions={0} | all-to-all | bytes 524288 | tf_op jit(solution)/shard_map/all_to_all | solution.py:158
  248.6 3.9 %reduce-scatter.2.cloned.1.call-done = bf16[4,32,1536]{2,1,0:T(8,128)(2,1)} async-done(((bf16[32,32,1536]{2,1,0:T(8,128)(2,1)}), bf16[4,32,1536]{2,1,0:T(8,128)(2,1)}) %reduce-scatter.2.cloned.1.call-update) | async-done | bytes 393232 | tf_op jit(solution)/shard_map/reduce_scatter | solution.py:231
  252.5 12.9 %all_to_all.38.near_ref = bf16[4,32,1536]{2,1,0:T(8,128)(2,1)} all-to-all(bf16[4,32,1536]{2,1,0:T(8,128)(2,1)} %reduce-scatter.2.cloned.1.call-done), channel_id=1, replica_groups=mesh['gr'=2,'zl'=4,'y'=8,'xh'=2,'xl'=2,'c'=2] {'zl'}, dimensions={0} | all-to-all | bytes 786432 | tf_op jit(solution)/shard_map/all_to_all | solution.py:158
  265.4 2.4 combine.1
  267.8 18.2 %all_to_all.39 = bf16[8,16,2048]{2,1,0:T(8,128)(2,1)S(1)} all-to-all(bf16[8,16,2048]{2,1,0:T(8,128)(2,1)} %bitcast.65), channel_id=1, replica_groups=mesh['gr'=2,'zl'=4,'y'=8,'xh'=2,'xl'=2,'c'=2] {'xh','xl','c'}, dimensions={0} | all-to-all | bytes 1048576 | tf_op jit(solution)/shard_map/all_to_all | solution.py:158
  286.0 0.7 fusion.2
  (14 shorter events, 0.1 us)
Async XLA Ops:
  9.3 33.4 %copy-start.2 = (bf16[32,2048]{1,0:T(8,128)(2,1)S(1)}, bf16[32,2048]{1,0:T(8,128)(2,1)}, u32[]{:S(2)}) copy-start(bf16[32,2048]{1,0:T(8,128)(2,1)} %dispatch.1) | copy-start | bytes 393220
  9.3 34.0 %collective-permute-start = (bf16[32,2048]{1,0:T(8,128)(2,1)}, bf16[32,2048]{1,0:T(8,128)(2,1)S(1)}, u32[]{:S(2)}, u32[]{:S(2)}) collective-permute-start(bf16[32,2048]{1,0:T(8,128)(2,1)} %dispatch.1), channel_id=1, source_target_pairs={{0,192},{64,0},{128,64},{192,128},{1,193},{65,1},{129,65},{193,129... | collective-permute-start | bytes 393224 | tf_op jit(solution)/shard_map/ppermute | solution.py:166
  17.9 26.1 %collective-permute-start.1 = (bf16[32,2048]{1,0:T(8,128)(2,1)}, bf16[32,2048]{1,0:T(8,128)(2,1)S(1)}, u32[]{:S(2)}, u32[]{:S(2)}) collective-permute-start(bf16[32,2048]{1,0:T(8,128)(2,1)} %dispatch.1), channel_id=1, source_target_pairs={{0,128},{64,192},{128,0},{192,64},{1,129},{65,193},{129,1},{193,65... | collective-permute-start | bytes 393224 | tf_op jit(solution)/shard_map/ppermute | solution.py:166
  19.8 24.9 %collective-permute-start.2 = (bf16[32,2048]{1,0:T(8,128)(2,1)}, bf16[32,2048]{1,0:T(8,128)(2,1)S(1)}, u32[]{:S(2)}, u32[]{:S(2)}) collective-permute-start(bf16[32,2048]{1,0:T(8,128)(2,1)} %dispatch.1), channel_id=1, source_target_pairs={{0,64},{64,128},{128,192},{192,0},{1,65},{65,129},{129,193},{193,1... | collective-permute-start | bytes 393224 | tf_op jit(solution)/shard_map/ppermute | solution.py:166
  34.0 35.8 %all-to-all-start.1 = ((bf16[16,128,256]{2,1,0:T(8,128)(2,1)}), bf16[16,128,256]{2,1,0:T(8,128)(2,1)S(1)}, u32[]{:S(2)}, u32[]{:S(2)}) async-start(bf16[16,128,256]{2,1,0:T(8,128)(2,1)} %bitcast.6), calls=%async_computation.1 | async-start | bytes 2097152 | tf_op jit(solution)/shard_map/all_to_all | solution.py:158
  42.6 28.6 %copy-start.3 = (f32[4,256,256]{2,1,0:T(8,128)S(1)}, f32[4,256,256]{2,1,0:T(8,128)}, u32[]{:S(2)}) copy-start(f32[4,256,256]{2,1,0:T(8,128)} %param.12) | copy-start | bytes 3145732
  42.6 119.2 %all-gather.2.cloned.1.call-start = ((), (), s32[]{:S(2)}) async-start(), calls=%async_computation.8 | async-start | bytes 4718592 | tf_op jit(solution)/shard_map/all_gather | solution.py:225
  71.2 10.4 %collective-permute-start.7 = (bf16[4,256,256]{2,1,0:T(8,128)(2,1)S(1)}, bf16[4,256,256]{2,1,0:T(8,128)(2,1)S(1)}, u32[]{:S(2)}, u32[]{:S(2)}) collective-permute-start(bf16[4,256,256]{2,1,0:T(8,128)(2,1)S(1)} %convert_element_type.77), channel_id=1, source_target_pairs={{0,0},{4,256},{256,4},{260,260},{1,1},{5,257},{257,5},{261,261},{2... | collective-permute-start | bytes 1572872 | tf_op jit(solution)/shard_map/ppermute | solution.py:202
  71.9 20.4 %collective-permute-start.8 = (bf16[4,256,256]{2,1,0:T(8,128)(2,1)S(1)}, bf16[4,256,256]{2,1,0:T(8,128)(2,1)S(1)}, u32[]{:S(2)}, u32[]{:S(2)}) collective-permute-start(bf16[4,256,256]{2,1,0:T(8,128)(2,1)S(1)} %convert_element_type.77), channel_id=1, source_target_pairs={{0,256},{4,0},{256,260},{260,4},{1,257},{5,1},{257,261},{261,5},{2... | collective-permute-start | bytes 1572872 | tf_op jit(solution)/shard_map/ppermute | solution.py:202
  93.4 37.1 %all-to-all-start.2 = ((bf16[4,2,256,256]{3,2,1,0:T(8,128)(2,1)}), bf16[4,2,256,256]{3,2,1,0:T(8,128)(2,1)S(1)}, u32[]{:S(2)}, u32[]{:S(2)}) async-start(bf16[4,2,256,256]{3,2,1,0:T(8,128)(2,1)} %pad_maximum_fusion), calls=%async_computation.2 | async-start | bytes 2097152 | tf_op jit(solution)/shard_map/all_to_all | solution.py:158
  109.0 143.6 %reduce-scatter.2.cloned.1.call-start = ((), (), s32[]{:S(2)}) async-start(), calls=%async_computation.9 | async-start | bytes 3538944 | tf_op jit(solution)/shard_map/reduce_scatter | solution.py:231
  109.0 27.7 %collective-permute-start.3 = (bf16[8,128,256]{2,1,0:T(8,128)(2,1)}, bf16[8,128,256]{2,1,0:T(8,128)(2,1)S(1)}, u32[]{:S(2)}, u32[]{:S(2)}) collective-permute-start(bf16[8,128,256]{2,1,0:T(8,128)(2,1)} %get-tuple-element.11), channel_id=1, source_target_pairs={{0,256},{2,64},{4,258},{6,66},{64,0},{66,320},{68,2},{70,322},{128... | collective-permute-start | bytes 1572872 | tf_op jit(solution)/shard_map/ppermute | solution.py:191
  117.0 19.6 %collective-permute-start.4 = (bf16[8,128,256]{2,1,0:T(8,128)(2,1)}, bf16[8,128,256]{2,1,0:T(8,128)(2,1)S(1)}, u32[]{:S(2)}, u32[]{:S(2)}) collective-permute-start(bf16[8,128,256]{2,1,0:T(8,128)(2,1)} %get-tuple-element.12), channel_id=1, source_target_pairs={{0,0},{2,320},{4,2},{6,322},{64,256},{66,64},{68,258},{70,66},{128... | collective-permute-start | bytes 1572872 | tf_op jit(solution)/shard_map/ppermute | solution.py:191
  118.7 38.5 %collective-permute-start.5 = (bf16[8,128,256]{2,1,0:T(8,128)(2,1)}, bf16[8,128,256]{2,1,0:T(8,128)(2,1)S(1)}, u32[]{:S(2)}, u32[]{:S(2)}) collective-permute-start(bf16[8,128,256]{2,1,0:T(8,128)(2,1)} %get-tuple-element.13), channel_id=1, source_target_pairs={{0,128},{2,192},{4,130},{6,194},{64,384},{66,448},{68,386},{70,450... | collective-permute-start | bytes 1572872 | tf_op jit(solution)/shard_map/ppermute | solution.py:191
  123.3 34.0 %collective-permute-start.6 = (bf16[8,128,256]{2,1,0:T(8,128)(2,1)}, bf16[8,128,256]{2,1,0:T(8,128)(2,1)S(1)}, u32[]{:S(2)}, u32[]{:S(2)}) collective-permute-start(bf16[8,128,256]{2,1,0:T(8,128)(2,1)} %get-tuple-element.14), channel_id=1, source_target_pairs={{0,384},{2,448},{4,386},{6,450},{64,128},{66,192},{68,130},{70,194... | collective-permute-start | bytes 1572872 | tf_op jit(solution)/shard_map/ppermute | solution.py:191
  130.5 1.0 copy-start.1
  136.6 20.6 %copy-start.4 = (bf16[8,128,256]{2,1,0:T(8,128)(2,1)}, bf16[8,128,256]{2,1,0:T(8,128)(2,1)S(1)}, u32[]{:S(2)}) copy-start(bf16[8,128,256]{2,1,0:T(8,128)(2,1)S(1)} %collective-permute-done.3.refs_0_) | copy-start | bytes 1572868
  136.6 20.6 %copy-start.5 = (bf16[8,128,256]{2,1,0:T(8,128)(2,1)}, bf16[8,128,256]{2,1,0:T(8,128)(2,1)S(1)}, u32[]{:S(2)}) copy-start(bf16[8,128,256]{2,1,0:T(8,128)(2,1)S(1)} %collective-permute-done.4.refs_1_) | copy-start | bytes 1572868
  157.2 0.8 copy-start.6
  158.0 0.8 copy-start.7
  161.8 3.9 %copy-start.9 = (bf16[4,8,64,256]{3,2,1,0:T(8,128)(2,1)S(1)}, bf16[4,8,64,256]{3,2,1,0:T(8,128)(2,1)}, u32[]{:S(2)}) copy-start(bf16[4,8,64,256]{3,2,1,0:T(8,128)(2,1)} %get-tuple-element.16) | copy-start | bytes 3145732
  161.8 4.1 %copy-start.8 = (bf16[32,32,2048]{2,1,0:T(8,128)(2,1)S(1)}, bf16[32,32,2048]{2,1,0:T(8,128)(2,1)}, u32[]{:S(2)}) copy-start(bf16[32,32,2048]{2,1,0:T(8,128)(2,1)} %all-gather.2.cloned.1.call-done) | copy-start | bytes 12582916
  165.9 1.3 copy-start
Sparse Core Ops, SparseCore 0:
  71.3 56.7 all-gather.1
  170.0 82.4 reduce-scatter.1

commit v5 on v4

--- a/solution.py
+++ b/solution.py
@@ -147,11 +147,30 @@
             num_scalar_prefetch=1,
             grid=(pieces, parts),
             in_specs=[pl.BlockSpec((1, 1, rows, width), lambda k, i, at: (i, k, 0, 0))],
-            out_specs=pl.BlockSpec((rows, width), lambda k, i, at: (0, (k ^ at[0]) * parts + i)),
+            out_specs=pl.BlockSpec(
+                (rows, width), lambda k, i, at: (0, (k ^ at[0]) * parts + (i ^ at[1]))
+            ),
         ),
         out_shape=jax.ShapeDtypeStruct((rows, pieces * parts * width), jnp.bfloat16),
         name="place_cols",
     )(at, blocks)
+
+
+def line_up_kernel(at_ref, *refs):
+    *pieces, out_ref = refs
+    for s, piece in enumerate(pieces):
+        out_ref[(at_ref[0] + s) % len(pieces)] = piece[...]
+
+
+def line_up(at, pieces):
+    vmem = pl.BlockSpec(memory_space=pltpu.VMEM)
+    return pl.pallas_call(
+        line_up_kernel,
+        in_specs=[pl.BlockSpec(memory_space=pltpu.SMEM)] + [vmem] * len(pieces),
+        out_specs=vmem,
+        out_shape=jax.ShapeDtypeStruct((len(pieces), *pieces[0].shape), jnp.bfloat16),
+        name="line_up",
+    )(at, *pieces)
 
 
 def exchange(value, axes):
@@ -164,8 +183,7 @@
     for step in range(1, count):
         pairs = [(z, (z - step) % count) for z in range(count)]
         behind.append(lax.ppermute(rows, "zl", pairs))
-    twice = jnp.stack(behind + behind)
-    return lax.dynamic_slice_in_dim(twice, (count - zl) % count, count, 0)
+    return line_up(zl.reshape(1), behind)
 
 
 def halves(by_core, gr, zl, xl):
@@ -195,14 +213,18 @@
     return place(jnp.stack(at), arrived)
 
 
-def down_to_servers(down, gr):
+def down_to_servers(down, gr, own):
     pieces = []
     for k in range(2):
         pairs = [(g * 2 + p, (k ^ p) * 2 + g) for g in range(2) for p in range(2)]
         pieces.append(lax.ppermute(down, ("gr", "xh"), pairs))
-    blocks = jnp.stack(pieces, axis=1)
-    blocks = exchange(blocks, ("xl", "c"))
-    return place_cols(gr.reshape(1), blocks)
+    blocks = []
+    for s in range(4):
+        block = jnp.stack([lax.dynamic_index_in_dim(p, own ^ s, 0, keepdims=False) for p in pieces])
+        if s:
+            block = lax.ppermute(block, ("xl", "c"), [(u, u ^ s) for u in range(4)])
+        blocks.append(block)
+    return place_cols(jnp.stack([gr, own]), jnp.stack(blocks))
 
 
 def body(prompt, expert_ids, route_weights, gate_master, up_master, down_master, ffn_gain):
@@ -212,7 +234,9 @@
     ids, weights = expert_ids.T, route_weights.T
     width = prompt.shape[1]
 
-    down_serving = down_to_servers(down_master.astype(jnp.bfloat16), gr)
+    down_serving = down_to_servers(
+        down_master.astype(jnp.bfloat16), gr, lax.axis_index(("xl", "c"))
+    )
     blocks = cut(gate_master, up_master, ffn_gain[None, :])
     by_core = exchange(blocks.reshape(2, 4, 2, -1, blocks.shape[-1]), "c")
     own_rows = dispatch(expert, ids, prompt)

time: 295 us -> 283 us (0.959)
  waiting for transfers between devices: 55.1 us -> 47.1 us
  local copies, waits for them, and re-layouts: 11.4 us -> 4.15 us
  blocking collectives: 117 us -> 112 us
  starting transfers between devices: 68.1 us -> 72.1 us
    ppermute x0 -> x3, starting transfers between devices: none -> 22.8 us  [down_to_servers(): block = lax.ppermute(block, ('xl', 'c'), [(u, u ^ s) for u in range(4)])]
    ppermute x0 -> x3, waiting for transfers between devices: none -> 20.8 us  [down_to_servers(): block = lax.ppermute(block, ('xl', 'c'), [(u, u ^ s) for u in range(4)])]
    ppermute x4, waiting for transfers between devices: 20.6 us -> 0.01 us  [to_servers(): arrived.append(lax.ppermute(piece, ('gr', 'zl', 'xh', 'xl'), pairs))]
    all_to_all x2 -> x1, starting transfers between devices: 24.1 us -> 4.17 us  [exchange(): return lax.all_to_all(value, axes, split_axis=0, concat_axis=0, tiled=True)]
    all_to_all x2 -> x1, waiting for transfers between devices: 19.9 us -> 2.15 us  [exchange(): return lax.all_to_all(value, axes, split_axis=0, concat_axis=0, tiled=True)]
    ppermute x3, waiting for transfers between devices: 0.01 us -> 8.39 us  [rows_of_line(): behind.append(lax.ppermute(rows, 'zl', pairs))]
    all_to_all x5, blocking collectives: 117 us -> 112 us  [exchange(): return lax.all_to_all(value, axes, split_axis=0, concat_axis=0, tiled=True)]
    unnamed x27 -> x26, local copies, waits for them, and re-layouts: 7.42 us -> 2.86 us
  transfers between devices with their start and end apart: 13 -> 15, of which waited for: 4 -> 5; matrix products, arithmetic and copies ran while one was open for 3% -> 2% of each run, Pallas kernels for 4% -> 5%
where the time goes in v5:
time: 283 us; the launch traced here: 282 us
  blocking collectives  112 us (40%)
  starting transfers between devices  72.1 us (25%)
  waiting for transfers between devices  47.1 us (17%)
  Pallas kernels  19 us (7%)
  between operations  14.4 us (5%)
  matrix products  8.23 us (3%)
  other arithmetic  5.18 us (2%)
  local copies, waits for them, and re-layouts  4.15 us (1%)
    all_to_all x5, blocking collectives, exchange(): return lax.all_to_all(value, axes, split_axis=0, concat_axis=0, tiled=True)  112 us
    ppermute x3, starting transfers between devices, down_to_servers(): block = lax.ppermute(block, ('xl', 'c'), [(u, u ^ s) for u in range(4)])  22.8 us
    ppermute x4, starting transfers between devices, to_servers(): arrived.append(lax.ppermute(piece, ('gr', 'zl', 'xh', 'xl'), pairs))  20.8 us
    ppermute x3, waiting for transfers between devices, down_to_servers(): block = lax.ppermute(block, ('xl', 'c'), [(u, u ^ s) for u in range(4)])  20.8 us
    ppermute x2, starting transfers between devices, down_to_servers(): pieces.append(lax.ppermute(down, ('gr', 'xh'), pairs))  12.6 us
    ppermute x3, starting transfers between devices, rows_of_line(): behind.append(lax.ppermute(rows, 'zl', pairs))  11.7 us
    ppermute x2, waiting for transfers between devices, down_to_servers(): pieces.append(lax.ppermute(down, ('gr', 'xh'), pairs))  10.6 us
    ppermute x3, waiting for transfers between devices, rows_of_line(): behind.append(lax.ppermute(rows, 'zl', pairs))  8.39 us
  transfers between devices with their start and end apart: 15, of which 5 were waited for; matrix products, arithmetic and copies ran while one was open for 2% of the time, Pallas kernels for 5%

profile of v5, /device:TPU:1, one launch (start us, length us, event | category | flops | bytes accessed | tf_op | source)
XLA Modules:
  0.0 281.9 jit_solution(819945945381625989)
XLA Ops:
  7.2 3.8 %cut.1 = bf16[2,4,2,2,64,256]{5,4,3,2,1,0:T(8,128)(2,1)} custom-call(f32[1,64]{1,0:T(1,128)} %bitcast.63, f32[4,64,1024]{2,1,0:T(8,128)} %gate_ref.1, f32[4,64,1024]{2,1,0:T(8,128)} %up_ref.1), custom_call_target="tpu_custom_call" | custom-call | tf_op jit(solution)/shard_map/cut/pallas_call | solution.py:36
  10.9 13.0 %all_to_all.30 = bf16[2,4,2,128,256]{4,3,2,1,0:T(8,128)(2,1)} all-to-all(bf16[2,4,2,128,256]{4,3,2,1,0:T(8,128)(2,1)} %bitcast.53), channel_id=1, replica_groups=mesh['gr'=2,'zl'=4,'y'=8,'xh'=2,'xl'=2,'c'=2] {'c'}, dimensions={0} | all-to-all | bytes 2097152 | tf_op jit(solution)/shard_map/all_to_all | solution.py:177
  24.0 4.2 %all-to-all-start.1 = ((bf16[16,128,256]{2,1,0:T(8,128)(2,1)}), bf16[16,128,256]{2,1,0:T(8,128)(2,1)S(1)}, u32[]{:S(2)}, u32[]{:S(2)}) async-start(bf16[16,128,256]{2,1,0:T(8,128)(2,1)} %bitcast.6), calls=%async_computation.1 | async-start | bytes 2097152 | tf_op jit(solution)/shard_map/all_to_all | solution.py:177
  28.2 0.0 all-gather.2.cloned.1.call-start
  28.2 2.1 dispatch.1.refs_0_
  30.3 7.6 %collective-permute-start = (bf16[32,2048]{1,0:T(8,128)(2,1)}, bf16[32,2048]{1,0:T(8,128)(2,1)S(1)}, u32[]{:S(2)}, u32[]{:S(2)}) collective-permute-start(bf16[32,2048]{1,0:T(8,128)(2,1)} %dispatch.1.refs_0_), channel_id=1, source_target_pairs={{0,192},{64,0},{128,64},{192,128},{1,193},{65,1},{129,65},{193,129... | collective-permute-start | bytes 393224 | tf_op jit(solution)/shard_map/ppermute | solution.py:185
  38.0 1.9 collective-permute-start.1
  39.9 2.2 collective-permute-start.2
  42.1 0.0 collective-permute-done.refs_1_
  42.1 0.0 copy-start.8
  42.1 8.4 %collective-permute-done.1.refs_2_ = bf16[32,2048]{1,0:T(8,128)(2,1)S(1)} collective-permute-done((bf16[32,2048]{1,0:T(8,128)(2,1)}, bf16[32,2048]{1,0:T(8,128)(2,1)S(1)}, u32[]{:S(2)}, u32[]{:S(2)}) %collective-permute-start.1) | collective-permute-done | bytes 131104 | tf_op jit(solution)/shard_map/ppermute | solution.py:185
  50.5 0.0 collective-permute-done.2.refs_3_
  50.5 0.6 copy-done.9
  51.2 0.0 copy-done.10
  51.2 2.0 line_up.1
  53.2 2.1 all-to-all-done.1
  55.3 1.2 dynamic-slice_bitcast_fusion
  56.5 0.0 all-gather.2.cloned.1.call-update
  56.5 0.0 reduce-scatter.2.cloned.1.call-start
  56.6 0.0 copy-done.1
  56.6 0.1 convert_element_type.77
  56.6 0.7 collective-permute-start.7
  57.4 11.9 %collective-permute-start.8 = (bf16[4,256,256]{2,1,0:T(8,128)(2,1)S(1)}, bf16[4,256,256]{2,1,0:T(8,128)(2,1)S(1)}, u32[]{:S(2)}, u32[]{:S(2)}) collective-permute-start(bf16[4,256,256]{2,1,0:T(8,128)(2,1)S(1)} %convert_element_type.77), channel_id=1, source_target_pairs={{0,256},{4,0},{256,260},{260,4},{1,257},{5,1},{257,261},{261,5},{2... | collective-permute-start | bytes 1572872 | tf_op jit(solution)/shard_map/ppermute | solution.py:220
  69.2 0.0 collective-permute-done.7
  69.3 10.6 %collective-permute-done.8 = bf16[4,256,256]{2,1,0:T(8,128)(2,1)S(1)} collective-permute-done((bf16[4,256,256]{2,1,0:T(8,128)(2,1)S(1)}, bf16[4,256,256]{2,1,0:T(8,128)(2,1)S(1)}, u32[]{:S(2)}, u32[]{:S(2)}) %collective-permute-start.8) | collective-permute-done | bytes 524320 | tf_op jit(solution)/shard_map/ppermute | solution.py:220
  80.0 14.5 %collective-permute-start.9 = (bf16[2,256,256]{2,1,0:T(8,128)(2,1)S(1)}, bf16[2,256,256]{2,1,0:T(8,128)(2,1)S(1)}, u32[]{:S(2)}, u32[]{:S(2)}) collective-permute-start(bf16[2,256,256]{2,1,0:T(8,128)(2,1)S(1)} %pad_maximum_fusion.1), channel_id=1, source_target_pairs={{0,1},{1,0},{2,3},{3,2},{4,5},{5,4},{6,7},{7,6},{8,9},{9,8},{10,11... | collective-permute-start | bytes 786440 | tf_op jit(solution)/shard_map/ppermute | solution.py:225
  94.5 2.2 collective-permute-start.10
  96.7 8.1 %collective-permute-start.3 = (bf16[8,128,256]{2,1,0:T(8,128)(2,1)}, bf16[8,128,256]{2,1,0:T(8,128)(2,1)S(1)}, u32[]{:S(2)}, u32[]{:S(2)}) collective-permute-start(bf16[8,128,256]{2,1,0:T(8,128)(2,1)} %get-tuple-element.11), channel_id=1, source_target_pairs={{0,256},{2,64},{4,258},{6,66},{64,0},{66,320},{68,2},{70,322},{128... | collective-permute-start | bytes 1572872 | tf_op jit(solution)/shard_map/ppermute | solution.py:209
  104.9 1.7 collective-permute-start.4
  106.6 4.7 %collective-permute-start.5 = (bf16[8,128,256]{2,1,0:T(8,128)(2,1)S(1)}, bf16[8,128,256]{2,1,0:T(8,128)(2,1)S(1)}, u32[]{:S(2)}, u32[]{:S(2)}) collective-permute-start(bf16[8,128,256]{2,1,0:T(8,128)(2,1)S(1)} %get-tuple-element.13), channel_id=1, source_target_pairs={{0,128},{2,192},{4,130},{6,194},{64,384},{66,448},{68,386},{70,450... | collective-permute-start | bytes 1572872 | tf_op jit(solution)/shard_map/ppermute | solution.py:209
  111.2 0.0 collective-permute-done.9
  111.2 0.0 copy-start.6
  111.2 6.3 %collective-permute-start.6 = (bf16[8,128,256]{2,1,0:T(8,128)(2,1)S(1)}, bf16[8,128,256]{2,1,0:T(8,128)(2,1)S(1)}, u32[]{:S(2)}, u32[]{:S(2)}) collective-permute-start(bf16[8,128,256]{2,1,0:T(8,128)(2,1)S(1)} %get-tuple-element.14), channel_id=1, source_target_pairs={{0,384},{2,448},{4,386},{6,450},{64,128},{66,192},{68,130},{70,194... | collective-permute-start | bytes 1572872 | tf_op jit(solution)/shard_map/ppermute | solution.py:209
  117.6 0.7 pad_maximum_fusion.3
  118.3 0.0 collective-permute-done.10
  118.3 6.1 %collective-permute-start.11 = (bf16[2,256,256]{2,1,0:T(8,128)(2,1)}, bf16[2,256,256]{2,1,0:T(8,128)(2,1)}, u32[]{:S(2)}, u32[]{:S(2)}) collective-permute-start(bf16[2,256,256]{2,1,0:T(8,128)(2,1)} %pad_maximum_fusion.3), channel_id=1, source_target_pairs={{0,3},{1,2},{2,1},{3,0},{4,7},{5,6},{6,5},{7,4},{8,11},{9,10},{10,... | collective-permute-start | bytes 786440 | tf_op jit(solution)/shard_map/ppermute | solution.py:225
  124.4 0.6 pad_add_fusion.1.at_ref
  125.0 0.7 pad_add_fusion.at_ref
  125.7 20.8 %collective-permute-done.11 = bf16[2,256,256]{2,1,0:T(8,128)(2,1)} collective-permute-done((bf16[2,256,256]{2,1,0:T(8,128)(2,1)}, bf16[2,256,256]{2,1,0:T(8,128)(2,1)}, u32[]{:S(2)}, u32[]{:S(2)}) %collective-permute-start.11) | collective-permute-done | bytes 262176 | tf_op jit(solution)/shard_map/ppermute | solution.py:225
  146.5 2.2 pad_maximum_fusion.blocks_ref
  148.7 5.9 %place_cols.1 = bf16[256,2048]{1,0:T(8,128)(2,1)} custom-call(s32[2]{0:T(128)} %pad_add_fusion.1.at_ref, bf16[4,2,256,256]{3,2,1,0:T(8,128)(2,1)} %pad_maximum_fusion.blocks_ref), custom_call_target="tpu_custom_call" | custom-call | tf_op jit(solution)/shard_map/place_cols/pallas_call | solution.py:144
  154.6 0.0 collective-permute-done.3.refs_0_
  154.6 0.0 collective-permute-done.4.refs_1_
  154.6 0.0 collective-permute-done.5.refs_2_
  154.6 0.0 collective-permute-done.6.refs_3_
  154.6 0.8 copy-done.2
  155.4 0.2 copy-done.3
  155.6 0.2 copy-done.4
  155.8 0.8 copy-done.5
  156.6 3.0 %place.1 = (bf16[4,8,64,256]{3,2,1,0:T(8,128)(2,1)}, bf16[4,8,64,256]{3,2,1,0:T(8,128)(2,1)}) custom-call(s32[4]{0:T(128)} %pad_add_fusion.at_ref, bf16[8,128,256]{2,1,0:T(8,128)(2,1)} %copy-done.2, bf16[8,128,256]{2,1,0:T(8,128)(2,1)} %copy-done.3, bf16[8,128,256]{2,1,0:T(8,128)(2,1)} %copy-done.4, bf16[8,128,256]{2,1,0:T(8,128)(2,1)} %copy-done.5), custom_call_target="tpu_custom_call" | custom-call | tf_op jit(solution)/shard_map/place/pallas_call | solution.py:129
  159.6 3.9 %fusion.3 = f32[1024,256]{1,0:T(8,128)S(1)} fusion(bf16[1024,2048]{1,0:T(8,128)(2,1)} %bitcast.64, bf16[2048,256]{1,0:T(8,128)(2,1)} %bitcast.66), kind=kOutput, calls=%fused_computation.27 | convolution fusion | flops 1073741824 | bytes 6291456 | tf_op jit(solution)/shard_map/dot_general | solution.py:250
  163.5 0.2 copy-done.11
  163.6 1.3 multiply_convert_fusion
  165.0 2.6 convolution_convert_fusion
  167.6 0.0 reduce-scatter.2.cloned.1.call-update
  167.6 0.4 convolution_convert_fusion.1
  168.1 47.6 %all_to_all.31 = bf16[4,256,512]{2,1,0:T(8,128)(2,1)S(1)} all-to-all(bf16[4,256,512]{2,1,0:T(8,128)(2,1)S(1)} %bitcast.52), channel_id=1, replica_groups=mesh['gr'=2,'zl'=4,'y'=8,'xh'=2,'xl'=2,'c'=2] {'zl'}, dimensions={0} | all-to-all | bytes 2097152 | tf_op jit(solution)/shard_map/all_to_all | solution.py:177
  215.7 0.1 add_convert_fusion
  215.8 20.1 %all_to_all.32.far_ref = bf16[8,32,512]{2,1,0:T(8,128)(2,1)} all-to-all(bf16[8,32,512]{2,1,0:T(8,128)(2,1)S(1)} %bitcast.57), channel_id=1, replica_groups=mesh['gr'=2,'zl'=4,'y'=8,'xh'=2,'xl'=2,'c'=2] {'y'}, dimensions={0} | all-to-all | bytes 524288 | tf_op jit(solution)/shard_map/all_to_all | solution.py:177
  235.9 5.1 %reduce-scatter.2.cloned.1.call-done = bf16[4,32,1536]{2,1,0:T(8,128)(2,1)} async-done(((bf16[32,32,1536]{2,1,0:T(8,128)(2,1)}), bf16[4,32,1536]{2,1,0:T(8,128)(2,1)}) %reduce-scatter.2.cloned.1.call-update) | async-done | bytes 393232 | tf_op jit(solution)/shard_map/reduce_scatter | solution.py:255
  241.0 13.3 %all_to_all.33.near_ref = bf16[4,32,1536]{2,1,0:T(8,128)(2,1)} all-to-all(bf16[4,32,1536]{2,1,0:T(8,128)(2,1)} %reduce-scatter.2.cloned.1.call-done), channel_id=1, replica_groups=mesh['gr'=2,'zl'=4,'y'=8,'xh'=2,'xl'=2,'c'=2] {'zl'}, dimensions={0} | all-to-all | bytes 786432 | tf_op jit(solution)/shard_map/all_to_all | solution.py:177
  254.4 2.4 combine.1
  256.7 17.7 %all_to_all.34 = bf16[8,16,2048]{2,1,0:T(8,128)(2,1)S(1)} all-to-all(bf16[8,16,2048]{2,1,0:T(8,128)(2,1)} %bitcast.56), channel_id=1, replica_groups=mesh['gr'=2,'zl'=4,'y'=8,'xh'=2,'xl'=2,'c'=2] {'xh','xl','c'}, dimensions={0} | all-to-all | bytes 1048576 | tf_op jit(solution)/shard_map/all_to_all | solution.py:177
  274.4 0.7 fusion.2
  (23 shorter events, 0.2 us)
Async XLA Ops:
  24.0 32.6 %copy-start.1 = (f32[4,256,256]{2,1,0:T(8,128)S(1)}, f32[4,256,256]{2,1,0:T(8,128)}, u32[]{:S(2)}) copy-start(f32[4,256,256]{2,1,0:T(8,128)} %param.12) | copy-start | bytes 3145732
  24.0 31.4 %all-to-all-start.1 = ((bf16[16,128,256]{2,1,0:T(8,128)(2,1)}), bf16[16,128,256]{2,1,0:T(8,128)(2,1)S(1)}, u32[]{:S(2)}, u32[]{:S(2)}) async-start(bf16[16,128,256]{2,1,0:T(8,128)(2,1)} %bitcast.6), calls=%async_computation.1 | async-start | bytes 2097152 | tf_op jit(solution)/shard_map/all_to_all | solution.py:177
  28.2 131.4 %all-gather.2.cloned.1.call-start = ((), (), s32[]{:S(2)}) async-start(), calls=%async_computation.7 | async-start | bytes 4718592 | tf_op jit(solution)/shard_map/all_gather | solution.py:249
  30.3 11.8 %collective-permute-start = (bf16[32,2048]{1,0:T(8,128)(2,1)}, bf16[32,2048]{1,0:T(8,128)(2,1)S(1)}, u32[]{:S(2)}, u32[]{:S(2)}) collective-permute-start(bf16[32,2048]{1,0:T(8,128)(2,1)} %dispatch.1.refs_0_), channel_id=1, source_target_pairs={{0,192},{64,0},{128,64},{192,128},{1,193},{65,1},{129,65},{193,129... | collective-permute-start | bytes 393224 | tf_op jit(solution)/shard_map/ppermute | solution.py:185
  38.0 12.6 %collective-permute-start.1 = (bf16[32,2048]{1,0:T(8,128)(2,1)}, bf16[32,2048]{1,0:T(8,128)(2,1)S(1)}, u32[]{:S(2)}, u32[]{:S(2)}) collective-permute-start(bf16[32,2048]{1,0:T(8,128)(2,1)} %dispatch.1.refs_0_), channel_id=1, source_target_pairs={{0,128},{64,192},{128,0},{192,64},{1,129},{65,193},{129,1},{193,65... | collective-permute-start | bytes 393224 | tf_op jit(solution)/shard_map/ppermute | solution.py:185
  39.9 10.7 %collective-permute-start.2 = (bf16[32,2048]{1,0:T(8,128)(2,1)}, bf16[32,2048]{1,0:T(8,128)(2,1)S(1)}, u32[]{:S(2)}, u32[]{:S(2)}) collective-permute-start(bf16[32,2048]{1,0:T(8,128)(2,1)} %dispatch.1.refs_0_), channel_id=1, source_target_pairs={{0,64},{64,128},{128,192},{192,0},{1,65},{65,129},{129,193},{193,1... | collective-permute-start | bytes 393224 | tf_op jit(solution)/shard_map/ppermute | solution.py:185
  42.1 8.4 %copy-start.8 = (bf16[32,2048]{1,0:T(8,128)(2,1)}, bf16[32,2048]{1,0:T(8,128)(2,1)S(1)}, u32[]{:S(2)}) copy-start(bf16[32,2048]{1,0:T(8,128)(2,1)S(1)} %collective-permute-done.refs_1_) | copy-start | bytes 393220
  50.5 0.7 copy-start.9
  50.5 0.7 copy-start.10
  56.5 184.5 %reduce-scatter.2.cloned.1.call-start = ((), (), s32[]{:S(2)}) async-start(), calls=%async_computation.8 | async-start | bytes 3538944 | tf_op jit(solution)/shard_map/reduce_scatter | solution.py:255
  56.6 12.6 %collective-permute-start.7 = (bf16[4,256,256]{2,1,0:T(8,128)(2,1)S(1)}, bf16[4,256,256]{2,1,0:T(8,128)(2,1)S(1)}, u32[]{:S(2)}, u32[]{:S(2)}) collective-permute-start(bf16[4,256,256]{2,1,0:T(8,128)(2,1)S(1)} %convert_element_type.77), channel_id=1, source_target_pairs={{0,0},{4,256},{256,4},{260,260},{1,1},{5,257},{257,5},{261,261},{2... | collective-permute-start | bytes 1572872 | tf_op jit(solution)/shard_map/ppermute | solution.py:220
  57.4 22.5 %collective-permute-start.8 = (bf16[4,256,256]{2,1,0:T(8,128)(2,1)S(1)}, bf16[4,256,256]{2,1,0:T(8,128)(2,1)S(1)}, u32[]{:S(2)}, u32[]{:S(2)}) collective-permute-start(bf16[4,256,256]{2,1,0:T(8,128)(2,1)S(1)} %convert_element_type.77), channel_id=1, source_target_pairs={{0,256},{4,0},{256,260},{260,4},{1,257},{5,1},{257,261},{261,5},{2... | collective-permute-start | bytes 1572872 | tf_op jit(solution)/shard_map/ppermute | solution.py:220
  80.0 31.3 %collective-permute-start.9 = (bf16[2,256,256]{2,1,0:T(8,128)(2,1)S(1)}, bf16[2,256,256]{2,1,0:T(8,128)(2,1)S(1)}, u32[]{:S(2)}, u32[]{:S(2)}) collective-permute-start(bf16[2,256,256]{2,1,0:T(8,128)(2,1)S(1)} %pad_maximum_fusion.1), channel_id=1, source_target_pairs={{0,1},{1,0},{2,3},{3,2},{4,5},{5,4},{6,7},{7,6},{8,9},{9,8},{10,11... | collective-permute-start | bytes 786440 | tf_op jit(solution)/shard_map/ppermute | solution.py:225
  94.5 23.8 %collective-permute-start.10 = (bf16[2,256,256]{2,1,0:T(8,128)(2,1)S(1)}, bf16[2,256,256]{2,1,0:T(8,128)(2,1)S(1)}, u32[]{:S(2)}, u32[]{:S(2)}) collective-permute-start(bf16[2,256,256]{2,1,0:T(8,128)(2,1)S(1)} %pad_maximum_fusion.2), channel_id=1, source_target_pairs={{0,2},{1,3},{2,0},{3,1},{4,6},{5,7},{6,4},{7,5},{8,10},{9,11},{10,... | collective-permute-start | bytes 786440 | tf_op jit(solution)/shard_map/ppermute | solution.py:225
  96.7 57.8 %collective-permute-start.3 = (bf16[8,128,256]{2,1,0:T(8,128)(2,1)}, bf16[8,128,256]{2,1,0:T(8,128)(2,1)S(1)}, u32[]{:S(2)}, u32[]{:S(2)}) collective-permute-start(bf16[8,128,256]{2,1,0:T(8,128)(2,1)} %get-tuple-element.11), channel_id=1, source_target_pairs={{0,256},{2,64},{4,258},{6,66},{64,0},{66,320},{68,2},{70,322},{128... | collective-permute-start | bytes 1572872 | tf_op jit(solution)/shard_map/ppermute | solution.py:209
  104.9 49.7 %collective-permute-start.4 = (bf16[8,128,256]{2,1,0:T(8,128)(2,1)}, bf16[8,128,256]{2,1,0:T(8,128)(2,1)S(1)}, u32[]{:S(2)}, u32[]{:S(2)}) collective-permute-start(bf16[8,128,256]{2,1,0:T(8,128)(2,1)} %get-tuple-element.12), channel_id=1, source_target_pairs={{0,0},{2,320},{4,2},{6,322},{64,256},{66,64},{68,258},{70,66},{128... | collective-permute-start | bytes 1572872 | tf_op jit(solution)/shard_map/ppermute | solution.py:209
  106.6 48.0 %collective-permute-start.5 = (bf16[8,128,256]{2,1,0:T(8,128)(2,1)S(1)}, bf16[8,128,256]{2,1,0:T(8,128)(2,1)S(1)}, u32[]{:S(2)}, u32[]{:S(2)}) collective-permute-start(bf16[8,128,256]{2,1,0:T(8,128)(2,1)S(1)} %get-tuple-element.13), channel_id=1, source_target_pairs={{0,128},{2,192},{4,130},{6,194},{64,384},{66,448},{68,386},{70,450... | collective-permute-start | bytes 1572872 | tf_op jit(solution)/shard_map/ppermute | solution.py:209
  111.2 7.1 %copy-start.6 = (bf16[2,256,256]{2,1,0:T(8,128)(2,1)}, bf16[2,256,256]{2,1,0:T(8,128)(2,1)S(1)}, u32[]{:S(2)}) copy-start(bf16[2,256,256]{2,1,0:T(8,128)(2,1)S(1)} %collective-permute-done.9) | copy-start | bytes 786436
  111.2 43.4 %collective-permute-start.6 = (bf16[8,128,256]{2,1,0:T(8,128)(2,1)S(1)}, bf16[8,128,256]{2,1,0:T(8,128)(2,1)S(1)}, u32[]{:S(2)}, u32[]{:S(2)}) collective-permute-start(bf16[8,128,256]{2,1,0:T(8,128)(2,1)S(1)} %get-tuple-element.14), channel_id=1, source_target_pairs={{0,384},{2,448},{4,386},{6,450},{64,128},{66,192},{68,130},{70,194... | collective-permute-start | bytes 1572872 | tf_op jit(solution)/shard_map/ppermute | solution.py:209
  118.3 6.1 %copy-start.7 = (bf16[2,256,256]{2,1,0:T(8,128)(2,1)}, bf16[2,256,256]{2,1,0:T(8,128)(2,1)S(1)}, u32[]{:S(2)}) copy-start(bf16[2,256,256]{2,1,0:T(8,128)(2,1)S(1)} %collective-permute-done.10) | copy-start | bytes 786436
  118.3 28.2 %collective-permute-start.11 = (bf16[2,256,256]{2,1,0:T(8,128)(2,1)}, bf16[2,256,256]{2,1,0:T(8,128)(2,1)}, u32[]{:S(2)}, u32[]{:S(2)}) collective-permute-start(bf16[2,256,256]{2,1,0:T(8,128)(2,1)} %pad_maximum_fusion.3), channel_id=1, source_target_pairs={{0,3},{1,2},{2,1},{3,0},{4,7},{5,6},{6,5},{7,4},{8,11},{9,10},{10,... | collective-permute-start | bytes 786440 | tf_op jit(solution)/shard_map/ppermute | solution.py:225
  154.6 0.8 copy-start.2
  154.6 1.0 copy-start.3
  154.6 1.2 copy-start.4
  155.8 0.8 copy-start.5
  159.6 3.9 %copy-start.12 = (bf16[4,8,64,256]{3,2,1,0:T(8,128)(2,1)S(1)}, bf16[4,8,64,256]{3,2,1,0:T(8,128)(2,1)}, u32[]{:S(2)}) copy-start(bf16[4,8,64,256]{3,2,1,0:T(8,128)(2,1)} %get-tuple-element.16) | copy-start | bytes 3145732
  159.6 4.1 %copy-start.11 = (bf16[32,32,2048]{2,1,0:T(8,128)(2,1)S(1)}, bf16[32,32,2048]{2,1,0:T(8,128)(2,1)}, u32[]{:S(2)}) copy-start(bf16[32,32,2048]{2,1,0:T(8,128)(2,1)} %all-gather.2.cloned.1.call-done) | copy-start | bytes 12582916
  163.6 1.3 copy-start
Sparse Core Ops, SparseCore 0:
  56.6 57.9 all-gather.1
  167.7 73.2 reduce-scatter.1

commit v6 on v5

--- a/solution.py
+++ b/solution.py
@@ -18,7 +18,7 @@
 
 
 def cut_kernel(gain_ref, gate_ref, up_ref, out_ref):
-    rows, width = out_ref.shape[-2:]
+    rows, width = out_ref.shape[-2], out_ref.shape[-1] // 2
     diagonal = lax.broadcasted_iota(jnp.int32, (rows, rows), 0) == lax.broadcasted_iota(
         jnp.int32, (rows, rows), 1
     )
@@ -26,19 +26,19 @@
     for i, w_ref in enumerate((gate_ref, up_ref)):
         for j in range(out_ref.shape[1]):
             cols = w_ref[0, :, j * width : (j + 1) * width]
-            out_ref[0, j, 0, i] = (cols * gain).astype(jnp.bfloat16)
+            out_ref[0, j, 0, :, i * width : (i + 1) * width] = (cols * gain).astype(jnp.bfloat16)
 
 
 def cut(gate, up, gain):
     _, rows, width = gate.shape
-    cols = width // 4
+    cols = width // 2
     weights = pl.BlockSpec((1, rows, width), lambda e: (e, 0, 0))
     return pl.pallas_call(
         cut_kernel,
         grid=(4,),
         in_specs=[pl.BlockSpec((1, rows), lambda e: (0, 0)), weights, weights],
-        out_specs=pl.BlockSpec((1, 4, 1, 2, rows, cols), lambda e: (e % 2, 0, e // 2, 0, 0, 0)),
-        out_shape=jax.ShapeDtypeStruct((2, 4, 2, 2, rows, cols), jnp.bfloat16),
+        out_specs=pl.BlockSpec((1, 4, 1, rows, cols), lambda e: (e % 2, 0, e // 2, 0, 0)),
+        out_shape=jax.ShapeDtypeStruct((2, 4, 2, rows, cols), jnp.bfloat16),
         name="cut",
     )(gain, gate, up)
 
@@ -116,16 +116,16 @@
 
 def place_kernel(at_ref, *refs):
     *pieces, gate_ref, up_ref = refs
-    rows = gate_ref.shape[2]
+    width = gate_ref.shape[2]
     for k, piece in enumerate(pieces):
-        gate_ref[at_ref[k]] = piece[:, :rows]
-        up_ref[at_ref[k]] = piece[:, rows:]
+        gate_ref[at_ref[k]] = piece[:, :width]
+        up_ref[at_ref[k]] = piece[:, width:]
 
 
 def place(at, pieces):
     vmem = pl.BlockSpec(memory_space=pltpu.VMEM)
-    ys, rows, cols = pieces[0].shape
-    out = jax.ShapeDtypeStruct((len(pieces), ys, rows // 2, cols), jnp.bfloat16)
+    rows, cols = pieces[0].shape
+    out = jax.ShapeDtypeStruct((len(pieces), rows, cols // 2), jnp.bfloat16)
     return pl.pallas_call(
         place_kernel,
         in_specs=[pl.BlockSpec(memory_space=pltpu.SMEM)] + [vmem] * len(pieces),
@@ -195,7 +195,8 @@
     for even, odd in zip(*STEPS):
         same, other = (jnp.where(xl == 0, e, o) for e, o in zip(even, odd))
         to = z + jnp.where((z & 1) == xl, same, other)
-        out.append(lax.dynamic_index_in_dim(by_y, (to >> 1) & 1, 1, keepdims=False))
+        half = lax.dynamic_index_in_dim(by_y, (to >> 1) & 1, 1, keepdims=False)
+        out.append(half.reshape(8 * rows, cols))
     return out
 
 
@@ -210,7 +211,7 @@
         same, other = (jnp.where((zl & 1) == 0, e, o) for e, o in zip(STEPS[0][k], STEPS[1][k]))
         z = (4 * gr + zl - same) & 7
         at.append(jnp.where((z >> 2) == xh, z, 4 * gr + zl - other) & 3)
-    return place(jnp.stack(at), arrived)
+    return arrived, at
 
 
 def down_to_servers(down, gr, own):
@@ -220,7 +221,8 @@
         pieces.append(lax.ppermute(down, ("gr", "xh"), pairs))
     blocks = []
     for s in range(4):
-        block = jnp.stack([lax.dynamic_index_in_dim(p, own ^ s, 0, keepdims=False) for p in pieces])
+        block = [lax.dynamic_index_in_dim(p, own ^ s, 0, keepdims=False) for p in pieces]
+        block = jnp.stack(block)
         if s:
             block = lax.ppermute(block, ("xl", "c"), [(u, u ^ s) for u in range(4)])
         blocks.append(block)
@@ -238,17 +240,21 @@
         down_master.astype(jnp.bfloat16), gr, lax.axis_index(("xl", "c"))
     )
     blocks = cut(gate_master, up_master, ffn_gain[None, :])
-    by_core = exchange(blocks.reshape(2, 4, 2, -1, blocks.shape[-1]), "c")
+    by_core = exchange(blocks, "c")
     own_rows = dispatch(expert, ids, prompt)
     pieces = halves(by_core, gr, zl, lax.axis_index("xl"))
     pieces, rows = lax.optimization_barrier((pieces, rows_of_line(own_rows, zl)))
-    gate, up = to_servers(pieces, gr, zl, lax.axis_index("xh"))
+    pieces, at = to_servers(pieces, gr, zl, lax.axis_index("xh"))
+    gate, up = place(jnp.stack(at), pieces)
     gate_serving = gate.reshape(-1, gate.shape[-1])
     up_serving = up.reshape(-1, up.shape[-1])
 
     rows = lax.all_gather(rows, "y", axis=0, tiled=True).reshape(-1, width)
-    gate_part = jnp.dot(rows, gate_serving, preferred_element_type=jnp.float32)
-    up_part = jnp.dot(rows, up_serving, preferred_element_type=jnp.float32)
+    both = 0.0
+    for k, piece in enumerate(pieces):
+        cols = lax.dynamic_slice_in_dim(rows, at[k] * piece.shape[0], piece.shape[0], 1)
+        both = both + jnp.dot(cols, piece, preferred_element_type=jnp.float32)
+    gate_part, up_part = jnp.split(both, 2, axis=1)
     hidden = (jax.nn.silu(gate_part) * up_part).astype(jnp.bfloat16)
     near = jnp.dot(hidden, down_serving[:, :NEAR], preferred_element_type=jnp.float32)
     near = near.astype(jnp.bfloat16).reshape(-1, SLOTS, NEAR)

time: 283 us -> 277 us (0.979)
  blocking collectives: 112 us -> 78.6 us
  waiting for transfers between devices: 47.1 us -> 66.2 us
  starting transfers between devices: 72.1 us -> 81.2 us
    all_to_all x5 -> x4, blocking collectives: 112 us -> 78.6 us  [exchange(): return lax.all_to_all(value, axes, split_axis=0, concat_axis=0, tiled=True)]
    ppermute x4, waiting for transfers between devices: 0.01 us -> 17 us  [to_servers(): arrived.append(lax.ppermute(piece, ('gr', 'zl', 'xh', 'xl'), pairs))]
    all_to_all x1 -> x2, starting transfers between devices: 4.17 us -> 13 us  [exchange(): return lax.all_to_all(value, axes, split_axis=0, concat_axis=0, tiled=True)]
    ppermute x3, waiting for transfers between devices: 20.8 us -> 14 us  [down_to_servers(): block = lax.ppermute(block, ('xl', 'c'), [(u, u ^ s) for u in range(4)])]
    all_to_all x1 -> x2, waiting for transfers between devices: 2.15 us -> 7.96 us  [exchange(): return lax.all_to_all(value, axes, split_axis=0, concat_axis=0, tiled=True)]
    reduce_scatter x1, waiting for transfers between devices: 5.11 us -> 8.18 us  [body(): near = lax.psum_scatter(near, 'y', scatter_dimension=0, tiled=True)]
    dot_general x2 -> x4, matrix products: 5.17 us -> 5.68 us  [body(): both = both + jnp.dot(cols, piece, preferred_element_type=jnp.float32)]
  transfers between devices with their start and end apart: 15 -> 16, of which waited for: 5 -> 8; matrix products, arithmetic and copies ran while one was open for 2% -> 3% of each run, Pallas kernels for 5% -> 5%
where the time goes in v6:
time: 277 us; the launch traced here: 275 us
  starting transfers between devices  81.2 us (29%)
  blocking collectives  78.6 us (28%)
  waiting for transfers between devices  66.2 us (24%)
  Pallas kernels  19 us (7%)
  between operations  14.5 us (5%)
  matrix products  8.74 us (3%)
  other arithmetic  3.63 us (1%)
  local copies, waits for them, and re-layouts  3.57 us (1%)
    all_to_all x4, blocking collectives, exchange(): return lax.all_to_all(value, axes, split_axis=0, concat_axis=0, tiled=True)  78.6 us
    ppermute x4, starting transfers between devices, to_servers(): arrived.append(lax.ppermute(piece, ('gr', 'zl', 'xh', 'xl'), pairs))  23.6 us
    ppermute x3, starting transfers between devices, down_to_servers(): block = lax.ppermute(block, ('xl', 'c'), [(u, u ^ s) for u in range(4)])  20.2 us
    ppermute x4, waiting for transfers between devices, to_servers(): arrived.append(lax.ppermute(piece, ('gr', 'zl', 'xh', 'xl'), pairs))  17 us
    ppermute x3, waiting for transfers between devices, down_to_servers(): block = lax.ppermute(block, ('xl', 'c'), [(u, u ^ s) for u in range(4)])  14 us
    all_to_all x2, starting transfers between devices, exchange(): return lax.all_to_all(value, axes, split_axis=0, concat_axis=0, tiled=True)  13 us
    ppermute x2, starting transfers between devices, down_to_servers(): pieces.append(lax.ppermute(down, ('gr', 'xh'), pairs))  12.6 us
    ppermute x3, starting transfers between devices, rows_of_line(): behind.append(lax.ppermute(rows, 'zl', pairs))  11.7 us
  transfers between devices with their start and end apart: 16, of which 8 were waited for; matrix products, arithmetic and copies ran while one was open for 3% of the time, Pallas kernels for 5%

profile of v6, /device:TPU:1, one launch (start us, length us, event | category | flops | bytes accessed | tf_op | source)
XLA Modules:
  0.0 275.4 jit_solution(6272579556766228958)
XLA Ops:
  7.2 3.8 %cut.1 = bf16[2,4,2,64,512]{4,3,2,1,0:T(8,128)(2,1)} custom-call(f32[1,64]{1,0:T(1,128)} %bitcast.61, f32[4,64,1024]{2,1,0:T(8,128)} %gate_ref.1, f32[4,64,1024]{2,1,0:T(8,128)} %up_ref.1), custom_call_target="tpu_custom_call" | custom-call | tf_op jit(solution)/shard_map/cut/pallas_call | solution.py:36
  10.9 13.0 %all_to_all.30 = bf16[2,4,2,64,512]{4,3,2,1,0:T(8,128)(2,1)} all-to-all(bf16[2,4,2,64,512]{4,3,2,1,0:T(8,128)(2,1)} %cut.1), channel_id=1, replica_groups=mesh['gr'=2,'zl'=4,'y'=8,'xh'=2,'xl'=2,'c'=2] {'c'}, dimensions={0} | all-to-all | bytes 2097152 | tf_op jit(solution)/shard_map/all_to_all | solution.py:177
  24.0 4.0 %all-to-all-start.1 = ((bf16[16,64,512]{2,1,0:T(8,128)(2,1)}), bf16[16,64,512]{2,1,0:T(8,128)(2,1)S(1)}, u32[]{:S(2)}, u32[]{:S(2)}) async-start(bf16[16,64,512]{2,1,0:T(8,128)(2,1)} %bitcast.5), calls=%async_computation.1 | async-start | bytes 2097152 | tf_op jit(solution)/shard_map/all_to_all | solution.py:177
  28.0 0.0 all-gather.2.cloned.1.call-start
  28.1 2.1 dispatch.1.refs_0_
  30.2 7.6 %collective-permute-start = (bf16[32,2048]{1,0:T(8,128)(2,1)}, bf16[32,2048]{1,0:T(8,128)(2,1)S(1)}, u32[]{:S(2)}, u32[]{:S(2)}) collective-permute-start(bf16[32,2048]{1,0:T(8,128)(2,1)} %dispatch.1.refs_0_), channel_id=1, source_target_pairs={{0,192},{64,0},{128,64},{192,128},{1,193},{65,1},{129,65},{193,129... | collective-permute-start | bytes 393224 | tf_op jit(solution)/shard_map/ppermute | solution.py:185
  37.8 1.9 collective-permute-start.1
  39.7 2.2 collective-permute-start.2
  42.0 0.0 collective-permute-done.refs_1_
  42.0 0.0 copy-start.7
  42.0 8.4 %collective-permute-done.1.refs_2_ = bf16[32,2048]{1,0:T(8,128)(2,1)S(1)} collective-permute-done((bf16[32,2048]{1,0:T(8,128)(2,1)}, bf16[32,2048]{1,0:T(8,128)(2,1)S(1)}, u32[]{:S(2)}, u32[]{:S(2)}) %collective-permute-start.1) | collective-permute-done | bytes 131104 | tf_op jit(solution)/shard_map/ppermute | solution.py:185
  50.4 0.0 collective-permute-done.2.refs_3_
  50.4 0.6 copy-done.8
  51.0 0.0 copy-done.9
  51.1 1.9 line_up.1
  53.0 2.2 all-to-all-done.1
  55.2 1.2 constant_dynamic-slice_fusion.8
  56.4 0.0 all-gather.2.cloned.1.call-update
  56.4 0.0 reduce-scatter.2.cloned.1.call-start
  56.5 0.5 copy-done.6
  57.0 0.1 convert_element_type.77
  57.0 0.7 collective-permute-start.7
  57.7 11.9 %collective-permute-start.8 = (bf16[4,256,256]{2,1,0:T(8,128)(2,1)S(1)}, bf16[4,256,256]{2,1,0:T(8,128)(2,1)S(1)}, u32[]{:S(2)}, u32[]{:S(2)}) collective-permute-start(bf16[4,256,256]{2,1,0:T(8,128)(2,1)S(1)} %convert_element_type.77), channel_id=1, source_target_pairs={{0,256},{4,0},{256,260},{260,4},{1,257},{5,1},{257,261},{261,5},{2... | collective-permute-start | bytes 1572872 | tf_op jit(solution)/shard_map/ppermute | solution.py:221
  69.6 0.0 collective-permute-done.7
  69.7 10.6 %collective-permute-done.8 = bf16[4,256,256]{2,1,0:T(8,128)(2,1)S(1)} collective-permute-done((bf16[4,256,256]{2,1,0:T(8,128)(2,1)S(1)}, bf16[4,256,256]{2,1,0:T(8,128)(2,1)S(1)}, u32[]{:S(2)}, u32[]{:S(2)}) %collective-permute-start.8) | collective-permute-done | bytes 524320 | tf_op jit(solution)/shard_map/ppermute | solution.py:221
  80.3 14.5 %collective-permute-start.9 = (bf16[2,256,256]{2,1,0:T(8,128)(2,1)S(1)}, bf16[2,256,256]{2,1,0:T(8,128)(2,1)S(1)}, u32[]{:S(2)}, u32[]{:S(2)}) collective-permute-start(bf16[2,256,256]{2,1,0:T(8,128)(2,1)S(1)} %pad_maximum_fusion.1), channel_id=1, source_target_pairs={{0,1},{1,0},{2,3},{3,2},{4,5},{5,4},{6,7},{7,6},{8,9},{9,8},{10,11... | collective-permute-start | bytes 786440 | tf_op jit(solution)/shard_map/ppermute | solution.py:227
  94.8 8.1 %collective-permute-start.3 = (bf16[512,512]{1,0:T(8,128)(2,1)}, bf16[512,512]{1,0:T(8,128)(2,1)S(1)}, u32[]{:S(2)}, u32[]{:S(2)}) collective-permute-start(bf16[512,512]{1,0:T(8,128)(2,1)} %bitcast.7), channel_id=1, source_target_pairs={{0,256},{2,64},{4,258},{6,66},{64,0},{66,320},{68,2},{70,322},{128... | collective-permute-start | bytes 1572872 | tf_op jit(solution)/shard_map/ppermute | solution.py:210
  103.0 1.9 collective-permute-start.10
  105.0 3.8 %collective-permute-start.11 = (bf16[2,256,256]{2,1,0:T(8,128)(2,1)S(1)}, bf16[2,256,256]{2,1,0:T(8,128)(2,1)S(1)}, u32[]{:S(2)}, u32[]{:S(2)}) collective-permute-start(bf16[2,256,256]{2,1,0:T(8,128)(2,1)S(1)} %pad_maximum_fusion.3), channel_id=1, source_target_pairs={{0,3},{1,2},{2,1},{3,0},{4,7},{5,6},{6,5},{7,4},{8,11},{9,10},{10,... | collective-permute-start | bytes 786440 | tf_op jit(solution)/shard_map/ppermute | solution.py:227
  108.9 0.6 pad_add_fusion.1.at_ref
  109.5 1.7 collective-permute-start.4
  111.2 0.0 collective-permute-done.9
  111.2 1.4 collective-permute-done.10
  112.6 12.6 %collective-permute-done.11 = bf16[2,256,256]{2,1,0:T(8,128)(2,1)S(1)} collective-permute-done((bf16[2,256,256]{2,1,0:T(8,128)(2,1)S(1)}, bf16[2,256,256]{2,1,0:T(8,128)(2,1)S(1)}, u32[]{:S(2)}, u32[]{:S(2)}) %collective-permute-start.11) | collective-permute-done | bytes 262176 | tf_op jit(solution)/shard_map/ppermute | solution.py:227
  125.2 1.1 pad_maximum_fusion.blocks_ref
  126.3 5.9 %place_cols.1 = bf16[256,2048]{1,0:T(8,128)(2,1)} custom-call(s32[2]{0:T(128)} %pad_add_fusion.1.at_ref, bf16[4,2,256,256]{3,2,1,0:T(8,128)(2,1)} %pad_maximum_fusion.blocks_ref), custom_call_target="tpu_custom_call" | custom-call | tf_op jit(solution)/shard_map/place_cols/pallas_call | solution.py:144
  132.2 2.2 collective-permute-start.5
  134.4 11.6 %collective-permute-start.6 = (bf16[512,512]{1,0:T(8,128)(2,1)S(1)}, bf16[512,512]{1,0:T(8,128)(2,1)S(1)}, u32[]{:S(2)}, u32[]{:S(2)}) collective-permute-start(bf16[512,512]{1,0:T(8,128)(2,1)S(1)} %bitcast.54), channel_id=1, source_target_pairs={{0,384},{2,448},{4,386},{6,450},{64,128},{66,192},{68,130},{70,194... | collective-permute-start | bytes 1572872 | tf_op jit(solution)/shard_map/ppermute | solution.py:210
  146.0 0.0 collective-permute-done.3.refs_0_
  146.0 0.0 all-gather.2.cloned.1.call-done
  146.0 2.1 fusion.9
  148.2 0.0 collective-permute-done.4.refs_1_
  148.2 2.1 fusion.7
  150.3 17.0 %collective-permute-done.5.refs_2_ = bf16[512,512]{1,0:T(8,128)(2,1)S(1)} collective-permute-done((bf16[512,512]{1,0:T(8,128)(2,1)}, bf16[512,512]{1,0:T(8,128)(2,1)S(1)}, u32[]{:S(2)}, u32[]{:S(2)}) %collective-permute-start.5) | collective-permute-done | bytes 524320 | tf_op jit(solution)/shard_map/ppermute | solution.py:210
  167.3 0.7 fusion.5
  168.1 0.1 copy-done.5
  168.1 0.7 add_add_fusion
  168.9 0.1 copy-done.2
  168.9 0.3 fusion
  169.3 0.9 copy-done
  170.2 2.6 convolution_convert_fusion
  172.8 0.0 reduce-scatter.2.cloned.1.call-update
  172.9 0.4 convolution_convert_fusion.1
  173.3 32.8 %all_to_all.31 = bf16[4,256,512]{2,1,0:T(8,128)(2,1)S(1)} all-to-all(bf16[4,256,512]{2,1,0:T(8,128)(2,1)S(1)} %bitcast.46), channel_id=1, replica_groups=mesh['gr'=2,'zl'=4,'y'=8,'xh'=2,'xl'=2,'c'=2] {'zl'}, dimensions={0} | all-to-all | bytes 2097152 | tf_op jit(solution)/shard_map/all_to_all | solution.py:177
  206.1 0.1 add_convert_fusion
  206.2 20.2 %all_to_all.32.far_ref = bf16[8,32,512]{2,1,0:T(8,128)(2,1)} all-to-all(bf16[8,32,512]{2,1,0:T(8,128)(2,1)S(1)} %bitcast.53), channel_id=1, replica_groups=mesh['gr'=2,'zl'=4,'y'=8,'xh'=2,'xl'=2,'c'=2] {'y'}, dimensions={0} | all-to-all | bytes 524288 | tf_op jit(solution)/shard_map/all_to_all | solution.py:177
  226.4 8.2 %reduce-scatter.2.cloned.1.call-done = bf16[4,32,1536]{2,1,0:T(8,128)(2,1)} async-done(((bf16[32,32,1536]{2,1,0:T(8,128)(2,1)}), bf16[4,32,1536]{2,1,0:T(8,128)(2,1)}) %reduce-scatter.2.cloned.1.call-update) | async-done | bytes 393232 | tf_op jit(solution)/shard_map/reduce_scatter | solution.py:261
  234.6 12.7 %all_to_all.33.near_ref = bf16[4,32,1536]{2,1,0:T(8,128)(2,1)} all-to-all(bf16[4,32,1536]{2,1,0:T(8,128)(2,1)} %reduce-scatter.2.cloned.1.call-done), channel_id=1, replica_groups=mesh['gr'=2,'zl'=4,'y'=8,'xh'=2,'xl'=2,'c'=2] {'zl'}, dimensions={0} | all-to-all | bytes 786432 | tf_op jit(solution)/shard_map/all_to_all | solution.py:177
  247.2 2.4 combine.1
  249.6 9.0 %all-to-all-start.5 = ((bf16[8,16,2048]{2,1,0:T(8,128)(2,1)}), bf16[8,16,2048]{2,1,0:T(8,128)(2,1)S(1)}, u32[]{:S(2)}, u32[]{:S(2)}) async-start(bf16[8,16,2048]{2,1,0:T(8,128)(2,1)} %bitcast.52), calls=%async_computation.6 | async-start | bytes 1048576 | tf_op jit(solution)/shard_map/all_to_all | solution.py:177
  258.6 0.6 pad_add_fusion.at_ref
  259.1 3.0 %place.1 = (bf16[4,512,256]{2,1,0:T(8,128)(2,1)}, bf16[4,512,256]{2,1,0:T(8,128)(2,1)}) custom-call(s32[4]{0:T(128)} %pad_add_fusion.at_ref, bf16[512,512]{1,0:T(8,128)(2,1)} %copy-done.3, bf16[512,512]{1,0:T(8,128)(2,1)} %copy-done.4, bf16[512,512]{1,0:T(8,128)(2,1)} %copy-done.5, bf16[512,512]{1,0:T(8,128)(2,1)} %copy-done.2), custom_call_target="tpu_custom_call" | custom-call | tf_op jit(solution)/shard_map/place/pallas_call | solution.py:129
  262.1 5.8 %all-to-all-done.5 = bf16[8,16,2048]{2,1,0:T(8,128)(2,1)S(1)} async-done(((bf16[8,16,2048]{2,1,0:T(8,128)(2,1)}), bf16[8,16,2048]{2,1,0:T(8,128)(2,1)S(1)}, u32[]{:S(2)}, u32[]{:S(2)}) %all-to-all-start.5) | async-done | bytes 524320 | tf_op jit(solution)/shard_map/all_to_all | solution.py:177
  267.9 0.7 fusion.13
  (21 shorter events, 0.3 us)
Async XLA Ops:
  24.0 31.2 %all-to-all-start.1 = ((bf16[16,64,512]{2,1,0:T(8,128)(2,1)}), bf16[16,64,512]{2,1,0:T(8,128)(2,1)S(1)}, u32[]{:S(2)}, u32[]{:S(2)}) async-start(bf16[16,64,512]{2,1,0:T(8,128)(2,1)} %bitcast.5), calls=%async_computation.1 | async-start | bytes 2097152 | tf_op jit(solution)/shard_map/all_to_all | solution.py:177
  28.0 118.0 %all-gather.2.cloned.1.call-start = ((), (), s32[]{:S(2)}) async-start(), calls=%async_computation.7 | async-start | bytes 4718592 | tf_op jit(solution)/shard_map/all_gather | solution.py:252
  30.2 11.8 %collective-permute-start = (bf16[32,2048]{1,0:T(8,128)(2,1)}, bf16[32,2048]{1,0:T(8,128)(2,1)S(1)}, u32[]{:S(2)}, u32[]{:S(2)}) collective-permute-start(bf16[32,2048]{1,0:T(8,128)(2,1)} %dispatch.1.refs_0_), channel_id=1, source_target_pairs={{0,192},{64,0},{128,64},{192,128},{1,193},{65,1},{129,65},{193,129... | collective-permute-start | bytes 393224 | tf_op jit(solution)/shard_map/ppermute | solution.py:185
  37.8 12.6 %collective-permute-start.1 = (bf16[32,2048]{1,0:T(8,128)(2,1)}, bf16[32,2048]{1,0:T(8,128)(2,1)S(1)}, u32[]{:S(2)}, u32[]{:S(2)}) collective-permute-start(bf16[32,2048]{1,0:T(8,128)(2,1)} %dispatch.1.refs_0_), channel_id=1, source_target_pairs={{0,128},{64,192},{128,0},{192,64},{1,129},{65,193},{129,1},{193,65... | collective-permute-start | bytes 393224 | tf_op jit(solution)/shard_map/ppermute | solution.py:185
  39.7 10.7 %collective-permute-start.2 = (bf16[32,2048]{1,0:T(8,128)(2,1)}, bf16[32,2048]{1,0:T(8,128)(2,1)S(1)}, u32[]{:S(2)}, u32[]{:S(2)}) collective-permute-start(bf16[32,2048]{1,0:T(8,128)(2,1)} %dispatch.1.refs_0_), channel_id=1, source_target_pairs={{0,64},{64,128},{128,192},{192,0},{1,65},{65,129},{129,193},{193,1... | collective-permute-start | bytes 393224 | tf_op jit(solution)/shard_map/ppermute | solution.py:185
  42.0 8.4 %copy-start.7 = (bf16[32,2048]{1,0:T(8,128)(2,1)}, bf16[32,2048]{1,0:T(8,128)(2,1)S(1)}, u32[]{:S(2)}) copy-start(bf16[32,2048]{1,0:T(8,128)(2,1)S(1)} %collective-permute-done.refs_1_) | copy-start | bytes 393220
  50.4 0.7 copy-start.8
  50.4 0.7 copy-start.9
  55.2 1.8 copy-start.6
  56.4 178.1 %reduce-scatter.2.cloned.1.call-start = ((), (), s32[]{:S(2)}) async-start(), calls=%async_computation.8 | async-start | bytes 3538944 | tf_op jit(solution)/shard_map/reduce_scatter | solution.py:261
  57.0 12.6 %collective-permute-start.7 = (bf16[4,256,256]{2,1,0:T(8,128)(2,1)S(1)}, bf16[4,256,256]{2,1,0:T(8,128)(2,1)S(1)}, u32[]{:S(2)}, u32[]{:S(2)}) collective-permute-start(bf16[4,256,256]{2,1,0:T(8,128)(2,1)S(1)} %convert_element_type.77), channel_id=1, source_target_pairs={{0,0},{4,256},{256,4},{260,260},{1,1},{5,257},{257,5},{261,261},{2... | collective-permute-start | bytes 1572872 | tf_op jit(solution)/shard_map/ppermute | solution.py:221
  57.7 22.5 %collective-permute-start.8 = (bf16[4,256,256]{2,1,0:T(8,128)(2,1)S(1)}, bf16[4,256,256]{2,1,0:T(8,128)(2,1)S(1)}, u32[]{:S(2)}, u32[]{:S(2)}) collective-permute-start(bf16[4,256,256]{2,1,0:T(8,128)(2,1)S(1)} %convert_element_type.77), channel_id=1, source_target_pairs={{0,256},{4,0},{256,260},{260,4},{1,257},{5,1},{257,261},{261,5},{2... | collective-permute-start | bytes 1572872 | tf_op jit(solution)/shard_map/ppermute | solution.py:221
  80.3 30.8 %collective-permute-start.9 = (bf16[2,256,256]{2,1,0:T(8,128)(2,1)S(1)}, bf16[2,256,256]{2,1,0:T(8,128)(2,1)S(1)}, u32[]{:S(2)}, u32[]{:S(2)}) collective-permute-start(bf16[2,256,256]{2,1,0:T(8,128)(2,1)S(1)} %pad_maximum_fusion.1), channel_id=1, source_target_pairs={{0,1},{1,0},{2,3},{3,2},{4,5},{5,4},{6,7},{7,6},{8,9},{9,8},{10,11... | collective-permute-start | bytes 786440 | tf_op jit(solution)/shard_map/ppermute | solution.py:227
  94.8 51.1 %collective-permute-start.3 = (bf16[512,512]{1,0:T(8,128)(2,1)}, bf16[512,512]{1,0:T(8,128)(2,1)S(1)}, u32[]{:S(2)}, u32[]{:S(2)}) collective-permute-start(bf16[512,512]{1,0:T(8,128)(2,1)} %bitcast.7), channel_id=1, source_target_pairs={{0,256},{2,64},{4,258},{6,66},{64,0},{66,320},{68,2},{70,322},{128... | collective-permute-start | bytes 1572872 | tf_op jit(solution)/shard_map/ppermute | solution.py:210
  103.0 9.6 %collective-permute-start.10 = (bf16[2,256,256]{2,1,0:T(8,128)(2,1)S(1)}, bf16[2,256,256]{2,1,0:T(8,128)(2,1)S(1)}, u32[]{:S(2)}, u32[]{:S(2)}) collective-permute-start(bf16[2,256,256]{2,1,0:T(8,128)(2,1)S(1)} %pad_maximum_fusion.2), channel_id=1, source_target_pairs={{0,2},{1,3},{2,0},{3,1},{4,6},{5,7},{6,4},{7,5},{8,10},{9,11},{10,... | collective-permute-start | bytes 786440 | tf_op jit(solution)/shard_map/ppermute | solution.py:227
  105.0 20.2 %collective-permute-start.11 = (bf16[2,256,256]{2,1,0:T(8,128)(2,1)S(1)}, bf16[2,256,256]{2,1,0:T(8,128)(2,1)S(1)}, u32[]{:S(2)}, u32[]{:S(2)}) collective-permute-start(bf16[2,256,256]{2,1,0:T(8,128)(2,1)S(1)} %pad_maximum_fusion.3), channel_id=1, source_target_pairs={{0,3},{1,2},{2,1},{3,0},{4,7},{5,6},{6,5},{7,4},{8,11},{9,10},{10,... | collective-permute-start | bytes 786440 | tf_op jit(solution)/shard_map/ppermute | solution.py:227
  109.5 38.7 %collective-permute-start.4 = (bf16[512,512]{1,0:T(8,128)(2,1)}, bf16[512,512]{1,0:T(8,128)(2,1)S(1)}, u32[]{:S(2)}, u32[]{:S(2)}) collective-permute-start(bf16[512,512]{1,0:T(8,128)(2,1)} %bitcast.8), channel_id=1, source_target_pairs={{0,0},{2,320},{4,2},{6,322},{64,256},{66,64},{68,258},{70,66},{128... | collective-permute-start | bytes 1572872 | tf_op jit(solution)/shard_map/ppermute | solution.py:210
  132.2 35.2 %collective-permute-start.5 = (bf16[512,512]{1,0:T(8,128)(2,1)}, bf16[512,512]{1,0:T(8,128)(2,1)S(1)}, u32[]{:S(2)}, u32[]{:S(2)}) collective-permute-start(bf16[512,512]{1,0:T(8,128)(2,1)} %bitcast.9), channel_id=1, source_target_pairs={{0,128},{2,192},{4,130},{6,194},{64,384},{66,448},{68,386},{70,450... | collective-permute-start | bytes 1572872 | tf_op jit(solution)/shard_map/ppermute | solution.py:210
  134.4 33.7 %collective-permute-start.6 = (bf16[512,512]{1,0:T(8,128)(2,1)S(1)}, bf16[512,512]{1,0:T(8,128)(2,1)S(1)}, u32[]{:S(2)}, u32[]{:S(2)}) collective-permute-start(bf16[512,512]{1,0:T(8,128)(2,1)S(1)} %bitcast.54), channel_id=1, source_target_pairs={{0,384},{2,448},{4,386},{6,450},{64,128},{66,192},{68,130},{70,194... | collective-permute-start | bytes 1572872 | tf_op jit(solution)/shard_map/ppermute | solution.py:210
  146.0 4.3 %copy-start.3 = (bf16[512,512]{1,0:T(8,128)(2,1)}, bf16[512,512]{1,0:T(8,128)(2,1)S(1)}, u32[]{:S(2)}) copy-start(bf16[512,512]{1,0:T(8,128)(2,1)S(1)} %collective-permute-done.3.refs_0_) | copy-start | bytes 1572868
  146.0 21.3 %copy-start.1 = (bf16[32,32,2048]{2,1,0:T(8,128)(2,1)S(1)}, bf16[32,32,2048]{2,1,0:T(8,128)(2,1)}, u32[]{:S(2)}) copy-start(bf16[32,32,2048]{2,1,0:T(8,128)(2,1)} %all-gather.2.cloned.1.call-done) | copy-start | bytes 12582916
  148.2 19.9 %copy-start.4 = (bf16[512,512]{1,0:T(8,128)(2,1)}, bf16[512,512]{1,0:T(8,128)(2,1)S(1)}, u32[]{:S(2)}) copy-start(bf16[512,512]{1,0:T(8,128)(2,1)S(1)} %collective-permute-done.4.refs_1_) | copy-start | bytes 1572868
  167.3 0.8 copy-start.5
  168.1 0.8 copy-start.2
  168.9 1.2 copy-start
  249.6 18.3 %all-to-all-start.5 = ((bf16[8,16,2048]{2,1,0:T(8,128)(2,1)}), bf16[8,16,2048]{2,1,0:T(8,128)(2,1)S(1)}, u32[]{:S(2)}, u32[]{:S(2)}) async-start(bf16[8,16,2048]{2,1,0:T(8,128)(2,1)} %bitcast.52), calls=%async_computation.6 | async-start | bytes 1048576 | tf_op jit(solution)/shard_map/all_to_all | solution.py:177
Sparse Core Ops, SparseCore 0:
  56.5 57.9 all-gather.1
  172.9 61.5 reduce-scatter.1

commit v7 on v6

--- a/solution.py
+++ b/solution.py
@@ -201,17 +201,24 @@
 
 
 def to_servers(pieces, gr, zl, xh):
-    arrived, at = [], []
-    for k, piece in enumerate(pieces):
+    at = []
+    for even, odd in zip(*STEPS):
+        same, other = (jnp.where((zl & 1) == 0, e, o) for e, o in zip(even, odd))
+        z = (4 * gr + zl - same) & 7
+        at.append(jnp.where((z >> 2) == xh, z, 4 * gr + zl - other) & 3)
+
+    def send(value, k, across):
         pairs = []
         for z, e, p in itertools.product(range(8), range(2), range(2)):
             to = (z + STEPS[p][k][(z ^ p) & 1]) % 8
-            pairs.append(((z * 2 + e) * 2 + p, (to * 2 + z // 4) * 2 + e))
-        arrived.append(lax.ppermute(piece, ("gr", "zl", "xh", "xl"), pairs))
-        same, other = (jnp.where((zl & 1) == 0, e, o) for e, o in zip(STEPS[0][k], STEPS[1][k]))
-        z = (4 * gr + zl - same) & 7
-        at.append(jnp.where((z >> 2) == xh, z, 4 * gr + zl - other) & 3)
-    return arrived, at
+            pairs.append(((z * 2 + e) * 2 + (p ^ across), (to * 2 + z // 4) * 2 + e))
+        return lax.ppermute(value, ("gr", "zl", "xh", "xl"), pairs)
+
+    half = pieces[0].shape[1] // 2
+    across = lax.ppermute(pieces[0][:, half:], "xl", [(0, 1), (1, 0)])
+    longest = [send(pieces[0][:, :half], 0, 0), send(across, 0, 1)]
+    arrived = [send(pieces[k], k, 0) for k in range(1, 4)]
+    return [jnp.concatenate(longest, axis=1)] + arrived, at
 
 
 def down_to_servers(down, gr, own):
@@ -226,7 +233,9 @@
         if s:
             block = lax.ppermute(block, ("xl", "c"), [(u, u ^ s) for u in range(4)])
         blocks.append(block)
-    return place_cols(jnp.stack([gr, own]), jnp.stack(blocks))
+    at = jnp.stack([gr, own])
+    blocks = jnp.stack(blocks)
+    return place_cols(at, blocks)
 
 
 def body(prompt, expert_ids, route_weights, gate_master, up_master, down_master, ffn_gain):
@@ -251,7 +260,8 @@
 
     rows = lax.all_gather(rows, "y", axis=0, tiled=True).reshape(-1, width)
     both = 0.0
-    for k, piece in enumerate(pieces):
+    for k in (1, 2, 3, 0):
+        piece = pieces[k]
         cols = lax.dynamic_slice_in_dim(rows, at[k] * piece.shape[0], piece.shape[0], 1)
         both = both + jnp.dot(cols, piece, preferred_element_type=jnp.float32)
     gate_part, up_part = jnp.split(both, 2, axis=1)

time: 277 us -> 274 us (0.989)
  waiting for transfers between devices: 66.2 us -> 55.6 us
  starting transfers between devices: 81.2 us -> 91.7 us
  blocking collectives: 78.6 us -> 73.6 us
    ppermute x3, waiting for transfers between devices: 14 us -> 0.01 us  [down_to_servers(): block = lax.ppermute(block, ('xl', 'c'), [(u, u ^ s) for u in range(4)])]
    ppermute x4 -> x6, starting transfers between devices: 23.6 us -> 35.2 us  [the longest x5 33 us: send(): return lax.ppermute(value, ('gr', 'zl', 'xh', 'xl'), pairs)]
    all_to_all x4, blocking collectives: 78.6 us -> 73.6 us  [exchange(): return lax.all_to_all(value, axes, split_axis=0, concat_axis=0, tiled=True)]
    ppermute x4 -> x6, waiting for transfers between devices: 17 us -> 21.4 us  [the longest x5 21.4 us: send(): return lax.ppermute(value, ('gr', 'zl', 'xh', 'xl'), pairs)]
  transfers between devices with their start and end apart: 16 -> 18, of which waited for: 8 -> 6; matrix products, arithmetic and copies ran while one was open for 3% -> 4% of each run, Pallas kernels for 5% -> 5%
where the time goes in v7:
time: 274 us; the launch traced here: 272 us
  starting transfers between devices  91.7 us (33%)
  blocking collectives  73.6 us (27%)
  waiting for transfers between devices  55.6 us (20%)
  Pallas kernels  19 us (7%)
  between operations  14.5 us (5%)
  matrix products  8.96 us (3%)
  other arithmetic  4.79 us (2%)
  local copies, waits for them, and re-layouts  4.19 us (2%)
    all_to_all x4, blocking collectives, exchange(): return lax.all_to_all(value, axes, split_axis=0, concat_axis=0, tiled=True)  73.6 us
    ppermute x5, starting transfers between devices, send(): return lax.ppermute(value, ('gr', 'zl', 'xh', 'xl'), pairs)  33 us
    ppermute x5, waiting for transfers between devices, send(): return lax.ppermute(value, ('gr', 'zl', 'xh', 'xl'), pairs)  21.4 us
    ppermute x3, starting transfers between devices, down_to_servers(): block = lax.ppermute(block, ('xl', 'c'), [(u, u ^ s) for u in range(4)])  20.2 us
    ppermute x2, starting transfers between devices, down_to_servers(): pieces.append(lax.ppermute(down, ('gr', 'xh'), pairs))  12.6 us
    all_to_all x2, starting transfers between devices, exchange(): return lax.all_to_all(value, axes, split_axis=0, concat_axis=0, tiled=True)  11.9 us
    ppermute x3, starting transfers between devices, rows_of_line(): behind.append(lax.ppermute(rows, 'zl', pairs))  11.7 us
    ppermute x2, waiting for transfers between devices, down_to_servers(): pieces.append(lax.ppermute(down, ('gr', 'xh'), pairs))  10.6 us
  transfers between devices with their start and end apart: 18, of which 6 were waited for; matrix products, arithmetic and copies ran while one was open for 4% of the time, Pallas kernels for 5%

profile of v7, /device:TPU:1, one launch (start us, length us, event | category | flops | bytes accessed | tf_op | source)
XLA Modules:
  0.0 272.4 jit_solution(11254038811891211991)
XLA Ops:
  7.2 3.8 %cut.1 = bf16[2,4,2,64,512]{4,3,2,1,0:T(8,128)(2,1)} custom-call(f32[1,64]{1,0:T(1,128)} %bitcast.62, f32[4,64,1024]{2,1,0:T(8,128)} %gate_ref.1, f32[4,64,1024]{2,1,0:T(8,128)} %up_ref.1), custom_call_target="tpu_custom_call" | custom-call | tf_op jit(solution)/shard_map/cut/pallas_call | solution.py:36
  10.9 13.0 %all_to_all.30 = bf16[2,4,2,64,512]{4,3,2,1,0:T(8,128)(2,1)} all-to-all(bf16[2,4,2,64,512]{4,3,2,1,0:T(8,128)(2,1)} %cut.1), channel_id=1, replica_groups=mesh['gr'=2,'zl'=4,'y'=8,'xh'=2,'xl'=2,'c'=2] {'c'}, dimensions={0} | all-to-all | bytes 2097152 | tf_op jit(solution)/shard_map/all_to_all | solution.py:177
  24.0 4.0 %all-to-all-start.1 = ((bf16[16,64,512]{2,1,0:T(8,128)(2,1)}), bf16[16,64,512]{2,1,0:T(8,128)(2,1)S(1)}, u32[]{:S(2)}, u32[]{:S(2)}) async-start(bf16[16,64,512]{2,1,0:T(8,128)(2,1)} %bitcast.5), calls=%async_computation.1 | async-start | bytes 2097152 | tf_op jit(solution)/shard_map/all_to_all | solution.py:177
  28.0 0.0 all-gather.2.cloned.1.call-start
  28.1 2.1 dispatch.1.refs_0_
  30.2 7.6 %collective-permute-start = (bf16[32,2048]{1,0:T(8,128)(2,1)}, bf16[32,2048]{1,0:T(8,128)(2,1)S(1)}, u32[]{:S(2)}, u32[]{:S(2)}) collective-permute-start(bf16[32,2048]{1,0:T(8,128)(2,1)} %dispatch.1.refs_0_), channel_id=1, source_target_pairs={{0,192},{64,0},{128,64},{192,128},{1,193},{65,1},{129,65},{193,129... | collective-permute-start | bytes 393224 | tf_op jit(solution)/shard_map/ppermute | solution.py:185
  37.8 1.9 collective-permute-start.1
  39.7 2.2 collective-permute-start.2
  42.0 0.0 copy-start.9
  42.0 8.4 %collective-permute-done.1.refs_2_ = bf16[32,2048]{1,0:T(8,128)(2,1)S(1)} collective-permute-done((bf16[32,2048]{1,0:T(8,128)(2,1)}, bf16[32,2048]{1,0:T(8,128)(2,1)S(1)}, u32[]{:S(2)}, u32[]{:S(2)}) %collective-permute-start.1) | collective-permute-done | bytes 131104 | tf_op jit(solution)/shard_map/ppermute | solution.py:185
  50.4 0.6 copy-done.10
  51.0 0.0 copy-done.11
  51.1 1.9 line_up.1
  53.0 2.2 all-to-all-done.1
  55.2 1.2 constant_dynamic-slice_fusion.8
  56.4 0.0 all-gather.2.cloned.1.call-update
  56.4 0.0 reduce-scatter.2.cloned.1.call-start
  56.4 0.2 copy-done.6
  56.7 0.1 convert_element_type.77
  56.7 0.7 collective-permute-start.9
  57.4 11.9 %collective-permute-start.10 = (bf16[4,256,256]{2,1,0:T(8,128)(2,1)S(1)}, bf16[4,256,256]{2,1,0:T(8,128)(2,1)S(1)}, u32[]{:S(2)}, u32[]{:S(2)}) collective-permute-start(bf16[4,256,256]{2,1,0:T(8,128)(2,1)S(1)} %convert_element_type.77), channel_id=1, source_target_pairs={{0,256},{4,0},{256,260},{260,4},{1,257},{5,1},{257,261},{261,5},{2... | collective-permute-start | bytes 1572872 | tf_op jit(solution)/shard_map/ppermute | solution.py:228
  69.3 0.0 collective-permute-done.9
  69.4 10.6 %collective-permute-done.10 = bf16[4,256,256]{2,1,0:T(8,128)(2,1)S(1)} collective-permute-done((bf16[4,256,256]{2,1,0:T(8,128)(2,1)S(1)}, bf16[4,256,256]{2,1,0:T(8,128)(2,1)S(1)}, u32[]{:S(2)}, u32[]{:S(2)}) %collective-permute-start.10) | collective-permute-done | bytes 524320 | tf_op jit(solution)/shard_map/ppermute | solution.py:228
  80.0 14.5 %collective-permute-start.11 = (bf16[2,256,256]{2,1,0:T(8,128)(2,1)S(1)}, bf16[2,256,256]{2,1,0:T(8,128)(2,1)S(1)}, u32[]{:S(2)}, u32[]{:S(2)}) collective-permute-start(bf16[2,256,256]{2,1,0:T(8,128)(2,1)S(1)} %pad_maximum_fusion.1), channel_id=1, source_target_pairs={{0,1},{1,0},{2,3},{3,2},{4,5},{5,4},{6,7},{7,6},{8,9},{9,8},{10,11... | collective-permute-start | bytes 786440 | tf_op jit(solution)/shard_map/ppermute | solution.py:234
  94.6 2.2 collective-permute-start.4
  96.8 3.1 %collective-permute-start.12 = (bf16[2,256,256]{2,1,0:T(8,128)(2,1)S(1)}, bf16[2,256,256]{2,1,0:T(8,128)(2,1)}, u32[]{:S(2)}, u32[]{:S(2)}) collective-permute-start(bf16[2,256,256]{2,1,0:T(8,128)(2,1)S(1)} %pad_maximum_fusion.2), channel_id=1, source_target_pairs={{0,2},{1,3},{2,0},{3,1},{4,6},{5,7},{6,4},{7,5},{8,10},{9,11},{10,... | collective-permute-start | bytes 786440 | tf_op jit(solution)/shard_map/ppermute | solution.py:234
  99.9 2.7 collective-permute-start.13
  102.6 1.7 collective-permute-start.6
  104.3 10.8 %collective-permute-start.3 = (bf16[512,256]{1,0:T(8,128)(2,1)S(1)}, bf16[512,256]{1,0:T(8,128)(2,1)S(1)}, u32[]{:S(2)}, u32[]{:S(2)}) collective-permute-start(bf16[512,256]{1,0:T(8,128)(2,1)S(1)} %get-tuple-element.31), channel_id=1, source_target_pairs={{0,256},{2,64},{4,258},{6,66},{64,0},{66,320},{68,2},{70,322},{128... | collective-permute-start | bytes 786440 | tf_op jit(solution)/shard_map/ppermute | solution.py:215
  115.1 0.7 pad_add_fusion.1.at_ref
  115.8 1.9 collective-permute-start.5
  117.8 0.0 collective-permute-done.12
  117.8 0.0 collective-permute-done.13
  117.8 0.0 copy-start.7
  117.8 2.2 pad_maximum_fusion.blocks_ref
  120.0 5.9 %place_cols.1 = bf16[256,2048]{1,0:T(8,128)(2,1)} custom-call(s32[2]{0:T(128)} %pad_add_fusion.1.at_ref, bf16[4,2,256,256]{3,2,1,0:T(8,128)(2,1)} %pad_maximum_fusion.blocks_ref), custom_call_target="tpu_custom_call" | custom-call | tf_op jit(solution)/shard_map/place_cols/pallas_call | solution.py:144
  125.9 2.5 collective-permute-start.7
  128.4 16.1 %collective-permute-start.8 = (bf16[512,512]{1,0:T(8,128)(2,1)S(1)}, bf16[512,512]{1,0:T(8,128)(2,1)S(1)}, u32[]{:S(2)}, u32[]{:S(2)}) collective-permute-start(bf16[512,512]{1,0:T(8,128)(2,1)S(1)} %bitcast.55), channel_id=1, source_target_pairs={{0,384},{2,448},{4,386},{6,450},{64,128},{66,192},{68,130},{70,194... | collective-permute-start | bytes 1572872 | tf_op jit(solution)/shard_map/ppermute | solution.py:215
  144.4 0.0 collective-permute-done.3
  144.5 1.0 constant_dynamic-update-slice_fusion.refs_0_
  145.5 0.0 all-gather.2.cloned.1.call-done
  145.5 2.3 fusion.6
  147.8 21.4 %collective-permute-done.7.refs_2_ = bf16[512,512]{1,0:T(8,128)(2,1)S(1)} collective-permute-done((bf16[512,512]{1,0:T(8,128)(2,1)S(1)}, bf16[512,512]{1,0:T(8,128)(2,1)S(1)}, u32[]{:S(2)}, u32[]{:S(2)}) %collective-permute-start.7) | collective-permute-done | bytes 524320 | tf_op jit(solution)/shard_map/ppermute | solution.py:215
  169.3 2.1 fusion.4
  171.4 0.7 fusion.2
  172.1 0.1 copy-done.5
  172.2 0.8 add_add_fusion
  173.0 0.0 copy-start
  173.0 0.3 fusion
  173.3 0.9 copy-done
  174.2 2.6 convolution_convert_fusion
  176.8 0.0 reduce-scatter.2.cloned.1.call-update
  176.9 0.4 convolution_convert_fusion.1
  177.3 27.2 %all_to_all.31 = bf16[4,256,512]{2,1,0:T(8,128)(2,1)S(1)} all-to-all(bf16[4,256,512]{2,1,0:T(8,128)(2,1)S(1)} %bitcast.46), channel_id=1, replica_groups=mesh['gr'=2,'zl'=4,'y'=8,'xh'=2,'xl'=2,'c'=2] {'zl'}, dimensions={0} | all-to-all | bytes 2097152 | tf_op jit(solution)/shard_map/all_to_all | solution.py:177
  204.5 0.1 add_convert_fusion
  204.7 19.6 %all_to_all.32.far_ref = bf16[8,32,512]{2,1,0:T(8,128)(2,1)} all-to-all(bf16[8,32,512]{2,1,0:T(8,128)(2,1)S(1)} %bitcast.54), channel_id=1, replica_groups=mesh['gr'=2,'zl'=4,'y'=8,'xh'=2,'xl'=2,'c'=2] {'y'}, dimensions={0} | all-to-all | bytes 524288 | tf_op jit(solution)/shard_map/all_to_all | solution.py:177
  224.2 7.2 %reduce-scatter.2.cloned.1.call-done = bf16[4,32,1536]{2,1,0:T(8,128)(2,1)} async-done(((bf16[32,32,1536]{2,1,0:T(8,128)(2,1)}), bf16[4,32,1536]{2,1,0:T(8,128)(2,1)}) %reduce-scatter.2.cloned.1.call-update) | async-done | bytes 393232 | tf_op jit(solution)/shard_map/reduce_scatter | solution.py:271
  231.4 13.8 %all_to_all.33.near_ref = bf16[4,32,1536]{2,1,0:T(8,128)(2,1)} all-to-all(bf16[4,32,1536]{2,1,0:T(8,128)(2,1)} %reduce-scatter.2.cloned.1.call-done), channel_id=1, replica_groups=mesh['gr'=2,'zl'=4,'y'=8,'xh'=2,'xl'=2,'c'=2] {'zl'}, dimensions={0} | all-to-all | bytes 786432 | tf_op jit(solution)/shard_map/all_to_all | solution.py:177
  245.3 2.4 combine.1
  247.7 7.9 %all-to-all-start.5 = ((bf16[8,16,2048]{2,1,0:T(8,128)(2,1)}), bf16[8,16,2048]{2,1,0:T(8,128)(2,1)S(1)}, u32[]{:S(2)}, u32[]{:S(2)}) async-start(bf16[8,16,2048]{2,1,0:T(8,128)(2,1)} %bitcast.52), calls=%async_computation.6 | async-start | bytes 1048576 | tf_op jit(solution)/shard_map/all_to_all | solution.py:177
  255.5 0.6 pad_add_fusion.at_ref
  256.1 3.0 %place.1 = (bf16[4,512,256]{2,1,0:T(8,128)(2,1)}, bf16[4,512,256]{2,1,0:T(8,128)(2,1)}) custom-call(s32[4]{0:T(128)} %pad_add_fusion.at_ref, bf16[512,512]{1,0:T(8,128)(2,1)} %copy-done.2, bf16[512,512]{1,0:T(8,128)(2,1)} %copy-done.3, bf16[512,512]{1,0:T(8,128)(2,1)} %copy-done.4, bf16[512,512]{1,0:T(8,128)(2,1)} %copy-done.5), custom_call_target="tpu_custom_call" | custom-call | tf_op jit(solution)/shard_map/place/pallas_call | solution.py:129
  259.1 5.8 %all-to-all-done.5 = bf16[8,16,2048]{2,1,0:T(8,128)(2,1)S(1)} async-done(((bf16[8,16,2048]{2,1,0:T(8,128)(2,1)}), bf16[8,16,2048]{2,1,0:T(8,128)(2,1)S(1)}, u32[]{:S(2)}, u32[]{:S(2)}) %all-to-all-start.5) | async-done | bytes 524320 | tf_op jit(solution)/shard_map/all_to_all | solution.py:177
  264.9 0.7 fusion.10
  (32 shorter events, 0.3 us)
Async XLA Ops:
  24.0 31.2 %all-to-all-start.1 = ((bf16[16,64,512]{2,1,0:T(8,128)(2,1)}), bf16[16,64,512]{2,1,0:T(8,128)(2,1)S(1)}, u32[]{:S(2)}, u32[]{:S(2)}) async-start(bf16[16,64,512]{2,1,0:T(8,128)(2,1)} %bitcast.5), calls=%async_computation.1 | async-start | bytes 2097152 | tf_op jit(solution)/shard_map/all_to_all | solution.py:177
  28.0 117.5 %all-gather.2.cloned.1.call-start = ((), (), s32[]{:S(2)}) async-start(), calls=%async_computation.7 | async-start | bytes 4718592 | tf_op jit(solution)/shard_map/all_gather | solution.py:261
  30.2 11.8 %collective-permute-start = (bf16[32,2048]{1,0:T(8,128)(2,1)}, bf16[32,2048]{1,0:T(8,128)(2,1)S(1)}, u32[]{:S(2)}, u32[]{:S(2)}) collective-permute-start(bf16[32,2048]{1,0:T(8,128)(2,1)} %dispatch.1.refs_0_), channel_id=1, source_target_pairs={{0,192},{64,0},{128,64},{192,128},{1,193},{65,1},{129,65},{193,129... | collective-permute-start | bytes 393224 | tf_op jit(solution)/shard_map/ppermute | solution.py:185
  37.8 12.6 %collective-permute-start.1 = (bf16[32,2048]{1,0:T(8,128)(2,1)}, bf16[32,2048]{1,0:T(8,128)(2,1)S(1)}, u32[]{:S(2)}, u32[]{:S(2)}) collective-permute-start(bf16[32,2048]{1,0:T(8,128)(2,1)} %dispatch.1.refs_0_), channel_id=1, source_target_pairs={{0,128},{64,192},{128,0},{192,64},{1,129},{65,193},{129,1},{193,65... | collective-permute-start | bytes 393224 | tf_op jit(solution)/shard_map/ppermute | solution.py:185
  39.7 10.7 %collective-permute-start.2 = (bf16[32,2048]{1,0:T(8,128)(2,1)}, bf16[32,2048]{1,0:T(8,128)(2,1)S(1)}, u32[]{:S(2)}, u32[]{:S(2)}) collective-permute-start(bf16[32,2048]{1,0:T(8,128)(2,1)} %dispatch.1.refs_0_), channel_id=1, source_target_pairs={{0,64},{64,128},{128,192},{192,0},{1,65},{65,129},{129,193},{193,1... | collective-permute-start | bytes 393224 | tf_op jit(solution)/shard_map/ppermute | solution.py:185
  42.0 8.4 %copy-start.9 = (bf16[32,2048]{1,0:T(8,128)(2,1)}, bf16[32,2048]{1,0:T(8,128)(2,1)S(1)}, u32[]{:S(2)}) copy-start(bf16[32,2048]{1,0:T(8,128)(2,1)S(1)} %collective-permute-done.refs_1_) | copy-start | bytes 393220
  50.4 0.7 copy-start.10
  50.4 0.7 copy-start.11
  55.2 1.5 copy-start.6
  56.4 175.1 %reduce-scatter.2.cloned.1.call-start = ((), (), s32[]{:S(2)}) async-start(), calls=%async_computation.8 | async-start | bytes 3538944 | tf_op jit(solution)/shard_map/reduce_scatter | solution.py:271
  56.7 12.6 %collective-permute-start.9 = (bf16[4,256,256]{2,1,0:T(8,128)(2,1)S(1)}, bf16[4,256,256]{2,1,0:T(8,128)(2,1)S(1)}, u32[]{:S(2)}, u32[]{:S(2)}) collective-permute-start(bf16[4,256,256]{2,1,0:T(8,128)(2,1)S(1)} %convert_element_type.77), channel_id=1, source_target_pairs={{0,0},{4,256},{256,4},{260,260},{1,1},{5,257},{257,5},{261,261},{2... | collective-permute-start | bytes 1572872 | tf_op jit(solution)/shard_map/ppermute | solution.py:228
  57.4 22.5 %collective-permute-start.10 = (bf16[4,256,256]{2,1,0:T(8,128)(2,1)S(1)}, bf16[4,256,256]{2,1,0:T(8,128)(2,1)S(1)}, u32[]{:S(2)}, u32[]{:S(2)}) collective-permute-start(bf16[4,256,256]{2,1,0:T(8,128)(2,1)S(1)} %convert_element_type.77), channel_id=1, source_target_pairs={{0,256},{4,0},{256,260},{260,4},{1,257},{5,1},{257,261},{261,5},{2... | collective-permute-start | bytes 1572872 | tf_op jit(solution)/shard_map/ppermute | solution.py:228
  80.0 24.3 %collective-permute-start.11 = (bf16[2,256,256]{2,1,0:T(8,128)(2,1)S(1)}, bf16[2,256,256]{2,1,0:T(8,128)(2,1)S(1)}, u32[]{:S(2)}, u32[]{:S(2)}) collective-permute-start(bf16[2,256,256]{2,1,0:T(8,128)(2,1)S(1)} %pad_maximum_fusion.1), channel_id=1, source_target_pairs={{0,1},{1,0},{2,3},{3,2},{4,5},{5,4},{6,7},{7,6},{8,9},{9,8},{10,11... | collective-permute-start | bytes 786440 | tf_op jit(solution)/shard_map/ppermute | solution.py:234
  94.6 21.2 %collective-permute-start.4 = (bf16[512,256]{1,0:T(8,128)(2,1)S(1)}, bf16[512,256]{1,0:T(8,128)(2,1)}, u32[]{:S(2)}, u32[]{:S(2)}) collective-permute-start(bf16[512,256]{1,0:T(8,128)(2,1)S(1)} %get-tuple-element.30), channel_id=1, source_target_pairs={{0,2},{2,0},{1,3},{3,1},{4,6},{6,4},{5,7},{7,5},{8,10},{10,8},{9,1... | collective-permute-start | bytes 786440 | tf_op jit(solution)/shard_map/ppermute | solution.py:218
  96.8 20.9 %collective-permute-start.12 = (bf16[2,256,256]{2,1,0:T(8,128)(2,1)S(1)}, bf16[2,256,256]{2,1,0:T(8,128)(2,1)}, u32[]{:S(2)}, u32[]{:S(2)}) collective-permute-start(bf16[2,256,256]{2,1,0:T(8,128)(2,1)S(1)} %pad_maximum_fusion.2), channel_id=1, source_target_pairs={{0,2},{1,3},{2,0},{3,1},{4,6},{5,7},{6,4},{7,5},{8,10},{9,11},{10,... | collective-permute-start | bytes 786440 | tf_op jit(solution)/shard_map/ppermute | solution.py:234
  99.9 17.8 %collective-permute-start.13 = (bf16[2,256,256]{2,1,0:T(8,128)(2,1)S(1)}, bf16[2,256,256]{2,1,0:T(8,128)(2,1)S(1)}, u32[]{:S(2)}, u32[]{:S(2)}) collective-permute-start(bf16[2,256,256]{2,1,0:T(8,128)(2,1)S(1)} %pad_maximum_fusion.3), channel_id=1, source_target_pairs={{0,3},{1,2},{2,1},{3,0},{4,7},{5,6},{6,5},{7,4},{8,11},{9,10},{10,... | collective-permute-start | bytes 786440 | tf_op jit(solution)/shard_map/ppermute | solution.py:234
  102.6 42.8 %collective-permute-start.6 = (bf16[512,512]{1,0:T(8,128)(2,1)}, bf16[512,512]{1,0:T(8,128)(2,1)S(1)}, u32[]{:S(2)}, u32[]{:S(2)}) collective-permute-start(bf16[512,512]{1,0:T(8,128)(2,1)} %bitcast.8), channel_id=1, source_target_pairs={{0,0},{2,320},{4,2},{6,322},{64,256},{66,64},{68,258},{70,66},{128... | collective-permute-start | bytes 1572872 | tf_op jit(solution)/shard_map/ppermute | solution.py:215
  104.3 13.4 %copy-start.8 = (bf16[2,256,256]{2,1,0:T(8,128)(2,1)}, bf16[2,256,256]{2,1,0:T(8,128)(2,1)S(1)}, u32[]{:S(2)}) copy-start(bf16[2,256,256]{2,1,0:T(8,128)(2,1)S(1)} %collective-permute-done.11) | copy-start | bytes 786436
  104.3 40.1 %collective-permute-start.3 = (bf16[512,256]{1,0:T(8,128)(2,1)S(1)}, bf16[512,256]{1,0:T(8,128)(2,1)S(1)}, u32[]{:S(2)}, u32[]{:S(2)}) collective-permute-start(bf16[512,256]{1,0:T(8,128)(2,1)S(1)} %get-tuple-element.31), channel_id=1, source_target_pairs={{0,256},{2,64},{4,258},{6,66},{64,0},{66,320},{68,2},{70,322},{128... | collective-permute-start | bytes 786440 | tf_op jit(solution)/shard_map/ppermute | solution.py:215
  115.8 28.7 %collective-permute-start.5 = (bf16[512,256]{1,0:T(8,128)(2,1)}, bf16[512,256]{1,0:T(8,128)(2,1)}, u32[]{:S(2)}, u32[]{:S(2)}) collective-permute-start(bf16[512,256]{1,0:T(8,128)(2,1)} %collective-permute-done.4), channel_id=1, source_target_pairs={{2,256},{0,64},{6,258},{4,66},{66,0},{64,320},{70,2},{68,322},{130... | collective-permute-start | bytes 786440 | tf_op jit(solution)/shard_map/ppermute | solution.py:215
  117.8 8.1 %copy-start.7 = (bf16[8,1,64,512]{3,2,1,0:T(8,128)(2,1)S(1)}, bf16[8,1,64,512]{3,2,1,0:T(8,128)(2,1)}, u32[]{:S(2)}) copy-start(bf16[8,1,64,512]{3,2,1,0:T(8,128)(2,1)} %get-tuple-element.19) | copy-start | bytes 1572868
  125.9 43.4 %collective-permute-start.7 = (bf16[512,512]{1,0:T(8,128)(2,1)S(1)}, bf16[512,512]{1,0:T(8,128)(2,1)S(1)}, u32[]{:S(2)}, u32[]{:S(2)}) collective-permute-start(bf16[512,512]{1,0:T(8,128)(2,1)S(1)} %bitcast.56), channel_id=1, source_target_pairs={{0,128},{2,192},{4,130},{6,194},{64,384},{66,448},{68,386},{70,450... | collective-permute-start | bytes 1572872 | tf_op jit(solution)/shard_map/ppermute | solution.py:215
  128.4 43.0 %collective-permute-start.8 = (bf16[512,512]{1,0:T(8,128)(2,1)S(1)}, bf16[512,512]{1,0:T(8,128)(2,1)S(1)}, u32[]{:S(2)}, u32[]{:S(2)}) collective-permute-start(bf16[512,512]{1,0:T(8,128)(2,1)S(1)} %bitcast.55), channel_id=1, source_target_pairs={{0,384},{2,448},{4,386},{6,450},{64,128},{66,192},{68,130},{70,194... | collective-permute-start | bytes 1572872 | tf_op jit(solution)/shard_map/ppermute | solution.py:215
  145.5 26.7 %copy-start.2 = (bf16[512,512]{1,0:T(8,128)(2,1)}, bf16[512,512]{1,0:T(8,128)(2,1)S(1)}, u32[]{:S(2)}) copy-start(bf16[512,512]{1,0:T(8,128)(2,1)S(1)} %constant_dynamic-update-slice_fusion.refs_0_) | copy-start | bytes 1572868
  145.5 25.9 %copy-start.3 = (bf16[512,512]{1,0:T(8,128)(2,1)}, bf16[512,512]{1,0:T(8,128)(2,1)S(1)}, u32[]{:S(2)}) copy-start(bf16[512,512]{1,0:T(8,128)(2,1)S(1)} %collective-permute-done.6.refs_1_) | copy-start | bytes 1572868
  145.5 25.9 %copy-start.1 = (bf16[32,32,2048]{2,1,0:T(8,128)(2,1)S(1)}, bf16[32,32,2048]{2,1,0:T(8,128)(2,1)}, u32[]{:S(2)}) copy-start(bf16[32,32,2048]{2,1,0:T(8,128)(2,1)} %all-gather.2.cloned.1.call-done) | copy-start | bytes 12582916
  169.3 2.9 %copy-start.4 = (bf16[512,512]{1,0:T(8,128)(2,1)}, bf16[512,512]{1,0:T(8,128)(2,1)S(1)}, u32[]{:S(2)}) copy-start(bf16[512,512]{1,0:T(8,128)(2,1)S(1)} %collective-permute-done.7.refs_2_) | copy-start | bytes 1572868
  171.4 0.8 copy-start.5
  173.0 1.2 copy-start
  247.7 17.2 %all-to-all-start.5 = ((bf16[8,16,2048]{2,1,0:T(8,128)(2,1)}), bf16[8,16,2048]{2,1,0:T(8,128)(2,1)S(1)}, u32[]{:S(2)}, u32[]{:S(2)}) async-start(bf16[8,16,2048]{2,1,0:T(8,128)(2,1)} %bitcast.52), calls=%async_computation.6 | async-start | bytes 1048576 | tf_op jit(solution)/shard_map/all_to_all | solution.py:177
Sparse Core Ops, SparseCore 0:
  56.5 57.9 all-gather.1
  177.0 54.4 reduce-scatter.1
